TPU v7x, 32 devices: a whole 2x2x4 slice. The times are simulated.
32 devices in a mesh: sp: 4 (over z), fs: 4 (over y, core), tp: 2 (over x).
Axes of the slice: x: 2, y: 2, z: 4, core: 2. Of those that a mesh axis runs over, the one named last changes fastest.
Arguments:
- tokens: bfloat16 [4, 4096, 2048], P('fs', 'sp', 'tp'), may hold values from -8 to 8
- norm_gain: float32 [2048], replicated, may hold values from 0.1 to 1.9
- w_query: bfloat16 [2048, 1024], P(('sp', 'fs'), 'tp'), may hold values from -4 to 4
- w_key: bfloat16 [2048, 512], P(('sp', 'fs'), 'tp'), may hold values from -0.16 to 0.16
- w_value: bfloat16 [2048, 512], P(('sp', 'fs'), 'tp'), may hold values from -0.125 to 0.125
- w_conv_in: bfloat16 [2048, 1024], P(('sp', 'fs'), 'tp'), may hold values from -0.125 to 0.125
- w_conv_b: bfloat16 [2048, 1024], P(('sp', 'fs'), 'tp'), may hold values from -0.125 to 0.125
- w_conv_c: bfloat16 [2048, 1024], P(('sp', 'fs'), 'tp'), may hold values from -0.125 to 0.125
- conv_taps: bfloat16 [3, 1024], P(None, 'tp'), may hold values from -3.5 to 3.5
- sink_logits: float32 [16], P('tp'), may hold values from 1 to 5
- w_attn_out: bfloat16 [1024, 2048], P('tp', ('sp', 'fs')), may hold values from -0.375 to 0.375
- w_conv_out: bfloat16 [1024, 2048], P('tp', ('sp', 'fs')), may hold values from -0.125 to 0.125
Outputs:
- mixed: bfloat16 [4, 4096, 2048], P('fs', ('sp', 'tp'))
All inputs are finite; a program needn't handle non-finite values.
Results may differ from a plain program's by a relative error of at most 0.02.
Values may be sent and summed in bfloat16 or wider, within the bound.
A program may use at most 128 MiB of HBM per device.

v0:
```python
import functools

import jax
import jax.numpy as jnp
from jax import lax
from jax.experimental import pallas as pl
from jax.experimental.pallas import tpu as pltpu
from jax.sharding import PartitionSpec as P

HEADS = 16
HEAD = 64
WINDOW = 128
MESH = pl.DeviceIdType.MESH
Z_FIRST = (True, True, False, True)


class Gather:
    def __init__(self, ring, fs, parts):
        self.ring, self.outer, self.parts = ring, fs // 2, parts

    def sends(self, part, key):
        d, o, i = key
        if i == 1:
            return []
        out = []
        heavy_right = (part // 2 + o) % 2 == 0
        right = self.ring // 2 if heavy_right else (self.ring - 1) // 2
        left = self.ring - 1 - right
        if Z_FIRST[part]:
            on_ring, on_outer = o == 0, o == 0
        else:
            on_ring, on_outer = True, o == 0 and d == 0
        if on_ring:
            if d < right:
                out.append(("right", (d + 1, o, 0)))
            if d == 0 and left > 0:
                out.append(("left", (self.ring - 1, o, 0)))
            elif d > right and self.ring - d < left:
                out.append(("left", (d - 1, o, 0)))
        if on_outer:
            for step in range(1, self.outer):
                out.append((("outer", step), (d, step, 0)))
        out.append(("core", (d, o, 1)))
        return out

    def plan(self):
        order, level = [], {}
        frontier = [(0, part, (0, 0, 0)) for part in range(self.parts)]
        while frontier:
            frontier.sort()
            hops, part, key = frontier.pop(0)
            order.append((part, key, self.sends(part, key)))
            for _, there in self.sends(part, key):
                frontier.append((hops + 1, part, there))
        return order


def gather_kernel(gather, n_tp, *refs):
    parts = gather.parts
    own = refs[:parts]
    tok = refs[parts]
    full = refs[parts + 1 : 2 * parts + 1]
    tok_full = refs[2 * parts + 1]
    send_sem, recv_sem, local_sem, tok_send, tok_recv = refs[2 * parts + 2 :]
    n_sp, n_out = gather.ring, gather.outer
    s, f, t = lax.axis_index("sp"), lax.axis_index("fs"), lax.axis_index("tp")
    o, i = f // 2, f % 2

    def device(where):
        if where == "right":
            return (lax.rem(s + 1, n_sp), f, t)
        if where == "left":
            return (lax.rem(s + n_sp - 1, n_sp), f, t)
        if where == "core":
            return (s, o * 2 + (1 - i), t)
        if where[0] == "outer":
            return (s, lax.rem(o + where[1], n_out) * 2 + i, t)
        return (s, f, lax.rem(t + where[1], n_tp))

    barrier = pltpu.get_barrier_semaphore()
    greeted = ["right", "left", "core"]
    greeted += [("outer", k) for k in range(1, n_out)] + [("tp", k) for k in range(1, n_tp)]
    for where in greeted:
        pl.semaphore_signal(barrier, inc=1, device_id=device(where), device_id_type=MESH)
    pl.semaphore_wait(barrier, len(greeted))

    def origin(key):
        d, od, c = key
        src_s = lax.rem(s + n_sp - d, n_sp)
        src_o = lax.rem(o + n_out - od, n_out)
        src_i = i if c == 0 else 1 - i
        return src_s * (2 * n_out) + src_o * 2 + src_i

    cols = tok.shape[1]
    tok_copies = []
    for k in range(1, n_tp):
        copy = pltpu.make_async_remote_copy(
            src_ref=tok,
            dst_ref=tok_full.at[:, pl.ds(pl.multiple_of(t * cols, cols), cols)],
            send_sem=tok_send.at[k],
            recv_sem=tok_recv.at[k],
            device_id=device(("tp", k)),
            device_id_type=MESH,
        )
        copy.start()
        tok_copies.append(copy)
    flat = lambda key: (key[0] * n_out + key[1]) * 2 + key[2]
    copies, arrived, last = [], {}, []
    for part, key, sends in gather.plan():
        rows = own[part].shape[0]
        place = full[part].at[pl.ds(pl.multiple_of(origin(key) * rows, rows), rows)]
        if key == (0, 0, 0):
            source = own[part]
        else:
            source = place
            if sends:
                arrived[(part, key)].wait_recv()
            else:
                last.append(arrived[(part, key)])
        for where, there in sends:
            copy = pltpu.make_async_remote_copy(
                src_ref=source,
                dst_ref=place,
                send_sem=send_sem.at[len(copies)],
                recv_sem=recv_sem.at[part * 2 * n_sp * n_out + flat(there)],
                device_id=device(where),
                device_id_type=MESH,
            )
            copy.start()
            copies.append(copy)
            arrived[(part, there)] = copy
    local = []
    for part in range(parts):
        rows = own[part].shape[0]
        mine = pl.ds(pl.multiple_of(origin((0, 0, 0)) * rows, rows), rows)
        local.append(pltpu.make_async_copy(own[part], full[part].at[mine], local_sem.at[part]))
    mine = pl.ds(pl.multiple_of(t * cols, cols), cols)
    local.append(pltpu.make_async_copy(tok, tok_full.at[:, mine], local_sem.at[parts]))
    for copy in local:
        copy.start()
    for copy in last:
        copy.wait_recv()
    for copy in tok_copies:
        copy.wait()
    for copy in copies:
        copy.wait_send()
    for copy in local:
        copy.wait()


def gather_all(tokens, blocks):
    n_sp, n_fs, n_tp = (lax.axis_size(axis) for axis in ("sp", "fs", "tp"))
    gather = Gather(n_sp, n_fs, len(blocks))
    number = sum(len(sends) for _, _, sends in gather.plan())
    shapes = [jax.ShapeDtypeStruct((n_sp * n_fs * b.shape[0], b.shape[1]), b.dtype) for b in blocks]
    shapes.append(jax.ShapeDtypeStruct((tokens.shape[0], tokens.shape[1] * n_tp), tokens.dtype))
    return pl.pallas_call(
        functools.partial(gather_kernel, gather, n_tp),
        out_shape=shapes,
        in_specs=[pl.BlockSpec(memory_space=pltpu.VMEM)] * (len(blocks) + 1),
        out_specs=[pl.BlockSpec(memory_space=pl.ANY)] * len(shapes),
        scratch_shapes=[
            pltpu.SemaphoreType.DMA((number,)),
            pltpu.SemaphoreType.DMA((len(blocks) * n_sp * n_fs,)),
            pltpu.SemaphoreType.DMA((len(blocks) + 1,)),
            pltpu.SemaphoreType.DMA((n_tp,)),
            pltpu.SemaphoreType.DMA((n_tp,)),
        ],
        compiler_params=pltpu.CompilerParams(collective_id=0, has_side_effects=True),
    )(*blocks, tokens)


def out_kernel(n_tp, chunks, mix, w_out, out, outbox, inbox, send_sem, recv_sem):
    s, f, t = lax.axis_index("sp"), lax.axis_index("fs"), lax.axis_index("tp")
    rows = out.shape[0]
    step = rows // chunks
    peers = [(s, f, lax.rem(t + k, n_tp)) for k in range(1, n_tp)]
    barrier = pltpu.get_barrier_semaphore()
    for peer in peers:
        pl.semaphore_signal(barrier, inc=1, device_id=peer, device_id_type=MESH)
    pl.semaphore_wait(barrier, n_tp - 1)

    def partial(owner, chunk):
        first = pl.multiple_of(owner * rows + chunk * step, step)
        return lax.dot_general(
            mix[pl.ds(first, step), :],
            w_out[...],
            (((1,), (1,)), ((), ())),
            preferred_element_type=jnp.float32,
        ).astype(jnp.bfloat16)

    copies = []
    for chunk in range(chunks):
        here = pl.ds(chunk * step, step)
        for k, peer in enumerate(peers):
            outbox[k, here] = partial(peer[2], chunk)
            copy = pltpu.make_async_remote_copy(
                src_ref=outbox.at[k, here],
                dst_ref=inbox.at[k, here],
                send_sem=send_sem.at[k, chunk],
                recv_sem=recv_sem.at[k, chunk],
                device_id=peer,
                device_id_type=MESH,
            )
            copy.start()
            copies.append(copy)
    for chunk in range(chunks):
        out[pl.ds(chunk * step, step)] = partial(t, chunk)
    for chunk in range(chunks):
        here = pl.ds(chunk * step, step)
        total = out[here].astype(jnp.float32)
        for k in range(n_tp - 1):
            copies[chunk * (n_tp - 1) + k].wait_recv()
            total = total + inbox[k, here].astype(jnp.float32)
        out[here] = total.astype(out.dtype)
    for copy in copies:
        copy.wait_send()


def project_out(mixers, w_out):
    n_tp = lax.axis_size("tp")
    rows, width = mixers.shape[0] // n_tp, w_out.shape[0]
    chunks = 4
    return pl.pallas_call(
        functools.partial(out_kernel, n_tp, chunks),
        out_shape=jax.ShapeDtypeStruct((rows, width), jnp.bfloat16),
        in_specs=[pl.BlockSpec(memory_space=pltpu.VMEM)] * 2,
        out_specs=pl.BlockSpec(memory_space=pltpu.VMEM),
        scratch_shapes=[
            pltpu.VMEM((n_tp - 1, rows, width), jnp.bfloat16),
            pltpu.VMEM((n_tp - 1, rows, width), jnp.bfloat16),
            pltpu.SemaphoreType.DMA((n_tp - 1, chunks)),
            pltpu.SemaphoreType.DMA((n_tp - 1, chunks)),
        ],
        compiler_params=pltpu.CompilerParams(collective_id=1, has_side_effects=True),
    )(mixers, w_out)


def shifted(block, axis, distance):
    devices = range(lax.axis_size(axis))
    route = [(i - distance, i) for i in devices if i - distance in devices]
    return lax.ppermute(block, axis, route)


def norm_rows(tokens, norm_gain):
    values = tokens.astype(jnp.float32)
    average = jnp.mean(values, axis=-1, keepdims=True)
    centred = values - average
    variance = jnp.mean(centred * centred, axis=-1, keepdims=True)
    return (centred * lax.rsqrt(variance + 1e-05) * norm_gain).astype(jnp.bfloat16)


def attend(queries, keys_values, earlier_rows, sink_logits, head_base, row_base):
    row_total = queries.shape[0]
    kv_cols = keys_values.shape[1] // 2
    kv_here = kv_cols // HEAD
    heads_here = queries.shape[1] // HEAD
    group = heads_here // kv_here
    keys_all = jnp.concatenate([earlier_rows, keys_values], axis=0)
    block_rows = min(512, row_total)
    head_ids = head_base + jnp.arange(heads_here, dtype=jnp.int32)
    slopes = jnp.exp2(-8.0 * (head_ids + 1).astype(jnp.float32) / HEADS).reshape(kv_here, group)[
        :, :, None, None
    ]
    sinks = sink_logits.reshape(kv_here, group)[:, :, None, None]
    row_ids = jnp.arange(block_rows, dtype=jnp.int32)[:, None]
    col_ids = jnp.arange(block_rows + WINDOW, dtype=jnp.int32)[None, :]
    distance = WINDOW + row_ids - col_ids
    outputs = []
    for block in range(row_total // block_rows):
        first_row = block * block_rows
        query_block = queries[first_row : first_row + block_rows].reshape(
            block_rows, kv_here, group, HEAD
        )
        band = keys_all[first_row : first_row + block_rows + WINDOW]
        band_keys = band[:, :kv_cols].reshape(block_rows + WINDOW, kv_here, HEAD)
        band_values = band[:, kv_cols:].reshape(block_rows + WINDOW, kv_here, HEAD)
        scores = jnp.einsum(
            "qkgd,skd->kgqs", query_block, band_keys, preferred_element_type=jnp.float32
        ) * HEAD ** (-0.5)
        scores = scores - slopes * distance.astype(jnp.float32)
        key_place = row_base + first_row - WINDOW + col_ids
        keep = (distance >= 0) & (distance < WINDOW) & (key_place >= 0)
        scores = jnp.where(keep, scores, -jnp.inf)
        highest = jnp.maximum(jnp.max(scores, axis=-1, keepdims=True), sinks)
        raised = jnp.exp(scores - highest)
        denominator = jnp.sum(raised, axis=-1, keepdims=True) + jnp.exp(sinks - highest)
        weights = (raised / denominator).astype(jnp.bfloat16)
        mixed = jnp.einsum(
            "kgqs,skd->qkgd", weights, band_values, preferred_element_type=jnp.float32
        )
        outputs.append(mixed.astype(jnp.bfloat16).reshape(block_rows, heads_here * HEAD))
    return jnp.concatenate(outputs, axis=0)


def on_device(
    tokens,
    norm_gain,
    w_query,
    w_key,
    w_value,
    w_conv_in,
    w_conv_b,
    w_conv_c,
    conv_taps,
    sink_logits,
    w_attn_out,
    w_conv_out,
):
    blocks = (
        jnp.concatenate([w_query, w_key, w_value], axis=1),
        jnp.concatenate([w_conv_in, w_conv_b], axis=1),
        w_conv_c,
        jnp.concatenate([w_attn_out, w_conv_out], axis=0).T,
    )
    w_qkv, w_conv, w_gate, w_out, gathered = gather_all(tokens[0], blocks)
    normed = norm_rows(gathered, norm_gain)
    row_total = normed.shape[0]
    q_cols, kv_cols, conv_cols = w_query.shape[1], w_key.shape[1], w_conv_in.shape[1]
    qkv = jnp.dot(normed, w_qkv, preferred_element_type=jnp.float32).astype(jnp.bfloat16)
    conv = jnp.dot(normed, w_conv, preferred_element_type=jnp.float32).astype(jnp.bfloat16)
    queries, keys_values = qkv[:, :q_cols], qkv[:, q_cols:]
    inner, gate_b = conv[:, :conv_cols], conv[:, conv_cols:]
    gate_c = jnp.dot(normed, w_gate, preferred_element_type=jnp.float32).astype(jnp.bfloat16)
    product = (gate_c.astype(jnp.float32) * inner.astype(jnp.float32)).astype(jnp.bfloat16)
    earlier_kv, earlier_product = shifted(
        (keys_values[row_total - WINDOW :], product[row_total - 2 :]), "sp", 1
    )
    heads_here = queries.shape[1] // HEAD
    head_base = lax.axis_index("tp") * heads_here
    row_base = lax.axis_index("sp") * row_total
    attended = attend(queries, keys_values, earlier_kv, sink_logits, head_base, row_base)
    taps = conv_taps.astype(jnp.float32)
    padded = jnp.concatenate([earlier_product, product], axis=0).astype(jnp.float32)
    filtered = (
        taps[0] * padded[0:row_total]
        + taps[1] * padded[1 : row_total + 1]
        + taps[2] * padded[2 : row_total + 2]
    )
    conv_out = (gate_b.astype(jnp.float32) * filtered).astype(jnp.bfloat16)
    mixers = jnp.concatenate([attended, conv_out], axis=1)
    summed = project_out(mixers, w_out)
    return summed[None]


def solution(mesh):
    placed = (
        P("fs", "sp", "tp"),
        P(),
        P(("sp", "fs"), "tp"),
        P(("sp", "fs"), "tp"),
        P(("sp", "fs"), "tp"),
        P(("sp", "fs"), "tp"),
        P(("sp", "fs"), "tp"),
        P(("sp", "fs"), "tp"),
        P(None, "tp"),
        P("tp"),
        P("tp", ("sp", "fs")),
        P("tp", ("sp", "fs")),
    )
    return jax.shard_map(
        on_device,
        mesh=mesh,
        in_specs=placed,
        out_specs=P("fs", ("sp", "tp"), None),
        check_vma=False,
    )
```

profile of v0, /device:TPU:0, one launch (start us, length us, event | category | flops | bytes accessed | tf_op | source)
XLA Modules:
  0.0 211.4 jit_solution(3079401443765181897)
XLA Ops:
  0.0 1.0 copy.19
  1.0 1.0 copy.20
  2.0 0.7 maximum_bitcast_fusion.refs_3_
  2.8 1.9 pad_maximum_fusion.3
  4.7 82.0 %shard_map.118 = (bf16[2048,1024]{1,0:T(8,128)(2,1)}, bf16[2048,1024]{1,0:T(8,128)(2,1)}, bf16[2048,512]{1,0:T(8,128)(2,1)}, bf16[2048,1024]{1,0:T(8,128)(2,1)}, bf16[1024,2048]{1,0:T(8,128)(2,1)}) custom-call(bf16[128,1024]{1,0:T(8,128)(2,1)} %get-tuple-element.33.refs_0_, bf16[128,1024]{1,0:T(8,128)(2,1)} %get-tuple-element.34.refs_1_, ...), custom_call_target="tpu_custom_call" | custom-call | tf_op jit(solution)/shard_map/pallas_call | solution.py:157
  86.8 0.0 copy-start.12
  86.8 3.0 %convert_reduce_fusion = f32[1024]{0:T(1024)S(1)} fusion(bf16[1024,2048]{1,0:T(8,128)(2,1)} %get-tuple-element.10), kind=kLoop, calls=%fused_computation.3 | loop fusion | flops 4193280 | bytes 4198400 | tf_op jit(solution)/shard_map/reduce_sum | solution.py:247
  89.7 0.5 copy-done
  90.2 1.2 fusion.6
  91.5 1.6 fusion.8
  93.1 0.5 copy-done.14
  93.6 4.7 %convolution_convert_fusion = bf16[1024,1024]{1,0:T(8,128)(2,1)S(1)} fusion(bf16[1024,2048]{1,0:T(8,128)(2,1)S(1)} %fusion.8, bf16[2048,1024]{1,0:T(8,128)(2,1)S(1)} %copy-done.14), kind=kOutput, calls=%fused_computation.30 | convolution fusion | flops 4296015872 | bytes 10485760 | tf_op jit(solution)/shard_map/dot_general | solution.py:321
  98.3 0.0 copy-start.5
  98.4 2.3 %multiply_convert_fusion = bf16[1024,512]{1,0:T(8,128)(2,1)S(1)} fusion(bf16[1024,2048]{1,0:T(8,128)(2,1)S(1)} %fusion.8, bf16[2048,512]{1,0:T(8,128)(2,1)S(1)} %copy-done.15, bf16[1024,1024]{1,0:T(8,128)(2,1)S(1)} %convolution_convert_fusion), kind=kOutput, calls=%fused_computation.29 | convolution fusion | flops 2150105088 | bytes 8388608 | tf_op jit(solution)/shard_map/dot_general | solution.py:324
  100.7 0.6 slice.88
  101.3 3.9 %collective-permute-start.1 = (bf16[2,512]{1,0:T(2,128)(2,1)}, bf16[2,512]{1,0:T(2,128)(2,1)}, u32[]{:S(2)}, u32[]{:S(2)}) collective-permute-start(bf16[2,512]{1,0:T(2,128)(2,1)} %slice.88), channel_id=1, source_target_pairs={{0,8},{8,16},{16,24},{1,9},{9,17},{17,25},{2,10},{10,18},{18,26},{... | collective-permute-start | bytes 6152 | tf_op jit(solution)/shard_map/ppermute | solution.py:242
  105.2 0.0 copy-done.13
  105.2 4.8 %convolution_convert_fusion.1 = bf16[1024,1024]{0,1:T(8,128)(2,1)S(1)} fusion(bf16[1024,2048]{1,0:T(8,128)(2,1)S(1)} %fusion.8, bf16[2048,1024]{1,0:T(8,128)(2,1)S(1)} %copy-done.13), kind=kOutput, calls=%fused_computation.31 | convolution fusion | flops 4296015872 | bytes 10485760 | tf_op jit(solution)/shard_map/dot_general | solution.py:320
  110.0 0.0 copy-start.2
  110.0 0.8 slice.79
  110.8 3.1 %collective-permute-start = (bf16[128,512]{0,1:T(8,128)(2,1)}, bf16[128,512]{0,1:T(8,128)(2,1)S(1)}, u32[]{:S(2)}, u32[]{:S(2)}) collective-permute-start(bf16[128,512]{0,1:T(8,128)(2,1)} %slice.79), channel_id=1, source_target_pairs={{0,8},{8,16},{16,24},{1,9},{9,17},{17,25},{2,10},{10,18},{18,26},{... | collective-permute-start | bytes 393224 | tf_op jit(solution)/shard_map/ppermute | solution.py:242
  114.0 0.9 fusion.30
  114.9 1.1 fusion.29
  116.0 0.6 fusion.31
  116.6 0.2 fusion.17
  116.8 1.3 fusion.23
  118.1 0.7 max.32
  118.9 0.0 collective-permute-done.1
  118.9 1.5 maximum_convert_fusion
  120.4 0.0 slice-start
  120.4 0.0 copy-start.7
  120.4 0.0 copy-start.10
  120.5 2.1 %fusion.15 = bf16[1024,512]{1,0:T(8,128)(2,1)S(1)} fusion(f32[1026,512]{1,0:T(8,128)S(1)} %maximum_convert_fusion, bf16[1024,1024]{1,0:T(8,128)(2,1)} %copy-done.5, f32[512]{0:T(512)} %bitcast.81, f32[512]{0:T(512)S(1)} %bitcast.80, f32[512]{0:T(512)S(1)} %bitcast.79), kind=kLoop, calls=%fused_computation.24 | loop fusion | flops 4194304 | bytes 8394752 | tf_op jit(solution)/shard_map/convert_element_type | solution.py:340
  122.6 0.0 collective-permute-done
  122.6 0.1 pad_maximum_fusion.2
  122.8 3.2 %fusion.10 = (f32[4,2,512]{2,1,0:T(2,128)S(1)}, f32[4,640,512,2]{2,1,3,0:T(8,128)S(1)}) fusion(f32[512,640]{0,1:T(8,128)S(1)} %fusion.17, f32[4,2]{1,0:T(4,128)S(1)} %multiply_exponential_fusion, pred[512,640]{0,1:T(8,128)(4,1)S(1)} %copy-done.10, bf16[640,4,64,1]{0,2,3,1:T(8,128)(2,1)S(1)} %bitcast.78, bf16[512,4,2,64]{0,3,2,1:T(8,128)(2,1)S(1)} %bitcast.74), kind=kOutput, calls=%fused_computation.18 | convolution fusion | flops 348647424 | bytes 12992544 | tf_op jit(solution)/shard_map/qkgd,skd->kgqs/dot_general | solution.py:278
  125.9 0.1 broadcast_maximum_fusion.1
  126.0 8.6 %fusion.4 = (f32[4,2,512]{2,1,0:T(2,128)S(1)}, f32[4,2,512]{2,1,0:T(2,128)S(1)}, f32[4,640,512,2]{2,1,3,0:T(8,128)}) fusion(f32[4,640,512,2]{2,1,3,0:T(8,128)S(1)} %get-tuple-element.31, f32[4,2,512]{2,1,0:T(2,128)S(1)} %broadcast_maximum_fusion.1, f32[512,640]{0,1:T(8,128)S(1)} %fusion.17, f32[4,2]{1,0:T(4,128)S(1)} %multiply_exponential_fusion, ...), kind=kOutput, calls=%fused_computation.12 | convolution fusion | flops 361750528 | bytes 23838752 | tf_op jit(solution)/shard_map/qkgd,skd->kgqs/dot_general | solution.py:278
  134.7 0.1 exponential_add_fusion.1
  134.8 4.5 %fusion.22 = bf16[4,64,2,512]{3,1,2,0:T(8,128)(2,1)} fusion(bf16[640,4,64,1]{0,2,3,1:T(8,128)(2,1)S(1)} %bitcast.77, f32[4,640,512,2]{2,1,3,0:T(8,128)S(1)} %get-tuple-element.31, f32[4,2,512]{2,1,0:T(2,128)S(1)} %get-tuple-element.26, f32[4,2,512]{2,1,0:T(2,128)S(1)} %broadcast_maximum_fusion.1, f32[512,640]{0,1:T(8,128)S(1)} %fusion.17, ...), kind=kOutput, calls=%fused_computation.39 | convolution fusion | flops 354156544 | bytes 13008928 | tf_op jit(solution)/shard_map/kgqs,skd->qkgd/dot_general | solution.py:289
  139.3 1.3 copy.23
  140.6 7.0 %fusion.5 = f32[4,2,512]{2,1,0:T(2,128)S(1)} fusion(f32[4,640,512,2]{2,1,3,0:T(8,128)} %get-tuple-element.32, f32[4,2,512]{2,1,0:T(2,128)S(1)} %get-tuple-element.27, f32[512,640]{0,1:T(8,128)S(1)} %fusion.17, f32[4,2]{1,0:T(4,128)S(1)} %multiply_exponential_fusion, pred[512,640]{0,1:T(8,128)(4,1)S(1)} %copy-done.3), kind=kLoop, calls=%fused_computation.13 | loop fusion | flops 15724544 | bytes 12156960 | tf_op jit(solution)/shard_map/reduce_sum | solution.py:287
  147.6 0.1 exponential_add_fusion
  147.7 4.5 %fusion.21 = bf16[4,64,2,512]{3,1,2,0:T(8,128)(2,1)} fusion(bf16[640,4,64,1]{0,2,3,1:T(8,128)(2,1)S(1)} %bitcast.75, f32[4,640,512,2]{2,1,3,0:T(8,128)S(1)} %copy-done.1, f32[4,2,512]{2,1,0:T(2,128)S(1)} %exponential_add_fusion, f32[4,2,512]{2,1,0:T(2,128)S(1)} %get-tuple-element.27, f32[512,640]{0,1:T(8,128)S(1)} %fusion.17, ...), kind=kOutput, calls=%fused_computation.38 | convolution fusion | flops 354156544 | bytes 13008928 | tf_op jit(solution)/shard_map/kgqs,skd->qkgd/dot_general | solution.py:289
  152.2 1.3 copy.24
  153.4 1.6 pad_maximum_fusion.mix
  155.1 53.2 %shard_map.119 = bf16[512,2048]{1,0:T(8,128)(2,1)} custom-call(bf16[1024,1024]{1,0:T(8,128)(2,1)} %pad_maximum_fusion.mix, bf16[2048,1024]{1,0:T(8,128)(2,1)} %get-tuple-element.14.w_out), custom_call_target="tpu_custom_call" | custom-call | tf_op jit(solution)/shard_map/pallas_call | solution.py:224
  208.3 3.2 %copy.32 = bf16[1,512,2048]{2,1,0:T(8,128)(2,1)} copy(bf16[1,512,2048]{2,1,0:T(8,128)(2,1)} %bitcast.69) | data formatting | bytes 4194304
  (30 shorter events, 0.1 us)
Async XLA Ops:
  86.8 3.5 %copy-start = (bf16[1024,2048]{1,0:T(8,128)(2,1)S(1)}, bf16[1024,2048]{1,0:T(8,128)(2,1)}, u32[]{:S(2)}) copy-start(bf16[1024,2048]{1,0:T(8,128)(2,1)} %get-tuple-element.10) | copy-start | bytes 12582916
  86.8 4.7 %copy-start.12 = (f32[2048]{0:T(1024)S(1)}, f32[2048]{0:T(1024)}, u32[]{:S(2)}) copy-start(f32[2048]{0:T(1024)} %param.13) | copy-start | bytes 24580
  91.5 2.2 %copy-start.14 = (bf16[2048,1024]{1,0:T(8,128)(2,1)S(1)}, bf16[2048,1024]{1,0:T(8,128)(2,1)}, u32[]{:S(2)}) copy-start(bf16[2048,1024]{1,0:T(8,128)(2,1)} %get-tuple-element.12) | copy-start | bytes 12582916
  93.6 4.7 %copy-start.15 = (bf16[2048,512]{1,0:T(8,128)(2,1)S(1)}, bf16[2048,512]{1,0:T(8,128)(2,1)}, u32[]{:S(2)}) copy-start(bf16[2048,512]{1,0:T(8,128)(2,1)} %get-tuple-element.13) | copy-start | bytes 6291460
  98.3 2.4 %copy-start.5 = (bf16[1024,1024]{1,0:T(8,128)(2,1)}, bf16[1024,1024]{1,0:T(8,128)(2,1)S(1)}, u32[]{:S(2)}) copy-start(bf16[1024,1024]{1,0:T(8,128)(2,1)S(1)} %convolution_convert_fusion) | copy-start | bytes 6291460
  98.4 6.8 %copy-start.13 = (bf16[2048,1024]{1,0:T(8,128)(2,1)S(1)}, bf16[2048,1024]{1,0:T(8,128)(2,1)}, u32[]{:S(2)}) copy-start(bf16[2048,1024]{1,0:T(8,128)(2,1)} %get-tuple-element.11) | copy-start | bytes 12582916
  100.7 4.5 %copy-start.4 = (bf16[1024,512]{1,0:T(8,128)(2,1)}, bf16[1024,512]{1,0:T(8,128)(2,1)S(1)}, u32[]{:S(2)}) copy-start(bf16[1024,512]{1,0:T(8,128)(2,1)S(1)} %multiply_convert_fusion) | copy-start | bytes 3145732
  101.3 17.5 %collective-permute-start.1 = (bf16[2,512]{1,0:T(2,128)(2,1)}, bf16[2,512]{1,0:T(2,128)(2,1)}, u32[]{:S(2)}, u32[]{:S(2)}) collective-permute-start(bf16[2,512]{1,0:T(2,128)(2,1)} %slice.88), channel_id=1, source_target_pairs={{0,8},{8,16},{16,24},{1,9},{9,17},{17,25},{2,10},{10,18},{18,26},{... | collective-permute-start | bytes 6152 | tf_op jit(solution)/shard_map/ppermute | solution.py:242
  105.2 10.8 %copy-start.11 = (bf16[3,512]{1,0:T(4,128)(2,1)S(1)}, bf16[3,512]{1,0:T(4,128)(2,1)}, u32[]{:S(2)}) copy-start(bf16[3,512]{1,0:T(4,128)(2,1)} %param.20) | copy-start | bytes 9220
  110.0 10.4 %copy-start.2 = (bf16[1024,1024]{0,1:T(8,128)(2,1)}, bf16[1024,1024]{0,1:T(8,128)(2,1)S(1)}, u32[]{:S(2)}) copy-start(bf16[1024,1024]{0,1:T(8,128)(2,1)S(1)} %convolution_convert_fusion.1) | copy-start | bytes 6291460
  110.8 11.8 %collective-permute-start = (bf16[128,512]{0,1:T(8,128)(2,1)}, bf16[128,512]{0,1:T(8,128)(2,1)S(1)}, u32[]{:S(2)}, u32[]{:S(2)}) collective-permute-start(bf16[128,512]{0,1:T(8,128)(2,1)} %slice.79), channel_id=1, source_target_pairs={{0,8},{8,16},{16,24},{1,9},{9,17},{17,25},{2,10},{10,18},{18,26},{... | collective-permute-start | bytes 393224 | tf_op jit(solution)/shard_map/ppermute | solution.py:242
  120.4 2.2 %slice-start = ((bf16[1024,1024]{0,1:T(8,128)(2,1)}), bf16[1024,512]{0,1:T(8,128)(2,1)S(1)}, s32[]{:S(2)}) async-start(bf16[1024,1024]{0,1:T(8,128)(2,1)} %copy-done.2), calls=%async_computation | async-start | bytes 2097152 | tf_op jit(solution)/shard_map/slice | solution.py:322
  120.4 2.3 %copy-start.7 = (bf16[512,512]{0,1:T(8,128)(2,1)S(1)}, bf16[512,512]{0,1:T(8,128)(2,1)}, u32[]{:S(2)}) copy-start(bf16[512,512]{0,1:T(8,128)(2,1)} %get-tuple-element.17) | copy-start | bytes 1572868
  120.4 2.3 %copy-start.10 = (pred[512,640]{0,1:T(8,128)(4,1)S(1)}, pred[512,640]{0,1:T(8,128)(4,1)}, u32[]{:S(2)}) copy-start(pred[512,640]{0,1:T(8,128)(4,1)} %get-tuple-element.29) | copy-start | bytes 983044
  122.7 3.3 %copy-start.3 = (pred[512,640]{0,1:T(8,128)(4,1)S(1)}, pred[512,640]{0,1:T(8,128)(4,1)}, u32[]{:S(2)}) copy-start(pred[512,640]{0,1:T(8,128)(4,1)} %get-tuple-element.28) | copy-start | bytes 983044
  122.7 3.3 %copy-start.6 = (bf16[512,512]{0,1:T(8,128)(2,1)S(1)}, bf16[512,512]{0,1:T(8,128)(2,1)}, u32[]{:S(2)}) copy-start(bf16[512,512]{0,1:T(8,128)(2,1)} %get-tuple-element.18) | copy-start | bytes 1572868
  122.7 3.3 %copy-start.9 = (bf16[640,256]{0,1:T(8,128)(2,1)S(1)}, bf16[640,256]{0,1:T(8,128)(2,1)}, u32[]{:S(2)}) copy-start(bf16[640,256]{0,1:T(8,128)(2,1)} %get-tuple-element.19) | copy-start | bytes 983044
  140.6 7.1 %copy-start.1 = (f32[4,640,512,2]{2,1,3,0:T(8,128)S(1)}, f32[4,640,512,2]{2,1,3,0:T(8,128)}, u32[]{:S(2)}) copy-start(f32[4,640,512,2]{2,1,3,0:T(8,128)} %get-tuple-element.32) | copy-start | bytes 31457284
  140.6 7.1 %copy-start.8 = (bf16[640,256]{0,1:T(8,128)(2,1)S(1)}, bf16[640,256]{0,1:T(8,128)(2,1)}, u32[]{:S(2)}) copy-start(bf16[640,256]{0,1:T(8,128)(2,1)} %get-tuple-element.20) | copy-start | bytes 983044
where the time goes:
time: 212 us; the launch traced here: 211 us
  Pallas kernels  135 us (64%)
  matrix products  32.7 us (15%)
  other arithmetic  22.7 us (11%)
  local copies, waits for them, and re-layouts  13.5 us (6%)
  starting transfers between devices  7.02 us (3%)
    pallas_call x1, Pallas kernels, gather_all(): pl.pallas_call(functools.partial(gather_kernel, gather, n_tp), out_shape=...  82 us
    pallas_call x1, Pallas kernels, project_out(): pl.pallas_call(functools.partial(out_kernel, n_tp, chunks), out_shape=jax...  53.2 us
    dot_general x2, matrix products, attend(): jnp.einsum('qkgd,skd->kgqs', query_block, band_keys, preferred_element_ty...  11.8 us
    dot_general x2, matrix products, attend(): jnp.einsum('kgqs,skd->qkgd', weights, band_values, preferred_element_type...  9.02 us
    ppermute x2, starting transfers between devices, shifted(): return lax.ppermute(block, axis, route)  7.02 us
    reduce_sum x1, other arithmetic, attend(): jnp.sum(raised, axis=-1, keepdims=True) + jnp.exp(sinks - highest)  7.01 us
    unnamed x35, local copies, waits for them, and re-layouts  6.23 us
    dot_general x1, matrix products, on_device(): jnp.dot(normed, w_qkv, preferred_element_type=jnp.float32)  4.82 us
  transfers between devices with their start and end apart: 2, of which 0 were waited for; matrix products, arithmetic and copies ran while one was open for 7% of the time, Pallas kernels for 0%

commit v1 on v0

v1 whole, which is shorter than its diff:
```python
import functools

import jax
import jax.numpy as jnp
from jax import lax
from jax.experimental import pallas as pl
from jax.experimental.pallas import tpu as pltpu
from jax.sharding import PartitionSpec as P

HEADS = 16
HEAD = 64
WINDOW = 128
HALO = 16
MESH = pl.DeviceIdType.MESH
BF16, F32 = jnp.bfloat16, jnp.float32


def when(condition, body):
    if condition is True:
        body()
    else:
        pl.when(condition)(body)


class Part:
    def __init__(self, number, wide, place, base):
        self.number, self.wide, self.place, self.base = number, wide, place, base


def part_kinds(out_rows):
    kinds = [(False, None), (True, None), (False, None), (False, None), (False, None)]
    quarter, eighth = out_rows // 4, out_rows // 8
    kinds += [(False, (n * quarter, quarter)) for n in range(3)]
    kinds += [(True, (3 * quarter, eighth)), (False, (3 * quarter + eighth, eighth))]
    return kinds


def layer_kernel(sizes, *refs):
    n_sp, n_out, n_tp, n_proj, separate = sizes
    tok, gain, taps, sinks = refs[:4]
    n_in = 6 if separate else 5
    w_own = refs[4 : 4 + n_in]
    out_own = refs[4 + n_in : 6 + n_in]
    out = refs[6 + n_in]
    (tokf, w_all, wo_all, q_buf, kv_buf, inner, gate_b, product, m_att, m_conv, r_att, r_conv, bias,
     send_sem, recv_sem, own_sem, wo_send, wo_recv, tok_send, tok_recv, halo_send, halo_recv,
     mix_send, mix_recv) = refs[7 + n_in :]
    n_fs = 2 * n_out
    shards = n_sp * n_fs
    s, f, t = lax.axis_index("sp"), lax.axis_index("fs"), lax.axis_index("tp")
    o, i = f // 2, f % 2
    rows_total, width = tokf.shape
    cols = tok.shape[1]
    q_cols = q_buf.shape[1]
    kv_cols = kv_buf.shape[1] // 2
    k_rows = w_own[0].shape[0]
    out_rows, out_cols = out_own[0].shape
    owned = rows_total // n_tp
    chunks = 4
    step = rows_total // chunks
    order = [chunks - 1] + list(range(chunks - 1))
    me = s * n_fs + f

    right, left, core = (s + 1, f, t), (s - 1, f, t), (s, o * 2 + (1 - i), t)
    across = [(s, lax.rem(o + k, n_out) * 2 + i, t) for k in range(1, n_out)]
    peers = [(s, f, lax.rem(t + k, n_tp)) for k in range(1, n_tp)]
    has_right, has_left = s < n_sp - 1, s > 0

    local = []
    spots = [(0, 0), (1, 0), (1, kv_cols), (2, 0), (3, 0), (4, 0)] if separate else [(n, 0) for n in range(5)]
    for n, (number, col) in enumerate(spots):
        place = w_all.at[number, pl.ds(me * k_rows, k_rows), pl.ds(col, w_own[n].shape[1])]
        local.append(pltpu.make_async_copy(w_own[n], place, own_sem.at[n]))
    for a in range(2):
        local.append(pltpu.make_async_copy(out_own[a], wo_all.at[2 * t + a, me], own_sem.at[6 + a]))
    my_cols = pl.ds(pl.multiple_of(t * cols, cols), cols)
    local.append(pltpu.make_async_copy(tok, tokf.at[:, my_cols], own_sem.at[8]))
    for copy in local:
        copy.start()

    barrier = pltpu.get_barrier_semaphore()
    greet = lambda where: pl.semaphore_signal(barrier, inc=1, device_id=where, device_id_type=MESH)
    when(has_right, lambda: greet(right))
    when(has_left, lambda: greet(left))
    for where in across + [core] + peers:
        greet(where)
    count = len(across) + 1 + len(peers)
    pl.semaphore_wait(barrier, count + has_right.astype(jnp.int32) + has_left.astype(jnp.int32))

    wo_copies, tok_copies = [], {}
    for k, peer in enumerate(peers):
        for a in range(2):
            copy = pltpu.make_async_remote_copy(
                src_ref=out_own[a], dst_ref=wo_all.at[2 * t + a, me],
                send_sem=wo_send.at[k, a], recv_sem=wo_recv.at[k, a], device_id=peer, device_id_type=MESH,
            )
            copy.start()
            wo_copies.append(copy)
    for n in order:
        here = pl.ds(n * step, step)
        for k, peer in enumerate(peers):
            copy = pltpu.make_async_remote_copy(
                src_ref=tok.at[here], dst_ref=tokf.at[here, my_cols],
                send_sem=tok_send.at[k, n], recv_sem=tok_recv.at[k, n], device_id=peer, device_id_type=MESH,
            )
            copy.start()
            tok_copies[k, n] = copy

    parts, base = [], 0
    for number, (wide, rows) in enumerate(part_kinds(out_rows)):
        if rows is None:
            place = lambda src, number=number: w_all.at[number, pl.ds(src * k_rows, k_rows)]
        else:
            place = lambda src, rows=rows: wo_all.at[:, src, pl.ds(*rows)]
        parts.append(Part(number, wide, place, base))
        base += (5 if wide else 4) * n_sp * 2 if n_out > 1 else 2 * n_sp * 2

    def copy_of(part, src, where, lane, distance, side):
        spot = part.place(src)
        return pltpu.make_async_remote_copy(
            src_ref=spot, dst_ref=spot,
            send_sem=send_sem.at[part.base + lane * n_sp * 2 + distance * 2 + side],
            recv_sem=recv_sem.at[part.number * shards + src],
            device_id=where, device_id_type=MESH,
        )

    def deal(part, distance, k, drain):
        ys = [(2 + n, where) for n, where in enumerate(across)]
        lanes = 0 if k == 0 else 2 + (len(across) if part.wide else len(across) - 1) + 2 * (k - 1) + (0 if part.wide else 1)
        lane_z, lane_core = (0, 1) if k == 0 else (lanes, lanes + (1 if part.wide else 0))
        source_o = lax.rem(o + n_out - k, n_out)
        first = isinstance(distance, int) and distance == 0
        for side in (0,) if first else (0, 1):
            source_s = s if first else (s - distance if side == 0 else s + distance)
            there = True if first else (source_s >= 0 if side == 0 else source_s < n_sp)
            src = source_s * n_fs + source_o * 2 + i

            def body(side=side, src=src):
                def go(where, lane, at):
                    copy = copy_of(part, src, where, lane, distance, at)
                    copy.wait_send() if drain else copy.start()

                if not (first and k == 0) and not drain:
                    copy_of(part, src, core, 0, 0, 0).wait_recv()
                if k == 0 or part.wide:
                    if first or side == 0:
                        when(has_right, lambda: go(right, lane_z, 0))
                    if first or side == 1:
                        when(has_left, lambda: go(left, lane_z, 1))
                if k == 0 and (first or not part.wide):
                    for lane, where in ys:
                        go(where, lane, side)
                go(core, lane_core, side)

            when(there, body)

    def stage(number, n):
        part = parts[number]
        last = n_sp - 1
        if not (isinstance(n, int) and n > last):
            deal(part, n, 0, False)
        if isinstance(n, int) and n == 0:
            return
        for k in range(1, n_out):
            deal(part, n - 1, k, False)

    def partner(number, source_s):
        part = parts[number]
        for source_o in range(n_out):
            copy_of(part, source_s * n_fs + source_o * 2 + (1 - i), core, 0, 0, 0).wait_recv()

    def finish(number):
        for source_s in range(n_sp):
            partner(number, source_s)

    def tokens_in(n):
        for k in range(n_tp - 1):
            tok_copies[k, n].wait_recv()

    def norm(n):
        size = 32

        def body(r, carry):
            here = pl.ds(pl.multiple_of(n * step + r * size, size), size)
            values = tokf[here, :].astype(F32)
            centred = values - jnp.sum(values, axis=1, keepdims=True) * (1.0 / width)
            variance = jnp.sum(centred * centred, axis=1, keepdims=True) * (1.0 / width)
            tokf[here, :] = (centred * lax.rsqrt(variance + 1e-05) * gain[...]).astype(BF16)
            return carry

        lax.fori_loop(0, step // size, body, 0)

    def project(number, ns):
        def body(m, carry):
            n = m if len(ns) == chunks else ns[0] + m
            first = n * step if isinstance(n, int) else pl.multiple_of(n * step, step)
            here = pl.ds(first, step)
            result = jnp.dot(tokf[here, :], w_all[number], preferred_element_type=F32).astype(BF16)
            if number == 0:
                q_buf[here, :] = result
            elif number == 1:
                kv_buf[pl.ds(first + WINDOW, step), :] = result
            elif number == 2:
                inner[here, :] = result
            elif number == 3:
                gate_b[here, :] = result
            else:
                made = result.astype(F32) * inner[here, :].astype(F32)
                product[pl.ds(first + HALO, step), :] = made.astype(BF16)
            return carry

        if len(ns) == 1:
            body(0, 0)
        else:
            lax.fori_loop(0, len(ns), body, 0)

    def halo_copy(which):
        buffer, size = ((kv_buf, WINDOW), (product, HALO))[which]
        return pltpu.make_async_remote_copy(
            src_ref=buffer.at[pl.ds(rows_total, size)], dst_ref=buffer.at[pl.ds(0, size)],
            send_sem=halo_send.at[which], recv_sem=halo_recv.at[which], device_id=right, device_id_type=MESH,
        )

    def halo_out(which):
        when(has_right, lambda: halo_copy(which).start())

        def clear():
            buffer, size = ((kv_buf, WINDOW), (product, HALO))[which]
            buffer[0:size, :] = jnp.zeros((size, buffer.shape[1]), BF16)

        when(s == 0, clear)

    def halo_in(which):
        when(has_left, lambda: halo_copy(which).wait_recv())

    heads_here = q_cols // HEAD
    kv_here = kv_cols // HEAD
    group = heads_here // kv_here
    tall = group * WINDOW

    def make_bias():
        row = lax.broadcasted_iota(jnp.int32, (tall, 2 * WINDOW), 0)
        col = lax.broadcasted_iota(jnp.int32, (tall, 2 * WINDOW), 1)
        distance = WINDOW + row % WINDOW - col
        keep = (distance >= 0) & (distance < WINDOW)
        for h in range(kv_here):
            head = (t * heads_here + h * group + row // WINDOW + 1).astype(F32)
            slope = jnp.exp2(head * (-8.0 / HEADS))
            bias[h] = jnp.where(keep, -(slope * distance.astype(F32)), -jnp.inf)

    def attend(n):
        row = lax.broadcasted_iota(jnp.int32, (tall, 1), 0) // WINDOW
        col = lax.broadcasted_iota(jnp.int32, (1, 2 * WINDOW), 1)

        def body(b, carry):
            block = n * (step // WINDOW) + b
            first = pl.multiple_of(block * WINDOW, WINDOW)
            before = jnp.where(col >= WINDOW, 0.0, jnp.where((s == 0) & (block == 0), -jnp.inf, 0.0))
            queries = q_buf[pl.ds(first, WINDOW), :]
            band = kv_buf[pl.ds(first, 2 * WINDOW), :]
            outs = []
            for h in range(kv_here):
                query = jnp.concatenate(
                    [queries[:, (h * group + g) * HEAD : (h * group + g + 1) * HEAD] for g in range(group)], axis=0
                )
                key = band[:, h * HEAD : (h + 1) * HEAD]
                value = band[:, kv_cols + h * HEAD : kv_cols + (h + 1) * HEAD]
                scores = lax.dot_general(query, key, (((1,), (1,)), ((), ())), preferred_element_type=F32)
                scores = scores * HEAD ** (-0.5) + bias[h] + before
                sink = jnp.full((tall, 1), sinks[h * group], F32)
                for g in range(1, group):
                    sink = jnp.where(row == g, sinks[h * group + g], sink)
                top = jnp.maximum(jnp.max(scores, axis=1, keepdims=True), sink)
                raised = jnp.exp(scores - top)
                total = jnp.sum(raised, axis=1, keepdims=True) + jnp.exp(sink - top)
                weights = (raised * (1.0 / total)).astype(BF16)
                mixed = jnp.dot(weights, value, preferred_element_type=F32).astype(BF16)
                outs += [mixed[g * WINDOW : (g + 1) * WINDOW] for g in range(group)]
            m_att[pl.ds(first, WINDOW), :] = jnp.concatenate(outs, axis=1)
            return carry

        lax.fori_loop(0, step // WINDOW, body, 0)

    def convolve():
        size = 64

        def body(r, carry):
            first = pl.multiple_of(r * size, size)
            padded = product[pl.ds(first, size + HALO), :].astype(F32)
            tap = taps[...].astype(F32)
            filtered = (
                tap[0:1] * padded[HALO - 2 : HALO - 2 + size]
                + tap[1:2] * padded[HALO - 1 : HALO - 1 + size]
                + tap[2:3] * padded[HALO : HALO + size]
            )
            m_conv[pl.ds(first, size), :] = (gate_b[pl.ds(first, size), :].astype(F32) * filtered).astype(BF16)
            return carry

        lax.fori_loop(0, rows_total // size, body, 0)

    def mix_copy(which, k):
        source, target = ((m_att, r_att), (m_conv, r_conv))[which]
        return pltpu.make_async_remote_copy(
            src_ref=source.at[pl.ds(pl.multiple_of(peers[k][2] * owned, owned), owned)], dst_ref=target.at[k],
            send_sem=mix_send.at[which, k], recv_sem=mix_recv.at[which, k],
            device_id=peers[k], device_id_type=MESH,
        )

    def mix_out(which):
        for k in range(n_tp - 1):
            mix_copy(which, k).start()

    def mix_in():
        for which in range(2):
            for k in range(n_tp - 1):
                mix_copy(which, k).wait_recv()

    def project_out(source_s):
        for number in range(n_proj, len(parts)):
            partner(number, source_s)
        block = n_fs * out_cols
        tile = min(256, owned)

        def weights(row):
            blocks = [wo_all[row, source_s * n_fs + n] for n in range(n_fs)]
            return jnp.concatenate(blocks, axis=1)

        def body(r, carry):
            total = jnp.zeros((tile, block), F32)
            for k in range(n_tp):
                g = lax.rem(t + n_tp - k, n_tp)
                if k == 0:
                    here = pl.ds(pl.multiple_of(t * owned + r * tile, tile), tile)
                    att, conv = m_att[here, :], m_conv[here, :]
                else:
                    here = pl.ds(pl.multiple_of(r * tile, tile), tile)
                    att, conv = r_att[k - 1, here, :], r_conv[k - 1, here, :]
                partial = jnp.dot(att, weights(2 * g), preferred_element_type=F32)
                partial = partial + jnp.dot(conv, weights(2 * g + 1), preferred_element_type=F32)
                total = total + partial.astype(BF16).astype(F32)
            where = pl.ds(pl.multiple_of(source_s * block, block), block)
            out[pl.ds(pl.multiple_of(r * tile, tile), tile), where] = total.astype(BF16)
            return carry

        lax.fori_loop(0, owned // tile, body, 0)

    def first_chunk():
        tokens_in(order[0])
        norm(order[0])
        project(0, [order[0]])
        project(1, [order[0]])
        halo_out(0)

    def chunk(n):
        tokens_in(n)
        norm(n)
        project(0, [n])
        project(1, [n])

    def wo_ready():
        for copy in wo_copies:
            copy.wait_recv()

    for copy in local[:6] if separate else local[:5]:
        copy.wait()
    if n_sp <= 4:
        work = {
            (0, 1): [make_bias],
            (0, 2): [local[-3].wait, local[-2].wait, local[-1].wait, wo_ready],
            (2, 1): [first_chunk],
            (3, 1): [lambda: chunk(0)],
            (3, 2): [lambda: halo_in(0), lambda: attend(0)],
            (3, 3): [lambda: project(2, [3]), lambda: project(2, [0])],
            (4, 1): [lambda: chunk(1)],
            (4, 2): [lambda: attend(1)],
            (4, 3): [lambda: project(2, [1]), lambda: project(3, [0, 1]), lambda: project(3, [3])],
            (5, 1): [lambda: chunk(2)],
            (5, 2): [lambda: attend(2)],
            (5, 3): [lambda: attend(3), lambda: mix_out(0)],
            (6, 1): [lambda: project(2, [2]), lambda: project(3, [2]), lambda: project(4, [0, 1, 2, 3]), lambda: halo_out(1)],
            (6, 2): [lambda: halo_in(1), convolve, lambda: mix_out(1)],
        }
        total = len(parts)
        stage(0, 0)
        for number in range(total):
            for n in range(1, n_sp + 1):
                stage(number, n)
                if n == 1 and number + 1 < total:
                    stage(number + 1, 0)
                for job in work.get((number, n), []):
                    job()
                if number == total - 1:
                    if n == 1:
                        mix_in()
                        project_out(s)
                    if n > 1:
                        d = n - 1
                        when(s - d >= 0, lambda: project_out(s - d))
                        when(s + d < n_sp, lambda: project_out(s + d))
            if number < n_proj:
                finish(number)
    else:
        for copy in local[-3:]:
            copy.wait()
        wo_ready()

        def spread(number):
            stage(number, 0)
            stage(number, 1)
            lax.fori_loop(2, n_sp, lambda n, c: (stage(number, n), c)[1], 0)
            stage(number, n_sp)

        for number in range(n_proj):
            spread(number)
            finish(number)
        make_bias()
        first_chunk()
        for n in order[1:]:
            chunk(n)
        halo_in(0)
        for n in range(chunks):
            attend(n)
        mix_out(0)
        for number in (2, 3, 4):
            project(number, list(range(chunks)))
        halo_out(1)
        halo_in(1)
        convolve()
        mix_out(1)
        for number in range(n_proj, len(parts)):
            spread(number)
        mix_in()
        lax.fori_loop(0, n_sp, lambda n, c: (project_out(n), c)[1], 0)

    for part in parts:
        for k in range(n_out):
            deal(part, 0, k, True)
            if n_sp <= 4:
                for distance in range(1, n_sp):
                    deal(part, distance, k, True)
            else:
                lax.fori_loop(1, n_sp, lambda n, c, part=part, k=k: (deal(part, n, k, True), c)[1], 0)
    for which in range(2):
        when(has_right, lambda which=which: halo_copy(which).wait_send())
        for k in range(n_tp - 1):
            mix_copy(which, k).wait_send()
    for copy in wo_copies + list(tok_copies.values()):
        copy.wait_send()


def on_device(tokens, norm_gain, w_query, w_key, w_value, w_conv_in, w_conv_b, w_conv_c,
              conv_taps, sink_logits, w_attn_out, w_conv_out):
    n_sp, n_fs, n_tp = (lax.axis_size(axis) for axis in ("sp", "fs", "tp"))
    n_out = n_fs // 2
    shards = n_sp * n_fs
    rows, cols = tokens.shape[1:]
    width = cols * n_tp
    q_cols, kv_cols, channels = w_query.shape[1], w_key.shape[1], w_conv_in.shape[1]
    out_rows, out_cols = w_attn_out.shape
    separate = kv_cols % 128 == 0
    weights = [w_query]
    weights += [w_key, w_value] if separate else [jnp.concatenate([w_key, w_value], axis=1)]
    weights += [w_conv_in, w_conv_b, w_conv_c]
    owned = rows // n_tp
    kinds = part_kinds(out_rows)
    lanes = sum((5 if wide else 4) if n_out > 1 else 2 for wide, _ in kinds)
    kv_here = kv_cols // HEAD
    group = q_cols // kv_cols
    dma = pltpu.SemaphoreType.DMA
    vmem, anywhere = pl.BlockSpec(memory_space=pltpu.VMEM), pl.BlockSpec(memory_space=pl.ANY)
    summed = pl.pallas_call(
        functools.partial(layer_kernel, (n_sp, n_out, n_tp, 5, separate)),
        out_shape=jax.ShapeDtypeStruct((owned, width), BF16),
        in_specs=[anywhere, vmem, vmem, pl.BlockSpec(memory_space=pltpu.SMEM)] + [anywhere] * (len(weights) + 2),
        out_specs=vmem,
        scratch_shapes=[
            pltpu.VMEM((rows, width), BF16),
            pltpu.VMEM((5, width, q_cols), BF16),
            pltpu.VMEM((2 * n_tp, shards, out_rows, out_cols), BF16),
            pltpu.VMEM((rows, q_cols), BF16),
            pltpu.VMEM((WINDOW + rows, 2 * kv_cols), BF16),
            pltpu.VMEM((rows, channels), BF16),
            pltpu.VMEM((rows, channels), BF16),
            pltpu.VMEM((HALO + rows, channels), BF16),
            pltpu.VMEM((rows, q_cols), BF16),
            pltpu.VMEM((rows, channels), BF16),
            pltpu.VMEM((n_tp - 1, owned, q_cols), BF16),
            pltpu.VMEM((n_tp - 1, owned, channels), BF16),
            pltpu.VMEM((kv_here, group * WINDOW, 2 * WINDOW), F32),
            dma((lanes * n_sp * 2,)),
            dma((len(kinds) * shards,)),
            dma((9,)),
            dma((n_tp - 1, 2)),
            dma((n_tp - 1, 2)),
            dma((n_tp - 1, 4)),
            dma((n_tp - 1, 4)),
            dma((2,)),
            dma((2,)),
            dma((2, n_tp - 1)),
            dma((2, n_tp - 1)),
        ],
        compiler_params=pltpu.CompilerParams(
            collective_id=0, has_side_effects=True, vmem_limit_bytes=60 * 1024 * 1024
        ),
    )(tokens[0], norm_gain[None], conv_taps, sink_logits, *weights, w_attn_out, w_conv_out)
    return summed[None]


def solution(mesh):
    placed = (
        P("fs", "sp", "tp"),
        P(),
        P(("sp", "fs"), "tp"),
        P(("sp", "fs"), "tp"),
        P(("sp", "fs"), "tp"),
        P(("sp", "fs"), "tp"),
        P(("sp", "fs"), "tp"),
        P(("sp", "fs"), "tp"),
        P(None, "tp"),
        P("tp"),
        P("tp", ("sp", "fs")),
        P("tp", ("sp", "fs")),
    )
    return jax.shard_map(
        on_device,
        mesh=mesh,
        in_specs=placed,
        out_specs=P("fs", ("sp", "tp"), None),
        check_vma=False,
    )
```

time: 212 us -> 151 us (0.71)
  matrix products: 32.7 us -> 0 us
  other arithmetic: 22.7 us -> 0 us
  Pallas kernels: 135 us -> 147 us
  local copies, waits for them, and re-layouts: 13.5 us -> 3.16 us
  starting transfers between devices: 7.02 us -> 0 us
    dot_general x7 -> x0, matrix products: 32.7 us -> none  [the longest x2 11.8 us: attend(): jnp.einsum('qkgd,skd->kgqs', query_block, band_keys, preferred_element_ty...]
    pallas_call x2 -> x1, Pallas kernels: 135 us -> 147 us  [on_device(): pl.pallas_call(functools.partial(layer_kernel, (n_sp, n_out, n_tp, 5, sep...]
    reduce_sum x3 -> x0, other arithmetic: 11.2 us -> none  [the longest x1 7.01 us: attend(): jnp.sum(raised, axis=-1, keepdims=True) + jnp.exp(sinks - highest)]
    ppermute x2 -> x0, starting transfers between devices: 7.02 us -> none  [shifted(): return lax.ppermute(block, axis, route)]
    convert_element_type x4 -> x0, other arithmetic: 5.49 us -> none  [the longest x1 2.15 us: on_device(): conv_out = (gate_b.astype(jnp.float32) * filtered).astype(jnp.bfloat16)]
    slice x7 -> x0, local copies, waits for them, and re-layouts: 3.98 us -> none  [the longest x1 1.07 us: attend(): queries[first_row:first_row + block_rows]]
    concatenate x2 -> x0, other arithmetic: 3.59 us -> none  [the longest x1 1.95 us: on_device(): jnp.concatenate([w_query, w_key, w_value], axis=1)]
    unnamed x35 -> x1, local copies, waits for them, and re-layouts: 6.23 us -> 3.16 us
  transfers between devices with their start and end apart: 2 -> 0, of which waited for: 0 -> 0; matrix products, arithmetic and copies ran while one was open for 7% -> 0% of each run, Pallas kernels for 0% -> 0%
where the time goes in v1:
time: 151 us
  Pallas kernels  147 us (97%)
  local copies, waits for them, and re-layouts  3.16 us (2%)
    pallas_call x1, Pallas kernels, on_device(): pl.pallas_call(functools.partial(layer_kernel, (n_sp, n_out, n_tp, 5, sep...  147 us
    unnamed x1, local copies, waits for them, and re-layouts  3.16 us

profile of v1, /device:TPU:0, one launch (start us, length us, event | category | flops | bytes accessed | tf_op | source)
XLA Modules:
  0.0 150.5 jit_solution(5341962556700873662)
XLA Ops:
  0.0 147.4 %shard_map.118 = bf16[512,2048]{1,0:T(8,128)(2,1)} custom-call(bf16[1024,1024]{1,0:T(8,128)(2,1)} %bitcast.4, f32[1,2048]{1,0:T(1,128)} %bitcast.5, bf16[3,512]{1,0:T(4,128)(2,1)} %refs_2_.1, f32[8]{0:T(128)} %refs_3_.1, bf16[128,512]{1,0:T(8,128)(2,1)} %refs_4_.1, bf16[128,256]{1,0:T(8,128)(2,1)} %refs_5_.1, bf16[128,256]{1,0:T(8,128)(2,1)} %refs_6_.1, ...), custom_call_target="tpu_custom_call" | custom-call | tf_op jit(solution)/shard_map/pallas_call | solution.py:471
  147.4 3.2 %copy.14 = bf16[1,512,2048]{2,1,0:T(8,128)(2,1)} copy(bf16[1,512,2048]{2,1,0:T(8,128)(2,1)} %bitcast.3) | data formatting | bytes 4194304

commit v2 on v1

--- a/solution.py
+++ b/solution.py
@@ -15,24 +15,99 @@
 BF16, F32 = jnp.bfloat16, jnp.float32
 
 
+TABLE_FOR = (4, 2, 2)
+TABLE = (
+    (0, 1, 0, 0, 0, 2), (0, 1, 0, 0, 0, 3), (0, 2, 0, 0, 0, 3), (0, 2, 0, 0, 0, 2), (0, 1, 1, 0, 0, 3),
+    (0, 0, 0, 0, 0, 2), (0, 0, 0, 0, 0, 1), (0, 1, 0, 0, 0, 1), (0, 0, 0, 1, 0, 2), (0, 1, 0, 0, 0, 0),
+    (0, 0, 0, 0, 0, 3), (0, 0, 0, 0, 0, 0), (0, 8, 0, 0, 0, 1), (0, 2, 0, 1, 1, 2), (0, 7, 0, 0, 0, 3),
+    (0, 4, 0, 0, 0, 2), (0, 1, 1, 0, 0, 2), (0, 1, 0, 1, 0, 2), (0, 0, 0, 1, 0, 3), (0, 7, 0, 0, 0, 0),
+    (0, 0, 0, 1, 1, 0), (0, 4, 0, 0, 0, 1), (0, 0, 0, 2, 0, 3), (0, 3, 0, 0, 0, 3), (0, 8, 0, 0, 0, 0),
+    (0, 2, 0, 0, 0, 1), (0, 5, 0, 0, 0, 0), (0, 1, 0, 1, 0, 1), (0, 1, 1, 0, 0, 1), (0, 0, 0, 1, 1, 2),
+    (0, 0, 0, 1, 1, 1), (0, 3, 0, 1, 1, 2), (0, 1, 1, 0, 0, 0), (0, 4, 0, 0, 0, 0), (0, 0, 1, 0, 0, 0),
+    (0, 6, 0, 0, 0, 3), (0, 6, 0, 0, 0, 2), (0, 2, 0, 1, 0, 2), (0, 0, 0, 1, 0, 1), (0, 4, 0, 1, 1, 2),
+    (0, 3, 0, 0, 0, 1), (0, 2, 0, 0, 0, 0), (0, 0, 1, 0, 0, 1), (0, 0, 0), (0, 4, 0, 0, 0, 3), (0, 1, 1, 1, 1, 0),
+    (0, 2, 0, 1, 1, 0), (0, 0, 0, 2, 1, 1), (0, 1, 0, 2, 0, 3), (0, 2, 0, 1, 0, 1), (0, 8, 1, 0, 0, 1),
+    (0, 3, 0, 2, 1, 1), (0, 2, 1, 0, 0, 0), (0, 1, 1, 1, 1, 2), (0, 0, 1, 0, 0, 3), (0, 1, 1, 1, 0, 2),
+    (0, 1, 0, 1, 1, 2), (0, 2, 0, 2, 1, 1), (0, 5, 0, 0, 0, 3), (0, 7, 0, 0, 0, 1), (0, 1, 1, 1, 0, 3),
+    (0, 6, 1, 0, 0, 3), (0, 0, 0, 3, 1, 0), (0, 3, 0, 0, 0, 0), (0, 8, 0, 0, 0, 2), (0, 3, 0, 3, 1, 0),
+    (0, 5, 0, 1, 0, 1), (0, 2, 1, 1, 1, 2), (0, 0, 0, 2, 0, 2), (0, 1, 0, 2, 0, 2), (0, 4, 0, 1, 0, 3),
+    (0, 6, 0, 0, 0, 0), (0, 0, 0, 2, 1, 0), (0, 1, 1, 1, 0, 1), (0, 4, 1, 1, 0, 3), (0, 8, 0, 1, 0, 2),
+    (0, 8, 0, 0, 0, 3), (0, 2, 1, 0, 0, 2), (0, 0, 1, 3, 1, 0), (0, 1, 1, 2, 1, 1), (0, 1, 0, 1, 1, 0),
+    (0, 4, 1, 0, 0, 2), (0, 2, 0, 2, 0, 2), (0, 4, 0, 1, 0, 1), (0, 0, 1, 2, 1, 1), (1, 3, 0), (1, 0, 0),
+    (0, 1, 0, 2, 1, 1), (0, 3, 0, 0, 0, 2), (0, 6, 1, 0, 0, 0), (0, 2, 0, 2, 0, 3), (0, 8, 1, 0, 0, 2),
+    (0, 8, 1, 1, 0, 3), (0, 8, 0, 2, 0, 3), (0, 8, 1, 0, 0, 0), (0, 0, 1, 2, 0, 2), (0, 3, 0, 1, 1, 1),
+    (0, 8, 0, 1, 1, 2), (0, 1, 1, 2, 0, 2), (0, 1, 0, 1, 1, 1), (0, 3, 0, 1, 0, 1), (0, 7, 1, 0, 0, 0),
+    (0, 5, 0, 0, 0, 2), (0, 8, 1, 0, 0, 3), (0, 7, 0, 1, 1, 2), (0, 0, 1, 1, 0, 2), (0, 2, 0, 3, 1, 0),
+    (0, 1, 0, 3, 0, 3), (0, 4, 1, 0, 0, 0), (0, 3, 0, 2, 1, 0), (0, 8, 1, 1, 1, 1), (0, 3, 0, 2, 0, 2),
+    (0, 2, 0, 1, 0, 3), (0, 2, 0, 1, 1, 1), (0, 5, 1, 1, 0, 1), (0, 1, 0, 1, 0, 3), (0, 0, 1, 2, 0, 3),
+    (0, 4, 0, 2, 1, 1), (0, 1, 1, 1, 1, 1), (0, 2, 1, 3, 1, 0), (0, 8, 1, 1, 0, 1), (0, 0, 0, 3, 0, 3),
+    (0, 2, 1, 1, 0, 1), (0, 0, 1, 1, 0, 3), (1, 1, 0), (0, 8, 0, 2, 0, 2), (0, 4, 1, 0, 0, 3), (0, 2, 0, 3, 0, 3),
+    (0, 1, 0, 2, 1, 0), (0, 7, 1, 0, 0, 3), (0, 3, 0, 3, 0, 3), (0, 3, 1, 3, 1, 0), (0, 8, 1, 1, 0, 2),
+    (1, 8, 1, 0, 0, 0), (0, 8, 0, 1, 0, 1), (0, 3, 0, 1, 1, 0), (0, 5, 1, 0, 0, 0), (0, 4, 0, 1, 1, 1),
+    (0, 0, 1, 0, 0, 2), (0, 1, 1, 3, 0, 3), (0, 1, 0, 3, 1, 0), (0, 0, 1, 3, 0, 3), (0, 7, 0, 1, 0, 1),
+    (0, 5, 1, 0, 0, 2), (0, 8, 1, 2, 0, 2), (0, 0, 1, 1, 1, 2), (0, 2, 1, 2, 0, 3), (0, 6, 0, 0, 0, 1),
+    (0, 5, 0, 2, 0, 2), (0, 0, 1, 1, 1, 0), (0, 8, 0, 2, 1, 1), (0, 0, 1, 2, 1, 0), (0, 5, 0, 0, 0, 1),
+    (0, 3, 1, 0, 0, 1), (0, 0, 1, 1, 1, 1), (0, 6, 0, 1, 1, 2), (0, 4, 1, 2, 1, 1), (0, 0, 1, 1, 0, 1),
+    (0, 3, 1, 0, 0, 2), (0, 1, 1, 3, 1, 0), (0, 1, 1, 2, 0, 3), (1, 8, 0, 0, 0, 0), (1, 2, 0), (0, 5, 1, 0, 0, 3),
+    (2, 0, 0), (0, 8, 0, 1, 0, 3), (0, 3, 1, 0, 0, 0), (0, 8, 0, 1, 1, 1), (0, 2, 0, 2, 1, 0), (0, 4, 1, 1, 1, 2),
+    (0, 2, 1, 3, 0, 3), (0, 8, 1, 1, 1, 2), (0, 5, 0, 1, 0, 3), (0, 5, 0, 1, 1, 1), (0, 3, 1, 2, 0, 2),
+    (0, 2, 1, 1, 1, 0), (0, 3, 0, 1, 0, 2), (0, 8, 0, 3, 0, 3), (0, 3, 1, 0, 0, 3), (0, 5, 0, 1, 1, 2), (2, 2, 0),
+    (0, 4, 0, 3, 1, 0), (1, 8, 0, 1, 0, 1), (0, 4, 0, 2, 0, 2), (0, 8, 1, 2, 1, 1), (0, 8, 1, 3, 0, 3),
+    (0, 6, 0, 1, 1, 1), (0, 1, 1, 2, 1, 0), (0, 3, 1, 3, 0, 3), (1, 8, 0, 2, 1, 1), (0, 4, 0, 1, 0, 2), (2, 1, 0),
+    (2, 3, 0), (0, 4, 0, 1, 1, 0), (0, 5, 0, 3, 0, 3), (0, 2, 1, 0, 0, 1), (0, 6, 0, 1, 0, 1), (0, 3, 0, 1, 0, 3),
+    (0, 7, 0, 2, 1, 1), (2, 2, 1), (2, 3, 1), (1, 8, 1, 0, 0, 2), (3, 3, 0), (0, 2, 1, 1, 0, 2), (2, 1, 1),
+    (1, 8, 0, 1, 1, 1), (0, 3, 1, 1, 1, 1), (0, 6, 1, 1, 1, 2), (2, 0, 1), (0, 4, 0, 2, 1, 0), (0, 5, 1, 2, 0, 2),
+    (0, 8, 0, 3, 1, 0), (0, 7, 0, 1, 0, 2), (0, 4, 1, 3, 1, 0), (0, 2, 1, 2, 0, 2), (0, 8, 1, 2, 1, 0),
+    (0, 6, 0, 1, 1, 0), (1, 8, 0, 2, 0, 3), (0, 3, 1, 1, 0, 2), (0, 8, 0, 1, 1, 0), (0, 2, 1, 2, 1, 1),
+    (0, 5, 0, 1, 1, 0), (0, 5, 1, 3, 0, 3), (1, 8, 1, 2, 1, 1), (0, 3, 1, 2, 1, 0), (0, 5, 1, 1, 0, 3),
+    (1, 8, 0, 0, 0, 2), (1, 8, 0, 1, 1, 2), (0, 7, 1, 1, 1, 2), (0, 3, 1, 1, 0, 1), (0, 3, 0, 2, 0, 3),
+    (0, 6, 0, 2, 0, 2), (0, 5, 1, 1, 1, 2), (0, 3, 1, 2, 1, 1), (0, 8, 1, 2, 0, 3), (1, 8, 1, 2, 0, 2),
+    (1, 8, 0, 1, 0, 3), (1, 8, 1, 3, 0, 3), (0, 4, 0, 3, 0, 3), (0, 2, 1, 0, 0, 3), (0, 7, 0, 0, 0, 2), (3, 1, 0),
+    (0, 4, 0, 2, 0, 3), (1, 8, 1, 0, 0, 3), (0, 3, 1, 1, 0, 3), (0, 3, 1, 1, 1, 2), (1, 8, 1, 0, 0, 1),
+    (0, 3, 1, 1, 1, 0), (3, 2, 0), (0, 5, 1, 1, 1, 1), (0, 2, 1, 1, 0, 3), (1, 8, 0, 0, 0, 3), (0, 4, 1, 0, 0, 1),
+    (0, 6, 0, 1, 0, 2), (0, 6, 1, 1, 1, 0), (0, 8, 1, 3, 1, 0), (0, 8, 0, 2, 1, 0), (3, 0, 0), (0, 3, 1, 2, 0, 3),
+    (0, 7, 0, 1, 1, 0), (0, 6, 1, 0, 0, 2), (0, 4, 1, 1, 1, 0), (0, 2, 1, 1, 1, 1), (0, 4, 1, 1, 0, 1),
+    (0, 4, 1, 1, 1, 1), (0, 4, 1, 1, 0, 2), (0, 2, 1, 2, 1, 0), (0, 6, 0, 1, 0, 3), (1, 8, 0, 3, 1, 0),
+    (0, 5, 0, 2, 1, 1), (1, 8, 1, 2, 1, 0), (0, 4, 1, 2, 0, 2), (4, 0, 0), (0, 4, 1, 2, 1, 0), (2, 0, 3),
+    (0, 7, 0, 2, 0, 3), (2, 3, 3), (2, 1, 2), (0, 7, 1, 2, 1, 1), (0, 5, 1, 0, 0, 1), (1, 8, 0, 2, 0, 2), (2, 3, 2),
+    (0, 5, 0, 2, 1, 0), (0, 7, 0, 2, 0, 2), (0, 4, 1, 2, 0, 3), (2, 2, 3), (0, 4, 1, 3, 0, 3), (1, 8, 1, 1, 0, 1),
+    (0, 6, 0, 3, 0, 3), (0, 7, 1, 0, 0, 1), (0, 5, 1, 2, 1, 1), (2, 1, 3), (0, 6, 0, 2, 1, 1), (2, 3, 4),
+    (1, 8, 0, 1, 0, 2), (2, 0, 2), (0, 7, 1, 0, 0, 2), (0, 7, 0, 1, 0, 3), (0, 5, 0, 3, 1, 0), (1, 8, 1, 2, 0, 3),
+    (2, 0, 4), (0, 7, 1, 1, 0, 2), (2, 1, 4), (0, 5, 0, 1, 0, 2), (1, 8, 1, 1, 0, 2), (2, 2, 2), (0, 7, 1, 2, 0, 2),
+    (0, 7, 0, 3, 0, 3), (0, 6, 0, 2, 1, 0), (0, 6, 1, 1, 0, 3), (0, 5, 1, 2, 1, 0), (1, 8, 0, 0, 0, 1),
+    (0, 6, 1, 1, 0, 1), (0, 6, 1, 0, 0, 1), (1, 8, 0, 1, 1, 0), (0, 7, 1, 1, 1, 0), (0, 7, 1, 1, 0, 1), (2, 2, 4),
+    (5, 0, 0), (0, 6, 0, 3, 1, 0), (0, 6, 1, 2, 1, 0), (1, 8, 1, 1, 1, 1), (0, 7, 1, 2, 0, 3), (0, 5, 1, 1, 1, 0),
+    (0, 6, 0, 2, 0, 3), (0, 5, 0, 2, 0, 3), (0, 6, 1, 2, 0, 2), (0, 6, 1, 1, 1, 1), (0, 7, 0, 3, 1, 0),
+    (1, 8, 1, 1, 0, 3), (0, 7, 0, 2, 1, 0), (0, 6, 1, 2, 1, 1), (0, 8, 1, 1, 1, 0), (0, 7, 1, 3, 1, 0),
+    (1, 8, 0, 2, 1, 0), (0, 6, 1, 3, 1, 0), (0, 7, 0, 1, 1, 1), (0, 6, 1, 3, 0, 3), (7, 0, 0), (0, 6, 1, 2, 0, 3),
+    (0, 6, 1, 1, 0, 2), (0, 7, 1, 1, 0, 3), (0, 5, 1, 2, 0, 3), (0, 5, 1, 3, 1, 0), (1, 8, 1, 1, 1, 2),
+    (0, 7, 1, 1, 1, 1), (1, 8, 1, 3, 1, 0), (0, 7, 1, 3, 0, 3), (0, 5, 1, 1, 0, 2), (7, 2, 0), (7, 1, 1), (7, 1, 0),
+    (7, 3, 1), (7, 3, 0), (1, 8, 0, 3, 0, 3), (0, 7, 1, 2, 1, 0), (7, 2, 1), (6, 0, 0), (8, 2, 1), (1, 8, 1, 1, 1, 0),
+    (8, 0, 0), (8, 3, 1), (8, 3, 0), (8, 1, 1), (8, 1, 0), (8, 2, 0),
+)
+
+
 def when(condition, body):
     if condition is True:
         body()
-    else:
+    elif condition is not False:
         pl.when(condition)(body)
 
 
 class Part:
-    def __init__(self, number, wide, place, base):
-        self.number, self.wide, self.place, self.base = number, wide, place, base
+    def __init__(self, number, wide, crossing, place, base):
+        self.number, self.wide, self.crossing, self.place, self.base = number, wide, crossing, place, base
 
 
 def part_kinds(out_rows):
-    kinds = [(False, None), (True, None), (False, None), (False, None), (False, None)]
-    quarter, eighth = out_rows // 4, out_rows // 8
-    kinds += [(False, (n * quarter, quarter)) for n in range(3)]
-    kinds += [(True, (3 * quarter, eighth)), (False, (3 * quarter + eighth, eighth))]
-    return kinds
+    kinds = [(False, False, None), (True, False, None)] + [(False, False, None)] * 3
+    quarter = out_rows // 4
+    kinds += [(False, False, (n * quarter, quarter)) for n in range(3)]
+    return kinds + [(True, True, (3 * quarter, quarter))]
+
+
+def lanes_of(wide, n_out):
+    return 1 + n_out + (2 if wide else 1) * (n_out - 1)
 
 
 def layer_kernel(sizes, *refs):
@@ -44,7 +119,7 @@
     out = refs[6 + n_in]
     (tokf, w_all, wo_all, q_buf, kv_buf, inner, gate_b, product, m_att, m_conv, r_att, r_conv, bias,
      send_sem, recv_sem, own_sem, wo_send, wo_recv, tok_send, tok_recv, halo_send, halo_recv,
-     mix_send, mix_recv) = refs[7 + n_in :]
+     mix_send, mix_recv, cross_send, cross_recv, pass_send, pass_recv) = refs[7 + n_in :]
     n_fs = 2 * n_out
     shards = n_sp * n_fs
     s, f, t = lax.axis_index("sp"), lax.axis_index("fs"), lax.axis_index("tp")
@@ -88,10 +163,11 @@
     pl.semaphore_wait(barrier, count + has_right.astype(jnp.int32) + has_left.astype(jnp.int32))
 
     wo_copies, tok_copies = [], {}
+    direct = pl.ds(0, 3 * (out_rows // 4))
     for k, peer in enumerate(peers):
         for a in range(2):
             copy = pltpu.make_async_remote_copy(
-                src_ref=out_own[a], dst_ref=wo_all.at[2 * t + a, me],
+                src_ref=out_own[a].at[direct], dst_ref=wo_all.at[2 * t + a, me, direct],
                 send_sem=wo_send.at[k, a], recv_sem=wo_recv.at[k, a], device_id=peer, device_id_type=MESH,
             )
             copy.start()
@@ -107,75 +183,95 @@
             tok_copies[k, n] = copy
 
     parts, base = [], 0
-    for number, (wide, rows) in enumerate(part_kinds(out_rows)):
+    for number, (wide, crossing, rows) in enumerate(part_kinds(out_rows)):
         if rows is None:
-            place = lambda src, number=number: w_all.at[number, pl.ds(src * k_rows, k_rows)]
+            place = lambda src, g, number=number: w_all.at[number, pl.ds(src * k_rows, k_rows)]
+        elif crossing:
+            place = lambda src, g, rows=rows: wo_all.at[pl.ds(2 * g, 2), src, pl.ds(*rows)]
         else:
-            place = lambda src, rows=rows: wo_all.at[:, src, pl.ds(*rows)]
-        parts.append(Part(number, wide, place, base))
-        base += (5 if wide else 4) * n_sp * 2 if n_out > 1 else 2 * n_sp * 2
+            place = lambda src, g, rows=rows: wo_all.at[:, src, pl.ds(*rows)]
+        parts.append(Part(number, wide, crossing, place, base))
+        base += lanes_of(wide, n_out) * n_sp * 2
 
     def copy_of(part, src, where, lane, distance, side):
-        spot = part.place(src)
+        spot = part.place(src, t)
         return pltpu.make_async_remote_copy(
             src_ref=spot, dst_ref=spot,
-            send_sem=send_sem.at[part.base + lane * n_sp * 2 + distance * 2 + side],
+            send_sem=send_sem.at[part.base + (lane * n_sp + distance) * 2 + side],
             recv_sem=recv_sem.at[part.number * shards + src],
             device_id=where, device_id_type=MESH,
         )
 
+    def cross_copy(part, src, k):
+        spot = part.place(src, t)
+        return pltpu.make_async_remote_copy(
+            src_ref=spot, dst_ref=spot, send_sem=cross_send.at[k, src], recv_sem=cross_recv.at[k, src],
+            device_id=peers[k], device_id_type=MESH,
+        )
+
+    def pass_copy(part, src, k):
+        spot = part.place(src, lax.rem(t + n_tp - k - 1, n_tp))
+        return pltpu.make_async_remote_copy(
+            src_ref=spot, dst_ref=spot, send_sem=pass_send.at[k, src], recv_sem=pass_recv.at[k, src],
+            device_id=core, device_id_type=MESH,
+        )
+
+    def source(k, at):
+        return at * n_fs + lax.rem(o + n_out - k, n_out) * 2 + i
+
+    def handle(part, k, distance, side, at, drain):
+        first = isinstance(distance, int) and distance == 0
+        src = source(k, at)
+        mine = (at + distance if side == 0 else at - distance) if isinstance(at, int) else s
+        more_right, more_left = mine < n_sp - 1, mine > 0
+        lane_z, lane_core = 0, 1
+        if k > 0:
+            lane_z = 2 + len(across) + 2 * (k - 1)
+            lane_core = lane_z + 1
+            if not part.wide:
+                lane_core = 2 + len(across) + k - 1
+
+        def go(where, lane, way):
+            copy = copy_of(part, src, where, lane, distance, way)
+            copy.wait_send() if drain else copy.start()
+
+        if not (first and k == 0) and not drain:
+            copy_of(part, src, core, 0, 0, 0).wait_recv()
+        if k == 0 or part.wide:
+            if first or side == 0:
+                when(more_right, lambda: go(right, lane_z, 0))
+            if first or side == 1:
+                when(more_left, lambda: go(left, lane_z, 1))
+        if k == 0 and (first or not part.wide):
+            for n, where in enumerate(across):
+                go(where, 2 + n, side)
+        if part.crossing:
+            for n in range(len(peers)):
+                copy = cross_copy(part, src, n)
+                copy.wait_send() if drain else copy.start()
+        go(core, lane_core, side)
+
+    def hand_over(part, src, drain):
+        for k in range(len(peers)):
+            if not drain:
+                cross_copy(part, src, k).wait_recv()
+            copy = pass_copy(part, src, k)
+            copy.wait_send() if drain else copy.start()
+
     def deal(part, distance, k, drain):
-        ys = [(2 + n, where) for n, where in enumerate(across)]
-        lanes = 0 if k == 0 else 2 + (len(across) if part.wide else len(across) - 1) + 2 * (k - 1) + (0 if part.wide else 1)
-        lane_z, lane_core = (0, 1) if k == 0 else (lanes, lanes + (1 if part.wide else 0))
-        source_o = lax.rem(o + n_out - k, n_out)
-        first = isinstance(distance, int) and distance == 0
-        for side in (0,) if first else (0, 1):
-            source_s = s if first else (s - distance if side == 0 else s + distance)
-            there = True if first else (source_s >= 0 if side == 0 else source_s < n_sp)
-            src = source_s * n_fs + source_o * 2 + i
-
-            def body(side=side, src=src):
-                def go(where, lane, at):
-                    copy = copy_of(part, src, where, lane, distance, at)
-                    copy.wait_send() if drain else copy.start()
-
-                if not (first and k == 0) and not drain:
-                    copy_of(part, src, core, 0, 0, 0).wait_recv()
-                if k == 0 or part.wide:
-                    if first or side == 0:
-                        when(has_right, lambda: go(right, lane_z, 0))
-                    if first or side == 1:
-                        when(has_left, lambda: go(left, lane_z, 1))
-                if k == 0 and (first or not part.wide):
-                    for lane, where in ys:
-                        go(where, lane, side)
-                go(core, lane_core, side)
-
-            when(there, body)
-
-    def stage(number, n):
-        part = parts[number]
-        last = n_sp - 1
-        if not (isinstance(n, int) and n > last):
-            deal(part, n, 0, False)
-        if isinstance(n, int) and n == 0:
+        if isinstance(distance, int) and distance == 0:
+            handle(part, k, 0, 0, s, drain)
             return
-        for k in range(1, n_out):
-            deal(part, n - 1, k, False)
+        when(s - distance >= 0, lambda: handle(part, k, distance, 0, s - distance, drain))
+        when(s + distance < n_sp, lambda: handle(part, k, distance, 1, s + distance, drain))
 
     def partner(number, source_s):
-        part = parts[number]
         for source_o in range(n_out):
-            copy_of(part, source_s * n_fs + source_o * 2 + (1 - i), core, 0, 0, 0).wait_recv()
+            copy_of(parts[number], source_s * n_fs + source_o * 2 + (1 - i), core, 0, 0, 0).wait_recv()
 
     def finish(number):
         for source_s in range(n_sp):
             partner(number, source_s)
-
-    def tokens_in(n):
-        for k in range(n_tp - 1):
-            tok_copies[k, n].wait_recv()
 
     def norm(n):
         size = 32
@@ -315,9 +411,14 @@
             for k in range(n_tp - 1):
                 mix_copy(which, k).wait_recv()
 
-    def project_out(source_s):
+    def project_out(source_s, own):
         for number in range(n_proj, len(parts)):
-            partner(number, source_s)
+            if own:
+                partner(number, source_s)
+            elif parts[number].crossing:
+                for source_o in range(n_out):
+                    for k in range(n_tp - 1):
+                        pass_copy(parts[number], source_s * n_fs + source_o * 2 + (1 - i), k).wait_recv()
         block = n_fs * out_cols
         tile = min(256, owned)
 
@@ -326,120 +427,161 @@
             return jnp.concatenate(blocks, axis=1)
 
         def body(r, carry):
-            total = jnp.zeros((tile, block), F32)
-            for k in range(n_tp):
+            here = pl.ds(pl.multiple_of(r * tile, tile), tile)
+            where = pl.ds(pl.multiple_of(source_s * block, block), block)
+            total = None if own else out[here, where].astype(F32)
+            for k in (0,) if own else range(1, n_tp):
                 g = lax.rem(t + n_tp - k, n_tp)
-                if k == 0:
-                    here = pl.ds(pl.multiple_of(t * owned + r * tile, tile), tile)
-                    att, conv = m_att[here, :], m_conv[here, :]
+                if own:
+                    mine = pl.ds(pl.multiple_of(t * owned + r * tile, tile), tile)
+                    att, conv = m_att[mine, :], m_conv[mine, :]
                 else:
-                    here = pl.ds(pl.multiple_of(r * tile, tile), tile)
                     att, conv = r_att[k - 1, here, :], r_conv[k - 1, here, :]
                 partial = jnp.dot(att, weights(2 * g), preferred_element_type=F32)
                 partial = partial + jnp.dot(conv, weights(2 * g + 1), preferred_element_type=F32)
-                total = total + partial.astype(BF16).astype(F32)
-            where = pl.ds(pl.multiple_of(source_s * block, block), block)
-            out[pl.ds(pl.multiple_of(r * tile, tile), tile), where] = total.astype(BF16)
+                total = partial if own else total + partial.astype(BF16).astype(F32)
+            out[here, where] = total.astype(BF16)
             return carry
 
         lax.fori_loop(0, owned // tile, body, 0)
 
-    def first_chunk():
-        tokens_in(order[0])
-        norm(order[0])
-        project(0, [order[0]])
-        project(1, [order[0]])
-        halo_out(0)
-
-    def chunk(n):
-        tokens_in(n)
-        norm(n)
-        project(0, [n])
-        project(1, [n])
+    own_weights, own_out, own_tokens = local[:-3], local[-3:-1], local[-1]
+    waited = set()
+
+    def once(key, body):
+        if key not in waited:
+            waited.add(key)
+            body()
+
+    def wait_all(copies):
+        for copy in copies:
+            copy.wait()
 
     def wo_ready():
         for copy in wo_copies:
             copy.wait_recv()
 
-    for copy in local[:6] if separate else local[:5]:
-        copy.wait()
-    if n_sp <= 4:
-        work = {
-            (0, 1): [make_bias],
-            (0, 2): [local[-3].wait, local[-2].wait, local[-1].wait, wo_ready],
-            (2, 1): [first_chunk],
-            (3, 1): [lambda: chunk(0)],
-            (3, 2): [lambda: halo_in(0), lambda: attend(0)],
-            (3, 3): [lambda: project(2, [3]), lambda: project(2, [0])],
-            (4, 1): [lambda: chunk(1)],
-            (4, 2): [lambda: attend(1)],
-            (4, 3): [lambda: project(2, [1]), lambda: project(3, [0, 1]), lambda: project(3, [3])],
-            (5, 1): [lambda: chunk(2)],
-            (5, 2): [lambda: attend(2)],
-            (5, 3): [lambda: attend(3), lambda: mix_out(0)],
-            (6, 1): [lambda: project(2, [2]), lambda: project(3, [2]), lambda: project(4, [0, 1, 2, 3]), lambda: halo_out(1)],
-            (6, 2): [lambda: halo_in(1), convolve, lambda: mix_out(1)],
-        }
-        total = len(parts)
-        stage(0, 0)
-        for number in range(total):
+    def job(kind, n, side):
+        if kind == 0:
+            make_bias()
+        elif kind == 1:
+            once("tokens", own_tokens.wait)
+            for k in range(n_tp - 1):
+                tok_copies[k, n].wait_recv()
+            norm(n)
+        elif kind == 2:
+            once(("part", side), lambda: finish(side))
+            project(side, [n])
+            if n == chunks - 1 and side in (1, 4):
+                halo_out(0 if side == 1 else 1)
+        elif kind == 3:
+            if n == 0:
+                halo_in(0)
+            attend(n)
+        elif kind == 4:
+            mix_out(0)
+        elif kind == 5:
+            halo_in(1)
+            convolve()
+            mix_out(1)
+        elif kind == 6:
+            mix_in()
+        elif n == 0:
+            project_out(s, kind == 7)
+        elif side == 0:
+            when(s - n >= 0, lambda: project_out(s - n, kind == 7))
+        else:
+            when(s + n < n_sp, lambda: project_out(s + n, kind == 7))
+
+    wait_all(own_weights)
+    tabled = (n_sp, n_out, n_tp) == TABLE_FOR
+    if tabled:
+        events = []
+
+        def flush():
+            for mine in range(n_sp):
+                turn = [entry for entry in events if entry[5] == mine]
+
+                def body(mine=mine, turn=turn):
+                    for passing, number, k, distance, side, _ in turn:
+                        part = parts[number]
+                        at = mine - distance if side == 0 else mine + distance
+                        if passing:
+                            hand_over(part, source(k, at), False)
+                            continue
+                        if distance == 0 and k == 0 and number >= n_proj:
+                            once(("own", mine), lambda: wait_all(own_out))
+                            if not part.crossing:
+                                once(("direct", mine), wo_ready)
+                        handle(part, k, distance, side, at, False)
+
+                if turn:
+                    pl.when(s == mine)(body)
+            events.clear()
+
+        for entry in TABLE:
+            if len(entry) == 6:
+                events.append(entry)
+            else:
+                flush()
+                job(*entry)
+        flush()
+    else:
+        wait_all(own_out)
+        wo_ready()
+
+        def spread(part):
+            deal(part, 0, 0, False)
             for n in range(1, n_sp + 1):
-                stage(number, n)
-                if n == 1 and number + 1 < total:
-                    stage(number + 1, 0)
-                for job in work.get((number, n), []):
-                    job()
-                if number == total - 1:
-                    if n == 1:
-                        mix_in()
-                        project_out(s)
-                    if n > 1:
-                        d = n - 1
-                        when(s - d >= 0, lambda: project_out(s - d))
-                        when(s + d < n_sp, lambda: project_out(s + d))
-            if number < n_proj:
-                finish(number)
+                if n < n_sp:
+                    deal(part, n, 0, False)
+                for k in range(1, n_out):
+                    deal(part, n - 1, k, False)
+
+        for part in parts[:n_proj]:
+            spread(part)
+        job(0, 0, 0)
+        for n in order:
+            job(1, n, 0)
+            job(2, n, 0)
+            job(2, n, 1)
+        for n in range(chunks):
+            job(3, n, 0)
+        job(4, 0, 0)
+        for number in (2, 3, 4):
+            for n in order:
+                job(2, n, number)
+        job(5, 0, 0)
+        for part in parts[n_proj:]:
+            spread(part)
+        for at in range(n_sp):
+            for k in range(n_out):
+                hand_over(parts[-1], source(k, at), False)
+        job(6, 0, 0)
+        for own in (True, False):
+            lax.fori_loop(0, n_sp, lambda n, c, own=own: (project_out(n, own), c)[1], 0)
+
+    if tabled:
+        events = [entry for entry in TABLE if len(entry) == 6]
+        for mine in range(n_sp):
+
+            def drain(mine=mine):
+                for passing, number, k, distance, side, _ in [entry for entry in events if entry[5] == mine]:
+                    at = mine - distance if side == 0 else mine + distance
+                    if passing:
+                        hand_over(parts[number], source(k, at), True)
+                    else:
+                        handle(parts[number], k, distance, side, at, True)
+
+            pl.when(s == mine)(drain)
     else:
-        for copy in local[-3:]:
-            copy.wait()
-        wo_ready()
-
-        def spread(number):
-            stage(number, 0)
-            stage(number, 1)
-            lax.fori_loop(2, n_sp, lambda n, c: (stage(number, n), c)[1], 0)
-            stage(number, n_sp)
-
-        for number in range(n_proj):
-            spread(number)
-            finish(number)
-        make_bias()
-        first_chunk()
-        for n in order[1:]:
-            chunk(n)
-        halo_in(0)
-        for n in range(chunks):
-            attend(n)
-        mix_out(0)
-        for number in (2, 3, 4):
-            project(number, list(range(chunks)))
-        halo_out(1)
-        halo_in(1)
-        convolve()
-        mix_out(1)
-        for number in range(n_proj, len(parts)):
-            spread(number)
-        mix_in()
-        lax.fori_loop(0, n_sp, lambda n, c: (project_out(n), c)[1], 0)
-
-    for part in parts:
-        for k in range(n_out):
-            deal(part, 0, k, True)
-            if n_sp <= 4:
-                for distance in range(1, n_sp):
+        for part in parts:
+            for k in range(n_out):
+                for distance in range(n_sp):
                     deal(part, distance, k, True)
-            else:
-                lax.fori_loop(1, n_sp, lambda n, c, part=part, k=k: (deal(part, n, k, True), c)[1], 0)
+        for at in range(n_sp):
+            for k in range(n_out):
+                hand_over(parts[-1], source(k, at), True)
     for which in range(2):
         when(has_right, lambda which=which: halo_copy(which).wait_send())
         for k in range(n_tp - 1):
@@ -463,7 +605,7 @@
     weights += [w_conv_in, w_conv_b, w_conv_c]
     owned = rows // n_tp
     kinds = part_kinds(out_rows)
-    lanes = sum((5 if wide else 4) if n_out > 1 else 2 for wide, _ in kinds)
+    lanes = sum(lanes_of(wide, n_out) for wide, _, _ in kinds)
     kv_here = kv_cols // HEAD
     group = q_cols // kv_cols
     dma = pltpu.SemaphoreType.DMA
@@ -498,6 +640,10 @@
             dma((2,)),
             dma((2, n_tp - 1)),
             dma((2, n_tp - 1)),
+            dma((n_tp - 1, shards)),
+            dma((n_tp - 1, shards)),
+            dma((n_tp - 1, shards)),
+            dma((n_tp - 1, shards)),
         ],
         compiler_params=pltpu.CompilerParams(
             collective_id=0, has_side_effects=True, vmem_limit_bytes=60 * 1024 * 1024

time: 151 us -> 120 us (0.79)
  Pallas kernels: 147 us -> 117 us
    pallas_call x1, Pallas kernels: 147 us -> 117 us  [on_device(): pl.pallas_call(functools.partial(layer_kernel, (n_sp, n_out, n_tp, 5, sep...]
where the time goes in v2:
time: 120 us
  Pallas kernels  117 us (98%)
  local copies, waits for them, and re-layouts  3.16 us (3%)
    pallas_call x1, Pallas kernels, on_device(): pl.pallas_call(functools.partial(layer_kernel, (n_sp, n_out, n_tp, 5, sep...  117 us
    unnamed x1, local copies, waits for them, and re-layouts  3.16 us

profile of v2, /device:TPU:0, one launch (start us, length us, event | category | flops | bytes accessed | tf_op | source)
XLA Modules:
  0.0 119.9 jit_solution(3722709325958397511)
XLA Ops:
  0.0 116.8 %shard_map.118 = bf16[512,2048]{1,0:T(8,128)(2,1)} custom-call(bf16[1024,1024]{1,0:T(8,128)(2,1)} %bitcast.4, f32[1,2048]{1,0:T(1,128)} %bitcast.5, bf16[3,512]{1,0:T(4,128)(2,1)} %refs_2_.1, f32[8]{0:T(128)} %refs_3_.1, bf16[128,512]{1,0:T(8,128)(2,1)} %refs_4_.1, bf16[128,256]{1,0:T(8,128)(2,1)} %refs_5_.1, bf16[128,256]{1,0:T(8,128)(2,1)} %refs_6_.1, ...), custom_call_target="tpu_custom_call" | custom-call | tf_op jit(solution)/shard_map/pallas_call | solution.py:613
  116.8 3.2 %copy.14 = bf16[1,512,2048]{2,1,0:T(8,128)(2,1)} copy(bf16[1,512,2048]{2,1,0:T(8,128)(2,1)} %bitcast.3) | data formatting | bytes 4194304

commit v3 on v2

--- a/solution.py
+++ b/solution.py
@@ -12,78 +12,137 @@
 WINDOW = 128
 HALO = 16
 MESH = pl.DeviceIdType.MESH
+DIRECT_AFTER = 0
+WAYS = RIGHT, LEFT, ACROSS, CROSS, CORE, HAND = range(6)
 BF16, F32 = jnp.bfloat16, jnp.float32
 
 
 TABLE_FOR = (4, 2, 2)
 TABLE = (
-    (0, 1, 0, 0, 0, 2), (0, 1, 0, 0, 0, 3), (0, 2, 0, 0, 0, 3), (0, 2, 0, 0, 0, 2), (0, 1, 1, 0, 0, 3),
-    (0, 0, 0, 0, 0, 2), (0, 0, 0, 0, 0, 1), (0, 1, 0, 0, 0, 1), (0, 0, 0, 1, 0, 2), (0, 1, 0, 0, 0, 0),
-    (0, 0, 0, 0, 0, 3), (0, 0, 0, 0, 0, 0), (0, 8, 0, 0, 0, 1), (0, 2, 0, 1, 1, 2), (0, 7, 0, 0, 0, 3),
-    (0, 4, 0, 0, 0, 2), (0, 1, 1, 0, 0, 2), (0, 1, 0, 1, 0, 2), (0, 0, 0, 1, 0, 3), (0, 7, 0, 0, 0, 0),
-    (0, 0, 0, 1, 1, 0), (0, 4, 0, 0, 0, 1), (0, 0, 0, 2, 0, 3), (0, 3, 0, 0, 0, 3), (0, 8, 0, 0, 0, 0),
-    (0, 2, 0, 0, 0, 1), (0, 5, 0, 0, 0, 0), (0, 1, 0, 1, 0, 1), (0, 1, 1, 0, 0, 1), (0, 0, 0, 1, 1, 2),
-    (0, 0, 0, 1, 1, 1), (0, 3, 0, 1, 1, 2), (0, 1, 1, 0, 0, 0), (0, 4, 0, 0, 0, 0), (0, 0, 1, 0, 0, 0),
-    (0, 6, 0, 0, 0, 3), (0, 6, 0, 0, 0, 2), (0, 2, 0, 1, 0, 2), (0, 0, 0, 1, 0, 1), (0, 4, 0, 1, 1, 2),
-    (0, 3, 0, 0, 0, 1), (0, 2, 0, 0, 0, 0), (0, 0, 1, 0, 0, 1), (0, 0, 0), (0, 4, 0, 0, 0, 3), (0, 1, 1, 1, 1, 0),
-    (0, 2, 0, 1, 1, 0), (0, 0, 0, 2, 1, 1), (0, 1, 0, 2, 0, 3), (0, 2, 0, 1, 0, 1), (0, 8, 1, 0, 0, 1),
-    (0, 3, 0, 2, 1, 1), (0, 2, 1, 0, 0, 0), (0, 1, 1, 1, 1, 2), (0, 0, 1, 0, 0, 3), (0, 1, 1, 1, 0, 2),
-    (0, 1, 0, 1, 1, 2), (0, 2, 0, 2, 1, 1), (0, 5, 0, 0, 0, 3), (0, 7, 0, 0, 0, 1), (0, 1, 1, 1, 0, 3),
-    (0, 6, 1, 0, 0, 3), (0, 0, 0, 3, 1, 0), (0, 3, 0, 0, 0, 0), (0, 8, 0, 0, 0, 2), (0, 3, 0, 3, 1, 0),
-    (0, 5, 0, 1, 0, 1), (0, 2, 1, 1, 1, 2), (0, 0, 0, 2, 0, 2), (0, 1, 0, 2, 0, 2), (0, 4, 0, 1, 0, 3),
-    (0, 6, 0, 0, 0, 0), (0, 0, 0, 2, 1, 0), (0, 1, 1, 1, 0, 1), (0, 4, 1, 1, 0, 3), (0, 8, 0, 1, 0, 2),
-    (0, 8, 0, 0, 0, 3), (0, 2, 1, 0, 0, 2), (0, 0, 1, 3, 1, 0), (0, 1, 1, 2, 1, 1), (0, 1, 0, 1, 1, 0),
-    (0, 4, 1, 0, 0, 2), (0, 2, 0, 2, 0, 2), (0, 4, 0, 1, 0, 1), (0, 0, 1, 2, 1, 1), (1, 3, 0), (1, 0, 0),
-    (0, 1, 0, 2, 1, 1), (0, 3, 0, 0, 0, 2), (0, 6, 1, 0, 0, 0), (0, 2, 0, 2, 0, 3), (0, 8, 1, 0, 0, 2),
-    (0, 8, 1, 1, 0, 3), (0, 8, 0, 2, 0, 3), (0, 8, 1, 0, 0, 0), (0, 0, 1, 2, 0, 2), (0, 3, 0, 1, 1, 1),
-    (0, 8, 0, 1, 1, 2), (0, 1, 1, 2, 0, 2), (0, 1, 0, 1, 1, 1), (0, 3, 0, 1, 0, 1), (0, 7, 1, 0, 0, 0),
-    (0, 5, 0, 0, 0, 2), (0, 8, 1, 0, 0, 3), (0, 7, 0, 1, 1, 2), (0, 0, 1, 1, 0, 2), (0, 2, 0, 3, 1, 0),
-    (0, 1, 0, 3, 0, 3), (0, 4, 1, 0, 0, 0), (0, 3, 0, 2, 1, 0), (0, 8, 1, 1, 1, 1), (0, 3, 0, 2, 0, 2),
-    (0, 2, 0, 1, 0, 3), (0, 2, 0, 1, 1, 1), (0, 5, 1, 1, 0, 1), (0, 1, 0, 1, 0, 3), (0, 0, 1, 2, 0, 3),
-    (0, 4, 0, 2, 1, 1), (0, 1, 1, 1, 1, 1), (0, 2, 1, 3, 1, 0), (0, 8, 1, 1, 0, 1), (0, 0, 0, 3, 0, 3),
-    (0, 2, 1, 1, 0, 1), (0, 0, 1, 1, 0, 3), (1, 1, 0), (0, 8, 0, 2, 0, 2), (0, 4, 1, 0, 0, 3), (0, 2, 0, 3, 0, 3),
-    (0, 1, 0, 2, 1, 0), (0, 7, 1, 0, 0, 3), (0, 3, 0, 3, 0, 3), (0, 3, 1, 3, 1, 0), (0, 8, 1, 1, 0, 2),
-    (1, 8, 1, 0, 0, 0), (0, 8, 0, 1, 0, 1), (0, 3, 0, 1, 1, 0), (0, 5, 1, 0, 0, 0), (0, 4, 0, 1, 1, 1),
-    (0, 0, 1, 0, 0, 2), (0, 1, 1, 3, 0, 3), (0, 1, 0, 3, 1, 0), (0, 0, 1, 3, 0, 3), (0, 7, 0, 1, 0, 1),
-    (0, 5, 1, 0, 0, 2), (0, 8, 1, 2, 0, 2), (0, 0, 1, 1, 1, 2), (0, 2, 1, 2, 0, 3), (0, 6, 0, 0, 0, 1),
-    (0, 5, 0, 2, 0, 2), (0, 0, 1, 1, 1, 0), (0, 8, 0, 2, 1, 1), (0, 0, 1, 2, 1, 0), (0, 5, 0, 0, 0, 1),
-    (0, 3, 1, 0, 0, 1), (0, 0, 1, 1, 1, 1), (0, 6, 0, 1, 1, 2), (0, 4, 1, 2, 1, 1), (0, 0, 1, 1, 0, 1),
-    (0, 3, 1, 0, 0, 2), (0, 1, 1, 3, 1, 0), (0, 1, 1, 2, 0, 3), (1, 8, 0, 0, 0, 0), (1, 2, 0), (0, 5, 1, 0, 0, 3),
-    (2, 0, 0), (0, 8, 0, 1, 0, 3), (0, 3, 1, 0, 0, 0), (0, 8, 0, 1, 1, 1), (0, 2, 0, 2, 1, 0), (0, 4, 1, 1, 1, 2),
-    (0, 2, 1, 3, 0, 3), (0, 8, 1, 1, 1, 2), (0, 5, 0, 1, 0, 3), (0, 5, 0, 1, 1, 1), (0, 3, 1, 2, 0, 2),
-    (0, 2, 1, 1, 1, 0), (0, 3, 0, 1, 0, 2), (0, 8, 0, 3, 0, 3), (0, 3, 1, 0, 0, 3), (0, 5, 0, 1, 1, 2), (2, 2, 0),
-    (0, 4, 0, 3, 1, 0), (1, 8, 0, 1, 0, 1), (0, 4, 0, 2, 0, 2), (0, 8, 1, 2, 1, 1), (0, 8, 1, 3, 0, 3),
-    (0, 6, 0, 1, 1, 1), (0, 1, 1, 2, 1, 0), (0, 3, 1, 3, 0, 3), (1, 8, 0, 2, 1, 1), (0, 4, 0, 1, 0, 2), (2, 1, 0),
-    (2, 3, 0), (0, 4, 0, 1, 1, 0), (0, 5, 0, 3, 0, 3), (0, 2, 1, 0, 0, 1), (0, 6, 0, 1, 0, 1), (0, 3, 0, 1, 0, 3),
-    (0, 7, 0, 2, 1, 1), (2, 2, 1), (2, 3, 1), (1, 8, 1, 0, 0, 2), (3, 3, 0), (0, 2, 1, 1, 0, 2), (2, 1, 1),
-    (1, 8, 0, 1, 1, 1), (0, 3, 1, 1, 1, 1), (0, 6, 1, 1, 1, 2), (2, 0, 1), (0, 4, 0, 2, 1, 0), (0, 5, 1, 2, 0, 2),
-    (0, 8, 0, 3, 1, 0), (0, 7, 0, 1, 0, 2), (0, 4, 1, 3, 1, 0), (0, 2, 1, 2, 0, 2), (0, 8, 1, 2, 1, 0),
-    (0, 6, 0, 1, 1, 0), (1, 8, 0, 2, 0, 3), (0, 3, 1, 1, 0, 2), (0, 8, 0, 1, 1, 0), (0, 2, 1, 2, 1, 1),
-    (0, 5, 0, 1, 1, 0), (0, 5, 1, 3, 0, 3), (1, 8, 1, 2, 1, 1), (0, 3, 1, 2, 1, 0), (0, 5, 1, 1, 0, 3),
-    (1, 8, 0, 0, 0, 2), (1, 8, 0, 1, 1, 2), (0, 7, 1, 1, 1, 2), (0, 3, 1, 1, 0, 1), (0, 3, 0, 2, 0, 3),
-    (0, 6, 0, 2, 0, 2), (0, 5, 1, 1, 1, 2), (0, 3, 1, 2, 1, 1), (0, 8, 1, 2, 0, 3), (1, 8, 1, 2, 0, 2),
-    (1, 8, 0, 1, 0, 3), (1, 8, 1, 3, 0, 3), (0, 4, 0, 3, 0, 3), (0, 2, 1, 0, 0, 3), (0, 7, 0, 0, 0, 2), (3, 1, 0),
-    (0, 4, 0, 2, 0, 3), (1, 8, 1, 0, 0, 3), (0, 3, 1, 1, 0, 3), (0, 3, 1, 1, 1, 2), (1, 8, 1, 0, 0, 1),
-    (0, 3, 1, 1, 1, 0), (3, 2, 0), (0, 5, 1, 1, 1, 1), (0, 2, 1, 1, 0, 3), (1, 8, 0, 0, 0, 3), (0, 4, 1, 0, 0, 1),
-    (0, 6, 0, 1, 0, 2), (0, 6, 1, 1, 1, 0), (0, 8, 1, 3, 1, 0), (0, 8, 0, 2, 1, 0), (3, 0, 0), (0, 3, 1, 2, 0, 3),
-    (0, 7, 0, 1, 1, 0), (0, 6, 1, 0, 0, 2), (0, 4, 1, 1, 1, 0), (0, 2, 1, 1, 1, 1), (0, 4, 1, 1, 0, 1),
-    (0, 4, 1, 1, 1, 1), (0, 4, 1, 1, 0, 2), (0, 2, 1, 2, 1, 0), (0, 6, 0, 1, 0, 3), (1, 8, 0, 3, 1, 0),
-    (0, 5, 0, 2, 1, 1), (1, 8, 1, 2, 1, 0), (0, 4, 1, 2, 0, 2), (4, 0, 0), (0, 4, 1, 2, 1, 0), (2, 0, 3),
-    (0, 7, 0, 2, 0, 3), (2, 3, 3), (2, 1, 2), (0, 7, 1, 2, 1, 1), (0, 5, 1, 0, 0, 1), (1, 8, 0, 2, 0, 2), (2, 3, 2),
-    (0, 5, 0, 2, 1, 0), (0, 7, 0, 2, 0, 2), (0, 4, 1, 2, 0, 3), (2, 2, 3), (0, 4, 1, 3, 0, 3), (1, 8, 1, 1, 0, 1),
-    (0, 6, 0, 3, 0, 3), (0, 7, 1, 0, 0, 1), (0, 5, 1, 2, 1, 1), (2, 1, 3), (0, 6, 0, 2, 1, 1), (2, 3, 4),
-    (1, 8, 0, 1, 0, 2), (2, 0, 2), (0, 7, 1, 0, 0, 2), (0, 7, 0, 1, 0, 3), (0, 5, 0, 3, 1, 0), (1, 8, 1, 2, 0, 3),
-    (2, 0, 4), (0, 7, 1, 1, 0, 2), (2, 1, 4), (0, 5, 0, 1, 0, 2), (1, 8, 1, 1, 0, 2), (2, 2, 2), (0, 7, 1, 2, 0, 2),
-    (0, 7, 0, 3, 0, 3), (0, 6, 0, 2, 1, 0), (0, 6, 1, 1, 0, 3), (0, 5, 1, 2, 1, 0), (1, 8, 0, 0, 0, 1),
-    (0, 6, 1, 1, 0, 1), (0, 6, 1, 0, 0, 1), (1, 8, 0, 1, 1, 0), (0, 7, 1, 1, 1, 0), (0, 7, 1, 1, 0, 1), (2, 2, 4),
-    (5, 0, 0), (0, 6, 0, 3, 1, 0), (0, 6, 1, 2, 1, 0), (1, 8, 1, 1, 1, 1), (0, 7, 1, 2, 0, 3), (0, 5, 1, 1, 1, 0),
-    (0, 6, 0, 2, 0, 3), (0, 5, 0, 2, 0, 3), (0, 6, 1, 2, 0, 2), (0, 6, 1, 1, 1, 1), (0, 7, 0, 3, 1, 0),
-    (1, 8, 1, 1, 0, 3), (0, 7, 0, 2, 1, 0), (0, 6, 1, 2, 1, 1), (0, 8, 1, 1, 1, 0), (0, 7, 1, 3, 1, 0),
-    (1, 8, 0, 2, 1, 0), (0, 6, 1, 3, 1, 0), (0, 7, 0, 1, 1, 1), (0, 6, 1, 3, 0, 3), (7, 0, 0), (0, 6, 1, 2, 0, 3),
-    (0, 6, 1, 1, 0, 2), (0, 7, 1, 1, 0, 3), (0, 5, 1, 2, 0, 3), (0, 5, 1, 3, 1, 0), (1, 8, 1, 1, 1, 2),
-    (0, 7, 1, 1, 1, 1), (1, 8, 1, 3, 1, 0), (0, 7, 1, 3, 0, 3), (0, 5, 1, 1, 0, 2), (7, 2, 0), (7, 1, 1), (7, 1, 0),
-    (7, 3, 1), (7, 3, 0), (1, 8, 0, 3, 0, 3), (0, 7, 1, 2, 1, 0), (7, 2, 1), (6, 0, 0), (8, 2, 1), (1, 8, 1, 1, 1, 0),
-    (8, 0, 0), (8, 3, 1), (8, 3, 0), (8, 1, 1), (8, 1, 0), (8, 2, 0),
+    (0, 0, 0, 0, 0, 0), (2, 0, 0, 0, 0, 0), (3, 8, 0, 0, 0, 0), (4, 0, 0, 0, 0, 0), (0, 1, 0, 0, 0, 0),
+    (2, 1, 0, 0, 0, 0), (4, 1, 0, 0, 0, 0), (4, 2, 0, 0, 0, 0), (4, 3, 0, 0, 0, 0), (4, 4, 0, 0, 0, 0),
+    (4, 8, 0, 0, 0, 0), (0, 2, 0, 0, 0, 0), (2, 2, 0, 0, 0, 0), (4, 0, 1, 0, 0, 0), (4, 0, 0, 1, 1, 0),
+    (0, 3, 0, 0, 0, 0), (2, 0, 0, 1, 1, 0), (4, 7, 0, 0, 0, 0), (4, 6, 0, 0, 0, 0), (4, 5, 0, 0, 0, 0),
+    (4, 1, 1, 0, 0, 0), (4, 1, 0, 1, 1, 0), (0, 1, 1, 0, 0, 0), (2, 3, 0, 0, 0, 0), (4, 2, 1, 0, 0, 0),
+    (4, 2, 0, 1, 1, 0), (0, 4, 0, 0, 0, 0), (2, 2, 0, 1, 1, 0), (4, 0, 1, 1, 1, 0), (4, 0, 0, 2, 1, 0),
+    (0, 7, 0, 0, 0, 0), (2, 0, 0, 2, 1, 0), (4, 1, 1, 1, 1, 0), (4, 3, 1, 0, 0, 0), (0, 8, 0, 0, 0, 0),
+    (2, 4, 0, 0, 0, 0), (0, 0, 0, 0, 0, 1), (1, 0, 0, 0, 0, 1), (2, 0, 0, 0, 0, 1), (3, 8, 0, 0, 0, 1),
+    (0, 1, 0, 0, 0, 1), (1, 1, 0, 0, 0, 1), (2, 1, 0, 0, 0, 1), (4, 0, 0, 0, 0, 1), (4, 1, 0, 0, 0, 1),
+    (4, 2, 0, 0, 0, 1), (4, 3, 0, 0, 0, 1), (4, 4, 0, 0, 0, 1), (4, 8, 0, 0, 0, 1), (0, 2, 0, 0, 0, 1),
+    (1, 2, 0, 0, 0, 1), (2, 2, 0, 0, 0, 1), (4, 0, 0, 1, 0, 1), (4, 0, 0, 1, 1, 1), (4, 0, 1, 0, 0, 1),
+    (0, 0, 0, 1, 0, 1), (1, 0, 0, 1, 1, 1), (2, 0, 0, 1, 0, 1), (4, 7, 0, 0, 0, 1), (4, 6, 0, 0, 0, 1),
+    (4, 5, 0, 0, 0, 1), (4, 1, 0, 1, 0, 1), (4, 1, 0, 1, 1, 1), (4, 1, 1, 0, 0, 1), (0, 1, 0, 1, 0, 1),
+    (1, 1, 1, 0, 0, 1), (2, 0, 0, 1, 1, 1), (4, 2, 0, 1, 0, 1), (4, 2, 0, 1, 1, 1), (4, 2, 1, 0, 0, 1),
+    (0, 1, 1, 0, 0, 1), (1, 1, 0, 1, 1, 1), (2, 2, 0, 1, 0, 1), (4, 3, 0, 1, 0, 1), (4, 0, 0, 2, 1, 1),
+    (4, 0, 1, 1, 0, 1), (0, 2, 0, 1, 0, 1), (1, 0, 0, 2, 1, 1), (2, 0, 0, 2, 1, 1), (4, 1, 1, 1, 0, 1),
+    (4, 1, 1, 1, 1, 1), (4, 0, 1, 1, 1, 1), (0, 1, 1, 1, 0, 1), (1, 1, 1, 1, 1, 1), (2, 2, 0, 1, 1, 1),
+    (0, 0, 0, 0, 0, 2), (1, 0, 0, 0, 0, 2), (2, 0, 0, 0, 0, 2), (3, 8, 0, 0, 0, 2), (0, 1, 0, 0, 0, 2),
+    (1, 1, 0, 0, 0, 2), (2, 1, 0, 0, 0, 2), (4, 0, 0, 0, 0, 2), (4, 1, 0, 0, 0, 2), (4, 2, 0, 0, 0, 2),
+    (4, 3, 0, 0, 0, 2), (4, 4, 0, 0, 0, 2), (4, 8, 0, 0, 0, 2), (0, 2, 0, 0, 0, 2), (1, 2, 0, 0, 0, 2),
+    (2, 2, 0, 0, 0, 2), (4, 0, 0, 1, 0, 2), (4, 0, 0, 1, 1, 2), (4, 0, 1, 0, 0, 2), (0, 0, 0, 1, 0, 2),
+    (1, 0, 0, 1, 1, 2), (2, 0, 0, 1, 0, 2), (4, 7, 0, 0, 0, 2), (4, 6, 0, 0, 0, 2), (4, 5, 0, 0, 0, 2),
+    (4, 1, 0, 1, 0, 2), (4, 1, 0, 1, 1, 2), (4, 1, 1, 0, 0, 2), (0, 1, 0, 1, 0, 2), (1, 1, 1, 0, 0, 2),
+    (2, 0, 0, 1, 1, 2), (4, 2, 0, 1, 0, 2), (4, 2, 0, 1, 1, 2), (4, 2, 1, 0, 0, 2), (0, 1, 1, 0, 0, 2),
+    (1, 1, 0, 1, 1, 2), (2, 2, 0, 1, 0, 2), (4, 0, 0, 2, 0, 2), (4, 3, 0, 1, 1, 2), (4, 0, 1, 1, 0, 2),
+    (0, 0, 0, 2, 0, 2), (1, 2, 0, 1, 1, 2), (2, 0, 0, 2, 0, 2), (4, 1, 0, 2, 0, 2), (4, 1, 1, 1, 1, 2),
+    (4, 0, 1, 1, 1, 2), (0, 1, 0, 2, 0, 2), (1, 1, 1, 1, 1, 2), (2, 2, 0, 1, 1, 2), (1, 0, 0, 0, 0, 3),
+    (2, 0, 0, 0, 0, 3), (3, 8, 0, 0, 0, 3), (4, 0, 0, 0, 0, 3), (1, 1, 0, 0, 0, 3), (2, 1, 0, 0, 0, 3),
+    (4, 1, 0, 0, 0, 3), (4, 2, 0, 0, 0, 3), (4, 3, 0, 0, 0, 3), (4, 4, 0, 0, 0, 3), (4, 8, 0, 0, 0, 3),
+    (1, 2, 0, 0, 0, 3), (2, 2, 0, 0, 0, 3), (4, 0, 0, 1, 0, 3), (4, 0, 1, 0, 0, 3), (1, 3, 0, 0, 0, 3),
+    (2, 0, 0, 1, 0, 3), (4, 7, 0, 0, 0, 3), (4, 6, 0, 0, 0, 3), (4, 5, 0, 0, 0, 3), (4, 1, 0, 1, 0, 3),
+    (4, 1, 1, 0, 0, 3), (1, 1, 1, 0, 0, 3), (2, 3, 0, 0, 0, 3), (4, 2, 0, 1, 0, 3), (4, 2, 1, 0, 0, 3),
+    (1, 4, 0, 0, 0, 3), (2, 2, 0, 1, 0, 3), (4, 0, 0, 2, 0, 3), (4, 0, 1, 1, 0, 3), (1, 7, 0, 0, 0, 3),
+    (2, 0, 0, 2, 0, 3), (4, 1, 0, 2, 0, 3), (4, 3, 1, 0, 0, 3), (1, 8, 0, 0, 0, 3), (2, 4, 0, 0, 0, 3), (1, 3, 0),
+    (0, 6, 0, 0, 0, 0), (4, 1, 0, 2, 1, 0), (4, 2, 1, 1, 1, 0), (4, 1, 0, 2, 1, 1), (4, 2, 1, 1, 0, 1),
+    (4, 4, 0, 1, 0, 1), (4, 1, 1, 1, 0, 2), (4, 2, 1, 1, 0, 2), (4, 4, 0, 1, 1, 2), (1, 6, 0, 0, 0, 3),
+    (4, 1, 1, 1, 0, 3), (4, 2, 1, 1, 0, 3), (0, 0, 0), (2, 7, 0, 0, 0, 0), (0, 5, 0, 0, 0, 0), (4, 0, 1, 2, 1, 0),
+    (4, 0, 0, 3, 1, 0), (2, 0, 0, 3, 1, 0), (4, 1, 1, 2, 1, 0), (4, 4, 1, 0, 0, 0), (2, 8, 0, 0, 0, 0),
+    (2, 6, 0, 0, 0, 0), (4, 1, 0, 3, 1, 0), (4, 7, 1, 0, 0, 0), (0, 3, 0, 1, 0, 1), (1, 1, 0, 2, 1, 1),
+    (2, 3, 0, 1, 0, 1), (4, 7, 0, 1, 0, 1), (4, 2, 0, 2, 1, 1), (4, 0, 1, 2, 1, 1), (0, 4, 0, 1, 0, 1),
+    (1, 2, 0, 2, 1, 1), (2, 2, 0, 2, 1, 1), (3, 8, 0, 1, 0, 1), (4, 8, 0, 1, 0, 1), (4, 1, 1, 2, 1, 1),
+    (4, 2, 1, 1, 1, 1), (0, 3, 0, 0, 0, 1), (1, 1, 1, 2, 1, 1), (2, 4, 0, 1, 0, 1), (4, 6, 0, 1, 0, 1),
+    (4, 3, 0, 2, 1, 1), (4, 3, 1, 1, 0, 1), (0, 4, 0, 0, 0, 1), (1, 2, 0, 1, 1, 1), (2, 3, 0, 2, 1, 1),
+    (4, 5, 0, 1, 0, 1), (0, 1, 1, 1, 0, 2), (1, 3, 0, 1, 1, 2), (2, 3, 0, 1, 1, 2), (4, 2, 0, 2, 0, 2),
+    (4, 7, 0, 1, 1, 2), (4, 0, 1, 2, 0, 2), (0, 2, 0, 2, 0, 2), (1, 4, 0, 1, 1, 2), (2, 2, 0, 2, 0, 2),
+    (3, 8, 0, 1, 1, 2), (4, 8, 0, 1, 1, 2), (4, 1, 1, 2, 0, 2), (4, 2, 1, 1, 1, 2), (0, 1, 1, 2, 0, 2),
+    (1, 3, 0, 0, 0, 2), (2, 4, 0, 1, 1, 2), (4, 6, 0, 1, 1, 2), (4, 3, 0, 2, 0, 2), (4, 3, 1, 1, 1, 2),
+    (0, 2, 0, 1, 0, 2), (1, 4, 0, 0, 0, 2), (2, 3, 0, 2, 0, 2), (4, 5, 0, 1, 1, 2), (2, 7, 0, 0, 0, 3),
+    (1, 5, 0, 0, 0, 3), (4, 0, 0, 3, 0, 3), (4, 0, 1, 2, 0, 3), (2, 0, 0, 3, 0, 3), (4, 1, 0, 3, 0, 3),
+    (4, 4, 1, 0, 0, 3), (2, 8, 0, 0, 0, 3), (2, 6, 0, 0, 0, 3), (4, 1, 1, 2, 0, 3), (4, 7, 1, 0, 0, 3), (1, 0, 0),
+    (2, 2, 0, 3, 1, 0), (4, 0, 1, 3, 1, 0), (4, 2, 0, 3, 1, 0), (0, 8, 1, 0, 0, 0), (3, 8, 1, 0, 0, 0),
+    (4, 8, 1, 0, 0, 0), (2, 5, 0, 0, 0, 0), (4, 1, 1, 3, 1, 0), (4, 6, 1, 0, 0, 0), (2, 2, 0, 2, 1, 0),
+    (4, 2, 0, 2, 1, 0), (4, 2, 1, 3, 1, 0), (2, 3, 0, 3, 1, 0), (4, 3, 0, 3, 1, 0), (4, 2, 1, 2, 1, 1),
+    (4, 4, 0, 2, 1, 1), (0, 7, 0, 1, 0, 1), (1, 3, 0, 2, 1, 1), (2, 4, 0, 2, 1, 1), (4, 3, 0, 1, 1, 1),
+    (4, 4, 1, 1, 0, 1), (0, 8, 0, 1, 0, 1), (1, 4, 0, 2, 1, 1), (2, 3, 0, 1, 1, 1), (3, 8, 1, 1, 0, 1),
+    (4, 8, 1, 1, 0, 1), (0, 8, 1, 1, 0, 1), (4, 4, 0, 1, 1, 1), (4, 3, 1, 2, 1, 1), (0, 6, 0, 1, 0, 1),
+    (1, 3, 0, 1, 1, 1), (2, 4, 0, 1, 1, 1), (4, 7, 0, 2, 1, 1), (4, 4, 1, 2, 1, 1), (0, 5, 0, 1, 0, 1),
+    (1, 4, 0, 1, 1, 1), (2, 3, 0, 0, 0, 1), (4, 2, 1, 2, 0, 2), (4, 4, 0, 2, 0, 2), (0, 3, 0, 2, 0, 2),
+    (1, 7, 0, 1, 1, 2), (2, 4, 0, 2, 0, 2), (4, 3, 0, 1, 0, 2), (4, 4, 1, 1, 1, 2), (0, 4, 0, 2, 0, 2),
+    (1, 8, 0, 1, 1, 2), (2, 3, 0, 1, 0, 2), (3, 8, 1, 1, 1, 2), (4, 8, 1, 1, 1, 2), (1, 8, 1, 1, 1, 2),
+    (4, 4, 0, 1, 0, 2), (4, 3, 1, 2, 0, 2), (0, 3, 0, 1, 0, 2), (1, 6, 0, 1, 1, 2), (2, 4, 0, 1, 0, 2),
+    (4, 7, 0, 2, 0, 2), (4, 4, 1, 2, 0, 2), (0, 4, 0, 1, 0, 2), (1, 5, 0, 1, 1, 2), (2, 3, 0, 0, 0, 2),
+    (3, 8, 0, 2, 0, 2), (4, 8, 0, 2, 0, 2), (2, 2, 0, 3, 0, 3), (4, 0, 1, 3, 0, 3), (4, 2, 0, 3, 0, 3),
+    (1, 8, 1, 0, 0, 3), (3, 8, 1, 0, 0, 3), (4, 8, 1, 0, 0, 3), (2, 5, 0, 0, 0, 3), (4, 1, 1, 3, 0, 3),
+    (4, 6, 1, 0, 0, 3), (2, 2, 0, 2, 0, 3), (4, 2, 0, 2, 0, 3), (4, 2, 1, 3, 0, 3), (2, 3, 0, 3, 0, 3),
+    (4, 3, 0, 3, 0, 3), (1, 1, 0), (2, 4, 0, 3, 1, 0), (4, 4, 0, 3, 1, 0), (4, 5, 1, 0, 0, 0), (3, 8, 1, 2, 1, 1),
+    (3, 8, 0, 2, 1, 1), (4, 3, 1, 1, 1, 1), (4, 8, 1, 2, 1, 1), (4, 8, 0, 2, 1, 1), (3, 8, 1, 2, 0, 2),
+    (4, 3, 1, 1, 0, 2), (4, 8, 1, 2, 0, 2), (2, 4, 0, 3, 0, 3), (4, 4, 0, 3, 0, 3), (4, 5, 1, 0, 0, 3), (2, 1, 1),
+    (0, 7, 0, 0, 0, 1), (1, 3, 0, 0, 0, 1), (2, 4, 0, 0, 0, 1), (0, 3, 0, 0, 0, 2), (1, 7, 0, 0, 0, 2),
+    (2, 4, 0, 0, 0, 2), (2, 1, 0), (4, 2, 1, 2, 1, 0), (4, 2, 1, 2, 0, 3), (2, 3, 1), (2, 3, 0, 2, 1, 0),
+    (4, 3, 0, 2, 1, 0), (4, 4, 1, 1, 1, 1), (4, 6, 0, 2, 1, 1), (4, 4, 1, 1, 0, 2), (4, 6, 0, 2, 0, 2),
+    (2, 3, 0, 2, 0, 3), (4, 3, 0, 2, 0, 3), (2, 0, 1), (2, 0, 0), (4, 3, 1, 3, 1, 0), (1, 4, 0, 0, 0, 1),
+    (2, 7, 0, 2, 1, 1), (1, 8, 0, 0, 0, 2), (2, 7, 0, 2, 0, 2), (4, 3, 1, 3, 0, 3), (2, 3, 2), (1, 6, 0, 0, 0, 2),
+    (2, 3, 0), (2, 4, 0, 2, 1, 0), (4, 4, 0, 2, 1, 0), (4, 3, 1, 0, 0, 1), (4, 5, 0, 2, 1, 1), (4, 3, 1, 0, 0, 2),
+    (4, 5, 0, 2, 0, 2), (2, 4, 0, 2, 0, 3), (4, 4, 0, 2, 0, 3), (3, 1, 0), (2, 3, 0, 1, 1, 0), (4, 4, 1, 3, 1, 0),
+    (4, 3, 0, 1, 1, 0), (0, 8, 0, 0, 0, 1), (0, 6, 0, 0, 0, 1), (1, 8, 1, 2, 1, 1), (1, 7, 0, 2, 1, 1),
+    (2, 6, 0, 2, 1, 1), (4, 4, 1, 0, 0, 1), (4, 7, 0, 1, 1, 1), (0, 4, 0, 0, 0, 2), (1, 5, 0, 0, 0, 2),
+    (2, 6, 0, 2, 0, 2), (4, 4, 1, 0, 0, 2), (4, 7, 0, 1, 0, 2), (2, 3, 0, 1, 0, 3), (4, 4, 1, 3, 0, 3),
+    (4, 3, 0, 1, 0, 3), (2, 0, 2), (2, 5, 0, 2, 1, 1), (3, 8, 0, 1, 1, 1), (4, 8, 0, 1, 1, 1), (0, 8, 1, 2, 0, 2),
+    (2, 5, 0, 2, 0, 2), (1, 2, 0), (2, 4, 0, 1, 1, 0), (4, 3, 1, 2, 1, 0), (4, 4, 0, 1, 1, 0), (0, 5, 0, 0, 0, 1),
+    (1, 8, 0, 2, 1, 1), (4, 7, 1, 2, 1, 1), (0, 7, 0, 2, 0, 2), (4, 7, 1, 2, 0, 2), (4, 3, 1, 2, 0, 3), (2, 2, 1),
+    (1, 6, 0, 2, 1, 1), (2, 7, 0, 1, 0, 1), (4, 6, 0, 1, 1, 1), (2, 7, 0, 1, 0, 2), (3, 8, 0, 1, 0, 2),
+    (4, 8, 0, 1, 0, 2), (2, 2, 2), (3, 8, 1, 3, 1, 0), (4, 4, 1, 2, 1, 0), (4, 8, 1, 3, 1, 0), (4, 4, 1, 2, 0, 3),
+    (2, 2, 0), (4, 6, 1, 2, 1, 1), (0, 8, 0, 2, 0, 2), (4, 6, 1, 2, 0, 2), (3, 2, 0), (2, 7, 0, 3, 1, 0),
+    (3, 8, 0, 3, 1, 0), (4, 3, 1, 1, 1, 0), (4, 7, 0, 3, 1, 0), (4, 8, 0, 3, 1, 0), (1, 5, 0, 2, 1, 1),
+    (2, 7, 0, 1, 1, 1), (4, 5, 1, 2, 1, 1), (4, 5, 0, 1, 1, 1), (0, 6, 0, 2, 0, 2), (2, 7, 0, 1, 1, 2),
+    (4, 5, 1, 2, 0, 2), (4, 6, 0, 1, 0, 2), (2, 4, 0, 1, 0, 3), (3, 8, 1, 3, 0, 3), (4, 3, 1, 1, 0, 3),
+    (4, 4, 0, 1, 0, 3), (4, 8, 1, 3, 0, 3), (3, 0, 0), (2, 6, 0, 3, 1, 0), (4, 4, 1, 1, 1, 0), (4, 6, 0, 3, 1, 0),
+    (1, 7, 0, 1, 1, 1), (2, 6, 0, 1, 0, 1), (4, 7, 1, 1, 0, 1), (0, 5, 0, 2, 0, 2), (2, 6, 0, 1, 0, 2),
+    (4, 7, 1, 1, 0, 2), (4, 5, 0, 1, 0, 2), (2, 7, 0, 3, 0, 3), (3, 8, 0, 3, 0, 3), (4, 7, 0, 3, 0, 3),
+    (4, 8, 0, 3, 0, 3), (3, 3, 0), (2, 5, 0, 3, 1, 0), (4, 7, 1, 3, 1, 0), (4, 5, 0, 3, 1, 0), (1, 8, 0, 1, 1, 1),
+    (1, 6, 0, 1, 1, 1), (2, 6, 0, 1, 1, 1), (4, 7, 1, 1, 1, 1), (0, 7, 0, 1, 0, 2), (2, 6, 0, 1, 1, 2),
+    (4, 7, 1, 1, 1, 2), (2, 6, 0, 3, 0, 3), (4, 4, 1, 1, 0, 3), (4, 6, 0, 3, 0, 3), (4, 0, 0), (2, 3, 4),
+    (2, 5, 0, 1, 0, 1), (0, 8, 0, 1, 0, 2), (2, 5, 0, 1, 0, 2), (4, 7, 1, 3, 0, 3), (2, 3, 3), (2, 5, 0, 3, 0, 3),
+    (4, 5, 0, 3, 0, 3), (2, 1, 3), (4, 6, 1, 3, 1, 0), (1, 5, 0, 1, 1, 1), (4, 6, 1, 1, 0, 1), (0, 6, 0, 1, 0, 2),
+    (4, 6, 1, 1, 0, 2), (2, 2, 3), (2, 7, 0, 2, 1, 0), (4, 7, 0, 2, 1, 0), (2, 5, 0, 1, 1, 1), (2, 5, 0, 1, 1, 2),
+    (2, 1, 2), (3, 8, 0, 2, 1, 0), (4, 8, 0, 2, 1, 0), (4, 6, 1, 3, 0, 3), (2, 1, 4), (1, 7, 0, 0, 0, 1),
+    (2, 7, 0, 2, 0, 3), (4, 7, 0, 2, 0, 3), (2, 0, 3), (4, 5, 1, 3, 1, 0), (4, 6, 1, 1, 1, 1), (0, 5, 0, 1, 0, 2),
+    (4, 6, 1, 1, 1, 2), (2, 2, 4), (2, 7, 0, 0, 0, 1), (2, 7, 0, 0, 0, 2), (3, 8, 0, 2, 0, 3), (4, 8, 0, 2, 0, 3),
+    (2, 0, 4), (2, 6, 0, 2, 1, 0), (4, 6, 0, 2, 1, 0), (4, 5, 1, 3, 0, 3), (5, 0, 0), (4, 7, 1, 2, 1, 0),
+    (1, 8, 0, 0, 0, 1), (4, 5, 1, 1, 0, 1), (0, 7, 0, 0, 0, 2), (4, 5, 1, 1, 0, 2), (7, 3, 0), (1, 6, 0, 0, 0, 1),
+    (2, 8, 0, 0, 0, 1), (2, 6, 0, 0, 0, 1), (4, 5, 1, 1, 1, 1), (1, 5, 0, 0, 0, 1), (2, 5, 0, 0, 0, 1),
+    (4, 7, 1, 0, 0, 1), (0, 8, 1, 0, 0, 1), (1, 8, 1, 0, 0, 1), (3, 8, 1, 0, 0, 1), (4, 8, 1, 0, 0, 1),
+    (4, 6, 1, 0, 0, 1), (1, 8, 1, 1, 1, 1), (3, 8, 1, 1, 1, 1), (4, 8, 1, 1, 1, 1), (4, 5, 1, 0, 0, 1),
+    (2, 8, 0, 0, 0, 2), (2, 6, 0, 0, 0, 2), (0, 8, 0, 0, 0, 2), (4, 5, 1, 1, 1, 2), (0, 6, 0, 0, 0, 2),
+    (2, 5, 0, 0, 0, 2), (4, 7, 1, 0, 0, 2), (0, 5, 0, 0, 0, 2), (1, 8, 1, 0, 0, 2), (3, 8, 1, 0, 0, 2),
+    (4, 8, 1, 0, 0, 2), (0, 8, 1, 0, 0, 2), (4, 6, 1, 0, 0, 2), (3, 8, 1, 1, 0, 2), (4, 8, 1, 1, 0, 2),
+    (0, 8, 1, 1, 0, 2), (4, 5, 1, 0, 0, 2), (2, 6, 0, 2, 0, 3), (4, 7, 1, 2, 0, 3), (4, 6, 0, 2, 0, 3), (7, 0, 0),
+    (2, 5, 0, 2, 1, 0), (4, 5, 0, 2, 1, 0), (2, 5, 0, 2, 0, 3), (4, 5, 0, 2, 0, 3), (4, 6, 1, 2, 0, 3),
+    (2, 7, 0, 1, 0, 3), (4, 7, 0, 1, 0, 3), (3, 8, 0, 1, 0, 3), (4, 8, 0, 1, 0, 3), (4, 5, 1, 2, 0, 3),
+    (2, 6, 0, 1, 0, 3), (4, 6, 0, 1, 0, 3), (4, 7, 1, 1, 0, 3), (2, 5, 0, 1, 0, 3), (4, 5, 0, 1, 0, 3),
+    (3, 8, 1, 1, 0, 3), (4, 8, 1, 1, 0, 3), (5, 8, 0, 0, 0, 3), (5, 8, 1, 0, 0, 3), (5, 8, 1, 3, 0, 3),
+    (5, 8, 0, 3, 0, 3), (5, 8, 0, 2, 0, 3), (4, 6, 1, 1, 0, 3), (3, 8, 1, 2, 0, 3), (4, 8, 1, 2, 0, 3), (7, 2, 0),
+    (4, 6, 1, 2, 1, 0), (2, 7, 0, 1, 1, 0), (4, 7, 0, 1, 1, 0), (3, 8, 0, 1, 1, 0), (4, 8, 0, 1, 1, 0),
+    (4, 5, 1, 2, 1, 0), (2, 6, 0, 1, 1, 0), (4, 6, 0, 1, 1, 0), (4, 7, 1, 1, 1, 0), (2, 5, 0, 1, 1, 0),
+    (4, 5, 0, 1, 1, 0), (3, 8, 1, 1, 1, 0), (4, 8, 1, 1, 1, 0), (4, 6, 1, 1, 1, 0), (3, 8, 1, 2, 1, 0),
+    (4, 8, 1, 2, 1, 0), (5, 8, 0, 0, 0, 0), (4, 5, 1, 1, 1, 0), (5, 8, 1, 0, 0, 0), (5, 8, 1, 3, 1, 0),
+    (5, 8, 0, 3, 1, 0), (5, 8, 0, 2, 1, 0), (5, 8, 0, 0, 0, 1), (5, 8, 0, 1, 0, 1), (5, 8, 1, 1, 0, 1),
+    (5, 8, 1, 2, 1, 1), (5, 8, 0, 2, 1, 1), (5, 8, 0, 1, 1, 1), (5, 8, 0, 0, 0, 2), (5, 8, 0, 1, 1, 2),
+    (5, 8, 1, 1, 1, 2), (5, 8, 0, 2, 0, 2), (5, 8, 1, 2, 0, 2), (5, 8, 0, 1, 0, 2), (4, 5, 1, 1, 0, 3),
+    (5, 8, 0, 1, 0, 3), (6, 0, 0), (7, 3, 1), (7, 2, 1), (5, 8, 0, 1, 1, 0), (7, 1, 1), (5, 8, 1, 1, 1, 0),
+    (5, 8, 1, 0, 0, 1), (5, 8, 1, 1, 1, 1), (5, 8, 1, 0, 0, 2), (8, 0, 0), (5, 8, 1, 1, 0, 2), (8, 1, 1),
+    (5, 8, 1, 2, 1, 0), (8, 3, 1), (5, 8, 1, 1, 0, 3), (7, 1, 0), (8, 1, 0), (5, 8, 1, 2, 0, 3), (8, 3, 0), (8, 2, 1),
+    (8, 2, 0),
 )
 
 
@@ -164,15 +223,19 @@
 
     wo_copies, tok_copies = [], {}
     direct = pl.ds(0, 3 * (out_rows // 4))
-    for k, peer in enumerate(peers):
-        for a in range(2):
-            copy = pltpu.make_async_remote_copy(
-                src_ref=out_own[a].at[direct], dst_ref=wo_all.at[2 * t + a, me, direct],
-                send_sem=wo_send.at[k, a], recv_sem=wo_recv.at[k, a], device_id=peer, device_id_type=MESH,
-            )
-            copy.start()
-            wo_copies.append(copy)
-    for n in order:
+    def send_direct():
+        for k, peer in enumerate(peers):
+            for a in range(2):
+                copy = pltpu.make_async_remote_copy(
+                    src_ref=out_own[a].at[direct], dst_ref=wo_all.at[2 * t + a, me, direct],
+                    send_sem=wo_send.at[k, a], recv_sem=wo_recv.at[k, a], device_id=peer, device_id_type=MESH,
+                )
+                copy.start()
+                wo_copies.append(copy)
+
+    for turn, n in enumerate(order):
+        if turn == DIRECT_AFTER:
+            send_direct()
         here = pl.ds(n * step, step)
         for k, peer in enumerate(peers):
             copy = pltpu.make_async_remote_copy(
@@ -219,7 +282,7 @@
     def source(k, at):
         return at * n_fs + lax.rem(o + n_out - k, n_out) * 2 + i
 
-    def handle(part, k, distance, side, at, drain):
+    def handle(part, k, distance, side, at, drain, ways=WAYS, arrival=True):
         first = isinstance(distance, int) and distance == 0
         src = source(k, at)
         mine = (at + distance if side == 0 else at - distance) if isinstance(at, int) else s
@@ -235,21 +298,22 @@
             copy = copy_of(part, src, where, lane, distance, way)
             copy.wait_send() if drain else copy.start()
 
-        if not (first and k == 0) and not drain:
+        if arrival and not (first and k == 0) and not drain:
             copy_of(part, src, core, 0, 0, 0).wait_recv()
         if k == 0 or part.wide:
-            if first or side == 0:
+            if RIGHT in ways and (first or side == 0):
                 when(more_right, lambda: go(right, lane_z, 0))
-            if first or side == 1:
+            if LEFT in ways and (first or side == 1):
                 when(more_left, lambda: go(left, lane_z, 1))
-        if k == 0 and (first or not part.wide):
+        if ACROSS in ways and k == 0 and (first or not part.wide):
             for n, where in enumerate(across):
                 go(where, 2 + n, side)
-        if part.crossing:
+        if CROSS in ways and part.crossing:
             for n in range(len(peers)):
                 copy = cross_copy(part, src, n)
                 copy.wait_send() if drain else copy.start()
-        go(core, lane_core, side)
+        if CORE in ways:
+            go(core, lane_core, side)
 
     def hand_over(part, src, drain):
         for k in range(len(peers)):
@@ -503,17 +567,19 @@
                 turn = [entry for entry in events if entry[5] == mine]
 
                 def body(mine=mine, turn=turn):
-                    for passing, number, k, distance, side, _ in turn:
+                    for way, number, k, distance, side, _ in turn:
                         part = parts[number]
                         at = mine - distance if side == 0 else mine + distance
-                        if passing:
+                        if way == HAND:
                             hand_over(part, source(k, at), False)
                             continue
                         if distance == 0 and k == 0 and number >= n_proj:
                             once(("own", mine), lambda: wait_all(own_out))
                             if not part.crossing:
                                 once(("direct", mine), wo_ready)
-                        handle(part, k, distance, side, at, False)
+                        piece = (mine, number, k, distance, side)
+                        handle(part, k, distance, side, at, False, (way,), piece not in waited)
+                        waited.add(piece)
 
                 if turn:
                     pl.when(s == mine)(body)
@@ -566,12 +632,12 @@
         for mine in range(n_sp):
 
             def drain(mine=mine):
-                for passing, number, k, distance, side, _ in [entry for entry in events if entry[5] == mine]:
+                for way, number, k, distance, side, _ in [entry for entry in events if entry[5] == mine]:
                     at = mine - distance if side == 0 else mine + distance
-                    if passing:
+                    if way == HAND:
                         hand_over(parts[number], source(k, at), True)
                     else:
-                        handle(parts[number], k, distance, side, at, True)
+                        handle(parts[number], k, distance, side, at, True, (way,))
 
             pl.when(s == mine)(drain)
     else:

time: 120 us -> 111 us (0.925)
  Pallas kernels: 117 us -> 108 us
    pallas_call x1, Pallas kernels: 117 us -> 108 us  [on_device(): pl.pallas_call(functools.partial(layer_kernel, (n_sp, n_out, n_tp, 5, sep...]
where the time goes in v3:
time: 111 us
  Pallas kernels  108 us (97%)
  local copies, waits for them, and re-layouts  3.16 us (3%)
    pallas_call x1, Pallas kernels, on_device(): pl.pallas_call(functools.partial(layer_kernel, (n_sp, n_out, n_tp, 5, sep...  108 us
    unnamed x1, local copies, waits for them, and re-layouts  3.16 us

profile of v3, /device:TPU:0, one launch (start us, length us, event | category | flops | bytes accessed | tf_op | source)
XLA Modules:
  0.0 111.3 jit_solution(18155215451818252382)
XLA Ops:
  0.0 108.1 %shard_map.118 = bf16[512,2048]{1,0:T(8,128)(2,1)} custom-call(bf16[1024,1024]{1,0:T(8,128)(2,1)} %bitcast.4, f32[1,2048]{1,0:T(1,128)} %bitcast.5, bf16[3,512]{1,0:T(4,128)(2,1)} %refs_2_.1, f32[8]{0:T(128)} %refs_3_.1, bf16[128,512]{1,0:T(8,128)(2,1)} %refs_4_.1, bf16[128,256]{1,0:T(8,128)(2,1)} %refs_5_.1, bf16[128,256]{1,0:T(8,128)(2,1)} %refs_6_.1, ...), custom_call_target="tpu_custom_call" | custom-call | tf_op jit(solution)/shard_map/pallas_call | solution.py:679
  108.1 3.2 %copy.14 = bf16[1,512,2048]{2,1,0:T(8,128)(2,1)} copy(bf16[1,512,2048]{2,1,0:T(8,128)(2,1)} %bitcast.3) | data formatting | bytes 4194304

commit v4 on v2

--- a/solution.py
+++ b/solution.py
@@ -12,78 +12,136 @@
 WINDOW = 128
 HALO = 16
 MESH = pl.DeviceIdType.MESH
+DIRECT_AFTER = 2
+WAYS = RIGHT, LEFT, ACROSS, CROSS, CORE, HAND = range(6)
 BF16, F32 = jnp.bfloat16, jnp.float32
 
 
 TABLE_FOR = (4, 2, 2)
 TABLE = (
-    (0, 1, 0, 0, 0, 2), (0, 1, 0, 0, 0, 3), (0, 2, 0, 0, 0, 3), (0, 2, 0, 0, 0, 2), (0, 1, 1, 0, 0, 3),
-    (0, 0, 0, 0, 0, 2), (0, 0, 0, 0, 0, 1), (0, 1, 0, 0, 0, 1), (0, 0, 0, 1, 0, 2), (0, 1, 0, 0, 0, 0),
-    (0, 0, 0, 0, 0, 3), (0, 0, 0, 0, 0, 0), (0, 8, 0, 0, 0, 1), (0, 2, 0, 1, 1, 2), (0, 7, 0, 0, 0, 3),
-    (0, 4, 0, 0, 0, 2), (0, 1, 1, 0, 0, 2), (0, 1, 0, 1, 0, 2), (0, 0, 0, 1, 0, 3), (0, 7, 0, 0, 0, 0),
-    (0, 0, 0, 1, 1, 0), (0, 4, 0, 0, 0, 1), (0, 0, 0, 2, 0, 3), (0, 3, 0, 0, 0, 3), (0, 8, 0, 0, 0, 0),
-    (0, 2, 0, 0, 0, 1), (0, 5, 0, 0, 0, 0), (0, 1, 0, 1, 0, 1), (0, 1, 1, 0, 0, 1), (0, 0, 0, 1, 1, 2),
-    (0, 0, 0, 1, 1, 1), (0, 3, 0, 1, 1, 2), (0, 1, 1, 0, 0, 0), (0, 4, 0, 0, 0, 0), (0, 0, 1, 0, 0, 0),
-    (0, 6, 0, 0, 0, 3), (0, 6, 0, 0, 0, 2), (0, 2, 0, 1, 0, 2), (0, 0, 0, 1, 0, 1), (0, 4, 0, 1, 1, 2),
-    (0, 3, 0, 0, 0, 1), (0, 2, 0, 0, 0, 0), (0, 0, 1, 0, 0, 1), (0, 0, 0), (0, 4, 0, 0, 0, 3), (0, 1, 1, 1, 1, 0),
-    (0, 2, 0, 1, 1, 0), (0, 0, 0, 2, 1, 1), (0, 1, 0, 2, 0, 3), (0, 2, 0, 1, 0, 1), (0, 8, 1, 0, 0, 1),
-    (0, 3, 0, 2, 1, 1), (0, 2, 1, 0, 0, 0), (0, 1, 1, 1, 1, 2), (0, 0, 1, 0, 0, 3), (0, 1, 1, 1, 0, 2),
-    (0, 1, 0, 1, 1, 2), (0, 2, 0, 2, 1, 1), (0, 5, 0, 0, 0, 3), (0, 7, 0, 0, 0, 1), (0, 1, 1, 1, 0, 3),
-    (0, 6, 1, 0, 0, 3), (0, 0, 0, 3, 1, 0), (0, 3, 0, 0, 0, 0), (0, 8, 0, 0, 0, 2), (0, 3, 0, 3, 1, 0),
-    (0, 5, 0, 1, 0, 1), (0, 2, 1, 1, 1, 2), (0, 0, 0, 2, 0, 2), (0, 1, 0, 2, 0, 2), (0, 4, 0, 1, 0, 3),
-    (0, 6, 0, 0, 0, 0), (0, 0, 0, 2, 1, 0), (0, 1, 1, 1, 0, 1), (0, 4, 1, 1, 0, 3), (0, 8, 0, 1, 0, 2),
-    (0, 8, 0, 0, 0, 3), (0, 2, 1, 0, 0, 2), (0, 0, 1, 3, 1, 0), (0, 1, 1, 2, 1, 1), (0, 1, 0, 1, 1, 0),
-    (0, 4, 1, 0, 0, 2), (0, 2, 0, 2, 0, 2), (0, 4, 0, 1, 0, 1), (0, 0, 1, 2, 1, 1), (1, 3, 0), (1, 0, 0),
-    (0, 1, 0, 2, 1, 1), (0, 3, 0, 0, 0, 2), (0, 6, 1, 0, 0, 0), (0, 2, 0, 2, 0, 3), (0, 8, 1, 0, 0, 2),
-    (0, 8, 1, 1, 0, 3), (0, 8, 0, 2, 0, 3), (0, 8, 1, 0, 0, 0), (0, 0, 1, 2, 0, 2), (0, 3, 0, 1, 1, 1),
-    (0, 8, 0, 1, 1, 2), (0, 1, 1, 2, 0, 2), (0, 1, 0, 1, 1, 1), (0, 3, 0, 1, 0, 1), (0, 7, 1, 0, 0, 0),
-    (0, 5, 0, 0, 0, 2), (0, 8, 1, 0, 0, 3), (0, 7, 0, 1, 1, 2), (0, 0, 1, 1, 0, 2), (0, 2, 0, 3, 1, 0),
-    (0, 1, 0, 3, 0, 3), (0, 4, 1, 0, 0, 0), (0, 3, 0, 2, 1, 0), (0, 8, 1, 1, 1, 1), (0, 3, 0, 2, 0, 2),
-    (0, 2, 0, 1, 0, 3), (0, 2, 0, 1, 1, 1), (0, 5, 1, 1, 0, 1), (0, 1, 0, 1, 0, 3), (0, 0, 1, 2, 0, 3),
-    (0, 4, 0, 2, 1, 1), (0, 1, 1, 1, 1, 1), (0, 2, 1, 3, 1, 0), (0, 8, 1, 1, 0, 1), (0, 0, 0, 3, 0, 3),
-    (0, 2, 1, 1, 0, 1), (0, 0, 1, 1, 0, 3), (1, 1, 0), (0, 8, 0, 2, 0, 2), (0, 4, 1, 0, 0, 3), (0, 2, 0, 3, 0, 3),
-    (0, 1, 0, 2, 1, 0), (0, 7, 1, 0, 0, 3), (0, 3, 0, 3, 0, 3), (0, 3, 1, 3, 1, 0), (0, 8, 1, 1, 0, 2),
-    (1, 8, 1, 0, 0, 0), (0, 8, 0, 1, 0, 1), (0, 3, 0, 1, 1, 0), (0, 5, 1, 0, 0, 0), (0, 4, 0, 1, 1, 1),
-    (0, 0, 1, 0, 0, 2), (0, 1, 1, 3, 0, 3), (0, 1, 0, 3, 1, 0), (0, 0, 1, 3, 0, 3), (0, 7, 0, 1, 0, 1),
-    (0, 5, 1, 0, 0, 2), (0, 8, 1, 2, 0, 2), (0, 0, 1, 1, 1, 2), (0, 2, 1, 2, 0, 3), (0, 6, 0, 0, 0, 1),
-    (0, 5, 0, 2, 0, 2), (0, 0, 1, 1, 1, 0), (0, 8, 0, 2, 1, 1), (0, 0, 1, 2, 1, 0), (0, 5, 0, 0, 0, 1),
-    (0, 3, 1, 0, 0, 1), (0, 0, 1, 1, 1, 1), (0, 6, 0, 1, 1, 2), (0, 4, 1, 2, 1, 1), (0, 0, 1, 1, 0, 1),
-    (0, 3, 1, 0, 0, 2), (0, 1, 1, 3, 1, 0), (0, 1, 1, 2, 0, 3), (1, 8, 0, 0, 0, 0), (1, 2, 0), (0, 5, 1, 0, 0, 3),
-    (2, 0, 0), (0, 8, 0, 1, 0, 3), (0, 3, 1, 0, 0, 0), (0, 8, 0, 1, 1, 1), (0, 2, 0, 2, 1, 0), (0, 4, 1, 1, 1, 2),
-    (0, 2, 1, 3, 0, 3), (0, 8, 1, 1, 1, 2), (0, 5, 0, 1, 0, 3), (0, 5, 0, 1, 1, 1), (0, 3, 1, 2, 0, 2),
-    (0, 2, 1, 1, 1, 0), (0, 3, 0, 1, 0, 2), (0, 8, 0, 3, 0, 3), (0, 3, 1, 0, 0, 3), (0, 5, 0, 1, 1, 2), (2, 2, 0),
-    (0, 4, 0, 3, 1, 0), (1, 8, 0, 1, 0, 1), (0, 4, 0, 2, 0, 2), (0, 8, 1, 2, 1, 1), (0, 8, 1, 3, 0, 3),
-    (0, 6, 0, 1, 1, 1), (0, 1, 1, 2, 1, 0), (0, 3, 1, 3, 0, 3), (1, 8, 0, 2, 1, 1), (0, 4, 0, 1, 0, 2), (2, 1, 0),
-    (2, 3, 0), (0, 4, 0, 1, 1, 0), (0, 5, 0, 3, 0, 3), (0, 2, 1, 0, 0, 1), (0, 6, 0, 1, 0, 1), (0, 3, 0, 1, 0, 3),
-    (0, 7, 0, 2, 1, 1), (2, 2, 1), (2, 3, 1), (1, 8, 1, 0, 0, 2), (3, 3, 0), (0, 2, 1, 1, 0, 2), (2, 1, 1),
-    (1, 8, 0, 1, 1, 1), (0, 3, 1, 1, 1, 1), (0, 6, 1, 1, 1, 2), (2, 0, 1), (0, 4, 0, 2, 1, 0), (0, 5, 1, 2, 0, 2),
-    (0, 8, 0, 3, 1, 0), (0, 7, 0, 1, 0, 2), (0, 4, 1, 3, 1, 0), (0, 2, 1, 2, 0, 2), (0, 8, 1, 2, 1, 0),
-    (0, 6, 0, 1, 1, 0), (1, 8, 0, 2, 0, 3), (0, 3, 1, 1, 0, 2), (0, 8, 0, 1, 1, 0), (0, 2, 1, 2, 1, 1),
-    (0, 5, 0, 1, 1, 0), (0, 5, 1, 3, 0, 3), (1, 8, 1, 2, 1, 1), (0, 3, 1, 2, 1, 0), (0, 5, 1, 1, 0, 3),
-    (1, 8, 0, 0, 0, 2), (1, 8, 0, 1, 1, 2), (0, 7, 1, 1, 1, 2), (0, 3, 1, 1, 0, 1), (0, 3, 0, 2, 0, 3),
-    (0, 6, 0, 2, 0, 2), (0, 5, 1, 1, 1, 2), (0, 3, 1, 2, 1, 1), (0, 8, 1, 2, 0, 3), (1, 8, 1, 2, 0, 2),
-    (1, 8, 0, 1, 0, 3), (1, 8, 1, 3, 0, 3), (0, 4, 0, 3, 0, 3), (0, 2, 1, 0, 0, 3), (0, 7, 0, 0, 0, 2), (3, 1, 0),
-    (0, 4, 0, 2, 0, 3), (1, 8, 1, 0, 0, 3), (0, 3, 1, 1, 0, 3), (0, 3, 1, 1, 1, 2), (1, 8, 1, 0, 0, 1),
-    (0, 3, 1, 1, 1, 0), (3, 2, 0), (0, 5, 1, 1, 1, 1), (0, 2, 1, 1, 0, 3), (1, 8, 0, 0, 0, 3), (0, 4, 1, 0, 0, 1),
-    (0, 6, 0, 1, 0, 2), (0, 6, 1, 1, 1, 0), (0, 8, 1, 3, 1, 0), (0, 8, 0, 2, 1, 0), (3, 0, 0), (0, 3, 1, 2, 0, 3),
-    (0, 7, 0, 1, 1, 0), (0, 6, 1, 0, 0, 2), (0, 4, 1, 1, 1, 0), (0, 2, 1, 1, 1, 1), (0, 4, 1, 1, 0, 1),
-    (0, 4, 1, 1, 1, 1), (0, 4, 1, 1, 0, 2), (0, 2, 1, 2, 1, 0), (0, 6, 0, 1, 0, 3), (1, 8, 0, 3, 1, 0),
-    (0, 5, 0, 2, 1, 1), (1, 8, 1, 2, 1, 0), (0, 4, 1, 2, 0, 2), (4, 0, 0), (0, 4, 1, 2, 1, 0), (2, 0, 3),
-    (0, 7, 0, 2, 0, 3), (2, 3, 3), (2, 1, 2), (0, 7, 1, 2, 1, 1), (0, 5, 1, 0, 0, 1), (1, 8, 0, 2, 0, 2), (2, 3, 2),
-    (0, 5, 0, 2, 1, 0), (0, 7, 0, 2, 0, 2), (0, 4, 1, 2, 0, 3), (2, 2, 3), (0, 4, 1, 3, 0, 3), (1, 8, 1, 1, 0, 1),
-    (0, 6, 0, 3, 0, 3), (0, 7, 1, 0, 0, 1), (0, 5, 1, 2, 1, 1), (2, 1, 3), (0, 6, 0, 2, 1, 1), (2, 3, 4),
-    (1, 8, 0, 1, 0, 2), (2, 0, 2), (0, 7, 1, 0, 0, 2), (0, 7, 0, 1, 0, 3), (0, 5, 0, 3, 1, 0), (1, 8, 1, 2, 0, 3),
-    (2, 0, 4), (0, 7, 1, 1, 0, 2), (2, 1, 4), (0, 5, 0, 1, 0, 2), (1, 8, 1, 1, 0, 2), (2, 2, 2), (0, 7, 1, 2, 0, 2),
-    (0, 7, 0, 3, 0, 3), (0, 6, 0, 2, 1, 0), (0, 6, 1, 1, 0, 3), (0, 5, 1, 2, 1, 0), (1, 8, 0, 0, 0, 1),
-    (0, 6, 1, 1, 0, 1), (0, 6, 1, 0, 0, 1), (1, 8, 0, 1, 1, 0), (0, 7, 1, 1, 1, 0), (0, 7, 1, 1, 0, 1), (2, 2, 4),
-    (5, 0, 0), (0, 6, 0, 3, 1, 0), (0, 6, 1, 2, 1, 0), (1, 8, 1, 1, 1, 1), (0, 7, 1, 2, 0, 3), (0, 5, 1, 1, 1, 0),
-    (0, 6, 0, 2, 0, 3), (0, 5, 0, 2, 0, 3), (0, 6, 1, 2, 0, 2), (0, 6, 1, 1, 1, 1), (0, 7, 0, 3, 1, 0),
-    (1, 8, 1, 1, 0, 3), (0, 7, 0, 2, 1, 0), (0, 6, 1, 2, 1, 1), (0, 8, 1, 1, 1, 0), (0, 7, 1, 3, 1, 0),
-    (1, 8, 0, 2, 1, 0), (0, 6, 1, 3, 1, 0), (0, 7, 0, 1, 1, 1), (0, 6, 1, 3, 0, 3), (7, 0, 0), (0, 6, 1, 2, 0, 3),
-    (0, 6, 1, 1, 0, 2), (0, 7, 1, 1, 0, 3), (0, 5, 1, 2, 0, 3), (0, 5, 1, 3, 1, 0), (1, 8, 1, 1, 1, 2),
-    (0, 7, 1, 1, 1, 1), (1, 8, 1, 3, 1, 0), (0, 7, 1, 3, 0, 3), (0, 5, 1, 1, 0, 2), (7, 2, 0), (7, 1, 1), (7, 1, 0),
-    (7, 3, 1), (7, 3, 0), (1, 8, 0, 3, 0, 3), (0, 7, 1, 2, 1, 0), (7, 2, 1), (6, 0, 0), (8, 2, 1), (1, 8, 1, 1, 1, 0),
-    (8, 0, 0), (8, 3, 1), (8, 3, 0), (8, 1, 1), (8, 1, 0), (8, 2, 0),
+    (0, 1, 0, 0, 0, 0), (0, 0, 0, 0, 0, 0), (2, 1, 0, 0, 0, 0), (2, 0, 0, 0, 0, 0), (3, 8, 0, 0, 0, 0),
+    (4, 1, 0, 0, 0, 0), (0, 2, 0, 0, 0, 0), (4, 0, 0, 0, 0, 0), (2, 2, 0, 0, 0, 0), (4, 2, 0, 0, 0, 0),
+    (4, 3, 0, 0, 0, 0), (4, 4, 0, 0, 0, 0), (4, 8, 0, 0, 0, 0), (0, 3, 0, 0, 0, 0), (2, 3, 0, 0, 0, 0),
+    (4, 1, 1, 0, 0, 0), (4, 1, 0, 1, 1, 0), (0, 1, 1, 0, 0, 0), (2, 4, 0, 0, 0, 0), (4, 0, 1, 0, 0, 0),
+    (4, 0, 0, 1, 1, 0), (0, 4, 0, 0, 0, 0), (2, 0, 0, 1, 1, 0), (4, 2, 1, 0, 0, 0), (4, 2, 0, 1, 1, 0),
+    (0, 8, 0, 0, 0, 0), (2, 2, 0, 1, 1, 0), (0, 1, 0, 0, 0, 1), (0, 0, 0, 0, 0, 1), (1, 1, 0, 0, 0, 1),
+    (1, 0, 0, 0, 0, 1), (2, 1, 0, 0, 0, 1), (2, 0, 0, 0, 0, 1), (0, 2, 0, 0, 0, 1), (3, 8, 0, 0, 0, 1),
+    (1, 2, 0, 0, 0, 1), (4, 1, 0, 0, 0, 1), (2, 2, 0, 0, 0, 1), (4, 0, 0, 0, 0, 1), (4, 2, 0, 0, 0, 1),
+    (4, 3, 0, 0, 0, 1), (4, 4, 0, 0, 0, 1), (4, 8, 0, 0, 0, 1), (0, 3, 0, 0, 0, 1), (1, 3, 0, 0, 0, 1),
+    (2, 3, 0, 0, 0, 1), (4, 1, 0, 1, 0, 1), (4, 1, 0, 1, 1, 1), (4, 1, 1, 0, 0, 1), (0, 1, 0, 1, 0, 1),
+    (1, 1, 1, 0, 0, 1), (2, 4, 0, 0, 0, 1), (4, 0, 0, 1, 0, 1), (4, 0, 0, 1, 1, 1), (4, 0, 1, 0, 0, 1),
+    (0, 1, 1, 0, 0, 1), (1, 1, 0, 1, 1, 1), (2, 0, 0, 1, 0, 1), (4, 2, 0, 1, 0, 1), (4, 2, 0, 1, 1, 1),
+    (4, 2, 1, 0, 0, 1), (0, 0, 0, 1, 0, 1), (1, 0, 0, 1, 1, 1), (2, 0, 0, 1, 1, 1), (4, 3, 0, 1, 0, 1),
+    (0, 1, 0, 0, 0, 2), (0, 0, 0, 0, 0, 2), (1, 1, 0, 0, 0, 2), (1, 0, 0, 0, 0, 2), (2, 1, 0, 0, 0, 2),
+    (2, 0, 0, 0, 0, 2), (0, 2, 0, 0, 0, 2), (3, 8, 0, 0, 0, 2), (1, 2, 0, 0, 0, 2), (4, 1, 0, 0, 0, 2),
+    (2, 2, 0, 0, 0, 2), (4, 0, 0, 0, 0, 2), (4, 2, 0, 0, 0, 2), (4, 3, 0, 0, 0, 2), (4, 4, 0, 0, 0, 2),
+    (4, 8, 0, 0, 0, 2), (0, 3, 0, 0, 0, 2), (1, 3, 0, 0, 0, 2), (2, 3, 0, 0, 0, 2), (4, 1, 0, 1, 0, 2),
+    (4, 1, 0, 1, 1, 2), (4, 1, 1, 0, 0, 2), (0, 1, 0, 1, 0, 2), (1, 1, 1, 0, 0, 2), (2, 4, 0, 0, 0, 2),
+    (4, 0, 0, 1, 0, 2), (4, 0, 0, 1, 1, 2), (4, 0, 1, 0, 0, 2), (0, 1, 1, 0, 0, 2), (1, 1, 0, 1, 1, 2),
+    (2, 0, 0, 1, 0, 2), (4, 2, 0, 1, 0, 2), (4, 2, 0, 1, 1, 2), (4, 2, 1, 0, 0, 2), (0, 0, 0, 1, 0, 2),
+    (1, 0, 0, 1, 1, 2), (2, 0, 0, 1, 1, 2), (4, 3, 0, 1, 0, 2), (4, 3, 0, 1, 1, 2), (1, 1, 0, 0, 0, 3),
+    (1, 0, 0, 0, 0, 3), (2, 1, 0, 0, 0, 3), (2, 0, 0, 0, 0, 3), (3, 8, 0, 0, 0, 3), (4, 1, 0, 0, 0, 3),
+    (1, 2, 0, 0, 0, 3), (4, 0, 0, 0, 0, 3), (2, 2, 0, 0, 0, 3), (4, 2, 0, 0, 0, 3), (4, 3, 0, 0, 0, 3),
+    (4, 4, 0, 0, 0, 3), (4, 8, 0, 0, 0, 3), (1, 3, 0, 0, 0, 3), (2, 3, 0, 0, 0, 3), (4, 1, 0, 1, 0, 3),
+    (4, 1, 1, 0, 0, 3), (1, 1, 1, 0, 0, 3), (2, 4, 0, 0, 0, 3), (4, 0, 0, 1, 0, 3), (4, 0, 1, 0, 0, 3),
+    (1, 4, 0, 0, 0, 3), (2, 0, 0, 1, 0, 3), (4, 2, 0, 1, 0, 3), (4, 2, 1, 0, 0, 3), (1, 8, 0, 0, 0, 3),
+    (2, 2, 0, 1, 0, 3), (4, 3, 0, 1, 0, 3), (1, 0, 0), (2, 3, 0, 1, 1, 0), (4, 3, 1, 0, 0, 0), (4, 3, 0, 1, 1, 0),
+    (4, 1, 1, 1, 1, 0), (4, 4, 1, 0, 0, 0), (2, 8, 0, 0, 0, 0), (4, 1, 0, 2, 1, 0), (4, 0, 1, 1, 1, 0),
+    (2, 0, 0, 2, 1, 0), (4, 0, 0, 2, 1, 0), (4, 2, 1, 1, 1, 0), (0, 2, 0, 1, 0, 1), (1, 2, 0, 1, 1, 1),
+    (2, 2, 0, 1, 0, 1), (4, 3, 1, 0, 0, 1), (4, 3, 0, 1, 1, 1), (4, 1, 1, 1, 0, 1), (4, 1, 1, 1, 1, 1),
+    (4, 4, 1, 0, 0, 1), (0, 1, 1, 1, 0, 1), (1, 1, 1, 1, 1, 1), (2, 2, 0, 1, 1, 1), (4, 4, 0, 1, 0, 1),
+    (4, 1, 0, 2, 1, 1), (4, 0, 1, 1, 0, 1), (0, 3, 0, 1, 0, 1), (1, 1, 0, 2, 1, 1), (3, 8, 0, 1, 0, 1),
+    (2, 3, 0, 1, 0, 1), (4, 8, 0, 1, 0, 1), (4, 0, 0, 2, 1, 1), (4, 0, 1, 1, 1, 1), (0, 4, 0, 1, 0, 1),
+    (1, 0, 0, 2, 1, 1), (2, 0, 0, 2, 1, 1), (0, 2, 0, 1, 0, 2), (1, 2, 0, 1, 1, 2), (2, 2, 0, 1, 0, 2),
+    (4, 3, 1, 0, 0, 2), (4, 1, 0, 2, 0, 2), (4, 1, 1, 1, 1, 2), (4, 4, 1, 0, 0, 2), (0, 1, 0, 2, 0, 2),
+    (1, 1, 1, 1, 1, 2), (2, 2, 0, 1, 1, 2), (4, 1, 1, 1, 0, 2), (4, 4, 0, 1, 1, 2), (4, 0, 1, 1, 0, 2),
+    (0, 1, 1, 1, 0, 2), (1, 3, 0, 1, 1, 2), (3, 8, 0, 1, 1, 2), (2, 3, 0, 1, 0, 2), (4, 8, 0, 1, 1, 2),
+    (4, 0, 0, 2, 0, 2), (4, 0, 1, 1, 1, 2), (0, 0, 0, 2, 0, 2), (1, 4, 0, 1, 1, 2), (2, 0, 0, 2, 0, 2),
+    (2, 3, 0, 1, 0, 3), (4, 3, 1, 0, 0, 3), (4, 1, 0, 2, 0, 3), (4, 4, 1, 0, 0, 3), (2, 8, 0, 0, 0, 3),
+    (4, 1, 1, 1, 0, 3), (4, 0, 1, 1, 0, 3), (2, 0, 0, 2, 0, 3), (4, 0, 0, 2, 0, 3), (4, 2, 1, 1, 0, 3), (1, 1, 0),
+    (0, 8, 1, 0, 0, 0), (2, 2, 0, 2, 1, 0), (3, 8, 1, 0, 0, 0), (4, 2, 0, 2, 1, 0), (4, 3, 1, 1, 1, 0),
+    (4, 8, 1, 0, 0, 0), (0, 4, 0, 0, 0, 1), (1, 2, 0, 2, 1, 1), (2, 2, 0, 2, 1, 1), (4, 2, 1, 1, 0, 1),
+    (4, 2, 0, 2, 1, 1), (0, 2, 0, 2, 0, 2), (1, 4, 0, 0, 0, 2), (2, 2, 0, 2, 0, 2), (4, 2, 0, 2, 0, 2),
+    (4, 2, 1, 1, 0, 2), (1, 8, 1, 0, 0, 3), (2, 2, 0, 2, 0, 3), (3, 8, 1, 0, 0, 3), (4, 2, 0, 2, 0, 3),
+    (4, 3, 1, 1, 0, 3), (4, 8, 1, 0, 0, 3), (0, 0, 0), (4, 1, 1, 2, 1, 0), (0, 6, 0, 0, 0, 0), (0, 7, 0, 0, 0, 0),
+    (2, 6, 0, 0, 0, 0), (2, 7, 0, 0, 0, 0), (4, 0, 1, 2, 1, 0), (4, 6, 0, 0, 0, 0), (0, 5, 0, 0, 0, 0),
+    (4, 7, 0, 0, 0, 0), (4, 5, 0, 0, 0, 0), (2, 5, 0, 0, 0, 0), (4, 1, 0, 3, 1, 0), (4, 2, 1, 2, 1, 0),
+    (2, 0, 0, 3, 1, 0), (4, 0, 0, 3, 1, 0), (4, 6, 1, 0, 0, 0), (2, 2, 0, 3, 1, 0), (4, 2, 0, 3, 1, 0),
+    (4, 7, 1, 0, 0, 0), (4, 1, 1, 3, 1, 0), (4, 1, 1, 2, 1, 1), (4, 2, 1, 1, 1, 1), (0, 8, 0, 0, 0, 1),
+    (4, 1, 1, 2, 0, 2), (4, 2, 1, 1, 1, 2), (4, 1, 0, 3, 0, 3), (1, 6, 0, 0, 0, 3), (1, 7, 0, 0, 0, 3),
+    (2, 6, 0, 0, 0, 3), (2, 7, 0, 0, 0, 3), (4, 0, 1, 2, 0, 3), (4, 6, 0, 0, 0, 3), (1, 5, 0, 0, 0, 3),
+    (4, 7, 0, 0, 0, 3), (4, 5, 0, 0, 0, 3), (2, 5, 0, 0, 0, 3), (4, 1, 1, 2, 0, 3), (4, 2, 1, 2, 0, 3),
+    (2, 0, 0, 3, 0, 3), (4, 0, 0, 3, 0, 3), (4, 6, 1, 0, 0, 3), (2, 2, 0, 3, 0, 3), (4, 2, 0, 3, 0, 3),
+    (4, 7, 1, 0, 0, 3), (4, 5, 1, 0, 0, 3), (4, 1, 1, 3, 0, 3), (2, 0, 1), (4, 5, 1, 0, 0, 0), (1, 1, 1, 2, 1, 1),
+    (2, 3, 0, 1, 1, 1), (4, 6, 0, 0, 0, 1), (4, 7, 0, 0, 0, 1), (4, 5, 0, 0, 0, 1), (3, 8, 1, 1, 0, 1),
+    (4, 8, 1, 1, 0, 1), (1, 6, 0, 0, 0, 2), (2, 3, 0, 1, 1, 2), (4, 6, 0, 0, 0, 2), (4, 7, 0, 0, 0, 2),
+    (4, 5, 0, 0, 0, 2), (4, 0, 1, 3, 0, 3), (2, 1, 1), (4, 3, 1, 1, 0, 1), (4, 3, 0, 2, 1, 1), (1, 3, 0, 2, 1, 1),
+    (2, 3, 0, 2, 1, 1), (0, 6, 0, 0, 0, 1), (4, 4, 0, 2, 1, 1), (4, 0, 1, 2, 1, 1), (4, 6, 0, 1, 0, 1),
+    (1, 4, 0, 2, 1, 1), (2, 4, 0, 2, 1, 1), (0, 7, 0, 0, 0, 1), (4, 4, 0, 1, 1, 1), (4, 2, 1, 2, 1, 1),
+    (4, 7, 0, 1, 0, 1), (1, 3, 0, 1, 1, 1), (2, 4, 0, 1, 0, 1), (0, 5, 0, 0, 0, 1), (4, 6, 0, 1, 1, 1),
+    (4, 3, 1, 1, 1, 1), (4, 5, 0, 1, 0, 1), (1, 4, 0, 1, 1, 1), (3, 8, 1, 1, 1, 2), (4, 3, 0, 2, 0, 2),
+    (4, 8, 1, 1, 1, 2), (4, 3, 1, 1, 0, 2), (0, 1, 1, 2, 0, 2), (1, 7, 0, 0, 0, 2), (2, 3, 0, 2, 0, 2),
+    (4, 4, 0, 2, 0, 2), (4, 0, 1, 2, 0, 2), (4, 6, 0, 1, 1, 2), (0, 3, 0, 2, 0, 2), (1, 5, 0, 0, 0, 2),
+    (2, 4, 0, 2, 0, 2), (4, 4, 0, 1, 0, 2), (4, 2, 1, 2, 0, 2), (4, 7, 0, 1, 1, 2), (0, 4, 0, 2, 0, 2),
+    (1, 8, 0, 0, 0, 2), (3, 8, 0, 1, 0, 2), (2, 4, 0, 1, 0, 2), (4, 8, 0, 1, 0, 2), (1, 6, 0, 1, 1, 2),
+    (4, 3, 1, 1, 1, 2), (4, 5, 0, 1, 1, 2), (0, 3, 0, 1, 0, 2), (1, 2, 0), (2, 3, 0, 3, 1, 0), (4, 0, 1, 3, 1, 0),
+    (4, 3, 0, 3, 1, 0), (2, 4, 0, 3, 1, 0), (4, 4, 0, 3, 1, 0), (0, 6, 0, 1, 0, 1), (2, 4, 0, 1, 1, 1),
+    (4, 3, 1, 2, 1, 1), (4, 7, 0, 1, 1, 1), (1, 7, 0, 1, 1, 2), (2, 4, 0, 1, 1, 2), (4, 3, 1, 2, 0, 2),
+    (2, 3, 0, 3, 0, 3), (4, 2, 1, 3, 0, 3), (4, 3, 0, 3, 0, 3), (2, 1, 0), (2, 0, 0), (4, 2, 1, 3, 1, 0),
+    (1, 4, 0, 0, 0, 1), (2, 6, 0, 0, 0, 1), (0, 4, 0, 1, 0, 2), (2, 6, 0, 0, 0, 2), (4, 6, 0, 1, 0, 2),
+    (2, 4, 0, 3, 0, 3), (4, 4, 0, 3, 0, 3), (2, 2, 0), (0, 7, 0, 1, 0, 1), (2, 2, 1), (2, 3, 0, 2, 1, 0),
+    (4, 3, 0, 2, 1, 0), (4, 4, 1, 2, 1, 1), (4, 5, 0, 1, 1, 1), (1, 5, 0, 1, 1, 2), (4, 4, 1, 2, 0, 2), (2, 1, 2),
+    (1, 6, 0, 0, 0, 1), (0, 4, 0, 0, 0, 2), (3, 0, 0), (2, 4, 0, 2, 1, 0), (4, 3, 1, 3, 1, 0), (4, 4, 0, 2, 1, 0),
+    (0, 5, 0, 1, 0, 1), (2, 7, 0, 0, 0, 1), (3, 8, 0, 1, 1, 1), (4, 4, 1, 1, 0, 1), (1, 7, 0, 0, 0, 1),
+    (4, 8, 0, 1, 1, 1), (2, 5, 0, 0, 0, 1), (4, 6, 0, 2, 1, 1), (1, 8, 0, 1, 1, 2), (2, 7, 0, 0, 0, 2),
+    (4, 4, 1, 1, 0, 2), (0, 6, 0, 0, 0, 2), (4, 7, 0, 1, 0, 2), (1, 8, 1, 1, 1, 2), (4, 5, 0, 1, 0, 2),
+    (2, 5, 0, 0, 0, 2), (2, 3, 0, 2, 0, 3), (4, 3, 1, 3, 0, 3), (4, 3, 0, 2, 0, 3), (3, 1, 0), (2, 4, 0, 1, 1, 0),
+    (4, 4, 1, 3, 1, 0), (4, 4, 0, 1, 1, 0), (5, 8, 0, 0, 0, 0), (0, 8, 0, 1, 0, 1), (0, 8, 1, 1, 0, 1),
+    (1, 5, 0, 0, 0, 1), (2, 8, 0, 0, 0, 1), (4, 4, 1, 1, 1, 1), (4, 7, 0, 2, 1, 1), (0, 7, 0, 0, 0, 2),
+    (4, 4, 1, 1, 1, 2), (4, 6, 0, 2, 0, 2), (2, 8, 0, 0, 0, 2), (2, 4, 0, 2, 0, 3), (4, 4, 1, 3, 0, 3),
+    (4, 4, 0, 2, 0, 3), (5, 8, 0, 0, 0, 3), (5, 8, 1, 0, 0, 3), (4, 0, 0), (2, 2, 2), (4, 3, 1, 2, 1, 0),
+    (5, 8, 1, 0, 0, 0), (2, 4, 0, 1, 0, 3), (4, 4, 0, 1, 0, 3), (1, 3, 0), (2, 6, 0, 1, 1, 0), (4, 6, 0, 1, 1, 0),
+    (4, 4, 1, 2, 1, 0), (2, 7, 0, 1, 1, 0), (4, 7, 0, 1, 1, 0), (4, 4, 1, 1, 1, 0), (2, 6, 0, 1, 0, 1),
+    (1, 8, 0, 0, 0, 1), (4, 6, 1, 0, 0, 1), (5, 8, 0, 0, 0, 1), (4, 5, 0, 2, 1, 1), (5, 8, 0, 1, 0, 1),
+    (2, 6, 0, 1, 0, 2), (4, 6, 1, 0, 0, 2), (0, 5, 0, 0, 0, 2), (5, 8, 0, 0, 0, 2), (4, 3, 1, 2, 0, 3),
+    (2, 6, 0, 1, 0, 3), (4, 6, 0, 1, 0, 3), (4, 4, 1, 2, 0, 3), (2, 7, 0, 1, 0, 3), (4, 7, 0, 1, 0, 3),
+    (4, 4, 1, 1, 0, 3), (2, 2, 4), (2, 5, 0, 1, 1, 0), (4, 5, 0, 1, 1, 0), (4, 7, 0, 2, 0, 2), (5, 8, 0, 1, 1, 2),
+    (2, 5, 0, 1, 0, 3), (4, 5, 0, 1, 0, 3), (2, 3, 1), (1, 6, 0, 1, 1, 1), (2, 6, 0, 1, 1, 1), (3, 8, 0, 2, 1, 1),
+    (4, 7, 1, 0, 0, 1), (4, 8, 0, 2, 1, 1), (5, 8, 1, 1, 0, 1), (2, 1, 4), (3, 8, 0, 1, 1, 0), (4, 8, 0, 1, 1, 0),
+    (4, 6, 1, 1, 1, 0), (2, 6, 0, 1, 1, 2), (4, 7, 1, 0, 0, 2), (5, 8, 1, 1, 1, 2), (3, 8, 0, 1, 0, 3),
+    (4, 8, 0, 1, 0, 3), (4, 6, 1, 1, 0, 3), (2, 0, 2), (3, 8, 1, 2, 1, 1), (4, 8, 1, 2, 1, 1), (5, 8, 0, 1, 1, 1),
+    (0, 8, 0, 0, 0, 2), (4, 5, 0, 2, 0, 2), (5, 8, 0, 1, 0, 2), (2, 0, 4), (2, 0, 3), (1, 7, 0, 1, 1, 1),
+    (2, 7, 0, 1, 0, 1), (4, 5, 1, 0, 0, 1), (0, 6, 0, 1, 0, 2), (2, 7, 0, 1, 0, 2), (3, 8, 0, 2, 0, 2),
+    (4, 5, 1, 0, 0, 2), (4, 8, 0, 2, 0, 2), (2, 2, 3), (2, 6, 0, 2, 1, 0), (4, 6, 0, 2, 1, 0), (4, 7, 1, 1, 1, 0),
+    (4, 7, 1, 1, 0, 3), (2, 1, 3), (0, 8, 1, 0, 0, 1), (3, 8, 1, 0, 0, 1), (4, 8, 1, 0, 0, 1), (1, 8, 1, 0, 0, 2),
+    (3, 8, 1, 0, 0, 2), (3, 8, 1, 2, 0, 2), (4, 8, 1, 0, 0, 2), (4, 8, 1, 2, 0, 2), (2, 6, 0, 2, 0, 3),
+    (4, 6, 0, 2, 0, 3), (2, 3, 2), (1, 5, 0, 1, 1, 1), (2, 7, 0, 1, 1, 1), (5, 8, 0, 1, 0, 3), (2, 3, 3),
+    (5, 8, 0, 1, 1, 0), (4, 6, 1, 1, 0, 1), (3, 8, 1, 1, 1, 1), (4, 8, 1, 1, 1, 1), (1, 8, 1, 0, 0, 1),
+    (2, 5, 0, 1, 0, 1), (1, 8, 0, 1, 1, 1), (4, 6, 1, 1, 1, 1), (1, 6, 0, 2, 1, 1), (2, 5, 0, 1, 1, 1),
+    (0, 7, 0, 1, 0, 2), (2, 7, 0, 1, 1, 2), (5, 0, 0), (2, 7, 0, 2, 1, 0), (4, 7, 0, 2, 1, 0), (4, 5, 1, 1, 1, 0),
+    (2, 7, 0, 2, 0, 3), (4, 7, 0, 2, 0, 3), (4, 5, 1, 1, 0, 3), (2, 3, 0), (4, 6, 1, 1, 0, 2), (2, 3, 4),
+    (4, 7, 1, 1, 0, 1), (3, 8, 1, 1, 0, 2), (2, 5, 0, 1, 0, 2), (4, 8, 1, 1, 0, 2), (3, 2, 0), (2, 5, 0, 2, 1, 0),
+    (3, 8, 1, 1, 1, 0), (4, 5, 0, 2, 1, 0), (4, 8, 1, 1, 1, 0), (4, 6, 1, 2, 1, 0), (1, 7, 0, 2, 1, 1),
+    (2, 6, 0, 2, 1, 1), (4, 7, 1, 1, 1, 1), (5, 8, 0, 2, 1, 1), (5, 8, 1, 2, 1, 1), (0, 5, 0, 1, 0, 2),
+    (4, 6, 1, 1, 1, 2), (2, 5, 0, 1, 1, 2), (2, 5, 0, 2, 0, 3), (3, 8, 0, 2, 0, 3), (4, 5, 0, 2, 0, 3),
+    (4, 8, 0, 2, 0, 3), (4, 6, 1, 2, 0, 3), (3, 3, 0), (3, 8, 0, 2, 1, 0), (4, 8, 0, 2, 1, 0), (4, 7, 1, 2, 1, 0),
+    (1, 5, 0, 2, 1, 1), (2, 7, 0, 2, 1, 1), (4, 5, 1, 1, 0, 1), (5, 8, 1, 0, 0, 1), (5, 8, 1, 1, 1, 1),
+    (0, 8, 0, 1, 0, 2), (0, 8, 1, 0, 0, 2), (4, 7, 1, 1, 0, 2), (2, 6, 0, 2, 0, 2), (5, 8, 0, 2, 0, 2),
+    (3, 8, 1, 1, 0, 3), (4, 8, 1, 1, 0, 3), (4, 7, 1, 2, 0, 3), (5, 1, 0), (2, 6, 0, 3, 1, 0), (4, 6, 0, 3, 1, 0),
+    (4, 5, 1, 2, 1, 0), (2, 7, 0, 3, 1, 0), (4, 7, 0, 3, 1, 0), (4, 6, 1, 3, 1, 0), (1, 8, 1, 1, 1, 1),
+    (2, 5, 0, 2, 1, 1), (1, 8, 0, 2, 1, 1), (4, 5, 1, 1, 1, 1), (1, 8, 1, 2, 1, 1), (4, 6, 1, 2, 1, 1),
+    (4, 7, 1, 2, 1, 1), (0, 6, 0, 2, 0, 2), (5, 8, 1, 0, 0, 2), (4, 7, 1, 1, 1, 2), (5, 8, 1, 2, 0, 2),
+    (2, 7, 0, 2, 0, 2), (0, 7, 0, 2, 0, 2), (4, 5, 1, 1, 0, 2), (2, 5, 0, 2, 0, 2), (0, 5, 0, 2, 0, 2),
+    (4, 5, 1, 1, 1, 2), (0, 8, 0, 2, 0, 2), (0, 8, 1, 1, 0, 2), (4, 6, 1, 2, 0, 2), (0, 8, 1, 2, 0, 2),
+    (4, 7, 1, 2, 0, 2), (2, 6, 0, 3, 0, 3), (4, 6, 0, 3, 0, 3), (4, 5, 1, 2, 0, 3), (2, 7, 0, 3, 0, 3),
+    (4, 7, 0, 3, 0, 3), (4, 6, 1, 3, 0, 3), (6, 0, 0), (7, 1, 1), (2, 5, 0, 3, 1, 0), (4, 5, 0, 3, 1, 0),
+    (4, 5, 1, 2, 1, 1), (7, 0, 0), (3, 8, 1, 2, 1, 0), (4, 8, 1, 2, 1, 0), (5, 8, 1, 1, 1, 0), (4, 7, 1, 3, 1, 0),
+    (5, 8, 0, 2, 1, 0), (3, 8, 0, 3, 1, 0), (4, 8, 0, 3, 1, 0), (3, 8, 1, 3, 1, 0), (4, 8, 1, 3, 1, 0),
+    (5, 8, 1, 2, 1, 0), (4, 5, 1, 3, 1, 0), (5, 8, 0, 3, 1, 0), (4, 5, 1, 2, 0, 2), (5, 8, 1, 1, 0, 2),
+    (2, 5, 0, 3, 0, 3), (4, 5, 0, 3, 0, 3), (7, 3, 1), (8, 0, 0), (5, 8, 1, 3, 1, 0), (5, 8, 0, 2, 0, 3), (8, 1, 1),
+    (7, 1, 0), (3, 8, 0, 3, 0, 3), (4, 8, 0, 3, 0, 3), (4, 7, 1, 3, 0, 3), (5, 8, 1, 1, 0, 3), (7, 2, 1), (8, 3, 1),
+    (3, 8, 1, 2, 0, 3), (4, 8, 1, 2, 0, 3), (7, 2, 0), (3, 8, 1, 3, 0, 3), (4, 5, 1, 3, 0, 3), (4, 8, 1, 3, 0, 3),
+    (8, 2, 1), (5, 8, 0, 3, 0, 3), (7, 3, 0), (5, 8, 1, 2, 0, 3), (8, 1, 0), (5, 8, 1, 3, 0, 3), (8, 2, 0), (8, 3, 0),
 )
 
 
@@ -94,6 +152,10 @@
         pl.when(condition)(body)
 
 
+def aligned(at, size):
+    return at if isinstance(at, int) else pl.multiple_of(at, size)
+
+
 class Part:
     def __init__(self, number, wide, crossing, place, base):
         self.number, self.wide, self.crossing, self.place, self.base = number, wide, crossing, place, base
@@ -112,14 +174,16 @@
 
 def layer_kernel(sizes, *refs):
     n_sp, n_out, n_tp, n_proj, separate = sizes
-    tok, gain, taps, sinks = refs[:4]
+    tok = refs[0]
     n_in = 6 if separate else 5
     w_own = refs[4 : 4 + n_in]
     out_own = refs[4 + n_in : 6 + n_in]
     out = refs[6 + n_in]
     (tokf, w_all, wo_all, q_buf, kv_buf, inner, gate_b, product, m_att, m_conv, r_att, r_conv, bias,
      send_sem, recv_sem, own_sem, wo_send, wo_recv, tok_send, tok_recv, halo_send, halo_recv,
-     mix_send, mix_recv, cross_send, cross_recv, pass_send, pass_recv) = refs[7 + n_in :]
+     mix_send, mix_recv, cross_send, cross_recv, pass_send, pass_recv,
+     out_buf, out_sem, gain, taps, sinks) = refs[7 + n_in :]
+    out_hbm, out = out, out_buf
     n_fs = 2 * n_out
     shards = n_sp * n_fs
     s, f, t = lax.axis_index("sp"), lax.axis_index("fs"), lax.axis_index("tp")
@@ -133,7 +197,12 @@
     owned = rows_total // n_tp
     chunks = 4
     step = rows_total // chunks
-    order = [chunks - 1] + list(range(chunks - 1))
+    tabled = (n_sp, n_out, n_tp) == TABLE_FOR
+    order = [3, 0, 1, 2]
+    attended = [0, 1, 2, 3]
+    if tabled:
+        order = [3, 2 - 2 * t, 1, 2 * t]
+        attended = [3 - 3 * t, 2 - t, 1 + t, 3 * t]
     me = s * n_fs + f
 
     right, left, core = (s + 1, f, t), (s - 1, f, t), (s, o * 2 + (1 - i), t)
@@ -148,6 +217,8 @@
         local.append(pltpu.make_async_copy(w_own[n], place, own_sem.at[n]))
     for a in range(2):
         local.append(pltpu.make_async_copy(out_own[a], wo_all.at[2 * t + a, me], own_sem.at[6 + a]))
+    for n, (source_ref, spot) in enumerate(zip(refs[1:4], (gain, taps, sinks))):
+        local.append(pltpu.make_async_copy(source_ref, spot, own_sem.at[9 + n]))
     my_cols = pl.ds(pl.multiple_of(t * cols, cols), cols)
     local.append(pltpu.make_async_copy(tok, tokf.at[:, my_cols], own_sem.at[8]))
     for copy in local:
@@ -164,23 +235,28 @@
 
     wo_copies, tok_copies = [], {}
     direct = pl.ds(0, 3 * (out_rows // 4))
-    for k, peer in enumerate(peers):
-        for a in range(2):
-            copy = pltpu.make_async_remote_copy(
-                src_ref=out_own[a].at[direct], dst_ref=wo_all.at[2 * t + a, me, direct],
-                send_sem=wo_send.at[k, a], recv_sem=wo_recv.at[k, a], device_id=peer, device_id_type=MESH,
-            )
-            copy.start()
-            wo_copies.append(copy)
-    for n in order:
-        here = pl.ds(n * step, step)
+    def send_direct():
+        for k, peer in enumerate(peers):
+            for a in range(2):
+                copy = pltpu.make_async_remote_copy(
+                    src_ref=out_own[a].at[direct], dst_ref=wo_all.at[2 * t + a, me, direct],
+                    send_sem=wo_send.at[k, a], recv_sem=wo_recv.at[k, a], device_id=peer, device_id_type=MESH,
+                )
+                copy.start()
+                wo_copies.append(copy)
+
+    wanted = [3, 2 * t, 1, 2 - 2 * t] if tabled else order
+    for turn, n in enumerate(wanted):
+        if turn == DIRECT_AFTER:
+            send_direct()
+        here = pl.ds(aligned(n * step, step), step)
         for k, peer in enumerate(peers):
             copy = pltpu.make_async_remote_copy(
                 src_ref=tok.at[here], dst_ref=tokf.at[here, my_cols],
-                send_sem=tok_send.at[k, n], recv_sem=tok_recv.at[k, n], device_id=peer, device_id_type=MESH,
+                send_sem=tok_send.at[k, turn], recv_sem=tok_recv.at[k, turn], device_id=peer, device_id_type=MESH,
             )
             copy.start()
-            tok_copies[k, n] = copy
+            tok_copies[k, turn] = copy
 
     parts, base = [], 0
     for number, (wide, crossing, rows) in enumerate(part_kinds(out_rows)):
@@ -219,7 +295,7 @@
     def source(k, at):
         return at * n_fs + lax.rem(o + n_out - k, n_out) * 2 + i
 
-    def handle(part, k, distance, side, at, drain):
+    def handle(part, k, distance, side, at, drain, ways=WAYS, arrival=True):
         first = isinstance(distance, int) and distance == 0
         src = source(k, at)
         mine = (at + distance if side == 0 else at - distance) if isinstance(at, int) else s
@@ -235,21 +311,22 @@
             copy = copy_of(part, src, where, lane, distance, way)
             copy.wait_send() if drain else copy.start()
 
-        if not (first and k == 0) and not drain:
+        if arrival and not (first and k == 0) and not drain:
             copy_of(part, src, core, 0, 0, 0).wait_recv()
         if k == 0 or part.wide:
-            if first or side == 0:
+            if RIGHT in ways and (first or side == 0):
                 when(more_right, lambda: go(right, lane_z, 0))
-            if first or side == 1:
+            if LEFT in ways and (first or side == 1):
                 when(more_left, lambda: go(left, lane_z, 1))
-        if k == 0 and (first or not part.wide):
+        if ACROSS in ways and k == 0 and (first or not part.wide):
             for n, where in enumerate(across):
                 go(where, 2 + n, side)
-        if part.crossing:
+        if CROSS in ways and part.crossing:
             for n in range(len(peers)):
                 copy = cross_copy(part, src, n)
                 copy.wait_send() if drain else copy.start()
-        go(core, lane_core, side)
+        if CORE in ways:
+            go(core, lane_core, side)
 
     def hand_over(part, src, drain):
         for k in range(len(peers)):
@@ -286,29 +363,21 @@
 
         lax.fori_loop(0, step // size, body, 0)
 
-    def project(number, ns):
-        def body(m, carry):
-            n = m if len(ns) == chunks else ns[0] + m
-            first = n * step if isinstance(n, int) else pl.multiple_of(n * step, step)
-            here = pl.ds(first, step)
-            result = jnp.dot(tokf[here, :], w_all[number], preferred_element_type=F32).astype(BF16)
-            if number == 0:
-                q_buf[here, :] = result
-            elif number == 1:
-                kv_buf[pl.ds(first + WINDOW, step), :] = result
-            elif number == 2:
-                inner[here, :] = result
-            elif number == 3:
-                gate_b[here, :] = result
-            else:
-                made = result.astype(F32) * inner[here, :].astype(F32)
-                product[pl.ds(first + HALO, step), :] = made.astype(BF16)
-            return carry
-
-        if len(ns) == 1:
-            body(0, 0)
+    def project(number, n):
+        first = aligned(n * step, step)
+        here = pl.ds(first, step)
+        result = jnp.dot(tokf[here, :], w_all[number], preferred_element_type=F32).astype(BF16)
+        if number == 0:
+            q_buf[here, :] = result
+        elif number == 1:
+            kv_buf[pl.ds(first + WINDOW, step), :] = result
+        elif number == 2:
+            inner[here, :] = result
+        elif number == 3:
+            gate_b[here, :] = result
         else:
-            lax.fori_loop(0, len(ns), body, 0)
+            made = result.astype(F32) * inner[here, :].astype(F32)
+            product[pl.ds(first + HALO, step), :] = made.astype(BF16)
 
     def halo_copy(which):
         buffer, size = ((kv_buf, WINDOW), (product, HALO))[which]
@@ -377,11 +446,11 @@
 
         lax.fori_loop(0, step // WINDOW, body, 0)
 
-    def convolve():
+    def convolve(start, count):
         size = 64
 
         def body(r, carry):
-            first = pl.multiple_of(r * size, size)
+            first = pl.multiple_of(start + r * size, size)
             padded = product[pl.ds(first, size + HALO), :].astype(F32)
             tap = taps[...].astype(F32)
             filtered = (
@@ -392,7 +461,7 @@
             m_conv[pl.ds(first, size), :] = (gate_b[pl.ds(first, size), :].astype(F32) * filtered).astype(BF16)
             return carry
 
-        lax.fori_loop(0, rows_total // size, body, 0)
+        lax.fori_loop(0, count // size, body, 0)
 
     def mix_copy(which, k):
         source, target = ((m_att, r_att), (m_conv, r_conv))[which]
@@ -444,8 +513,15 @@
             return carry
 
         lax.fori_loop(0, owned // tile, body, 0)
-
-    own_weights, own_out, own_tokens = local[:-3], local[-3:-1], local[-1]
+        if not own:
+            out_copy(source_s).start()
+
+    def out_copy(source_s):
+        block = n_fs * out_cols
+        where = pl.ds(pl.multiple_of(source_s * block, block), block)
+        return pltpu.make_async_copy(out.at[:, where], out_hbm.at[:, where], out_sem.at[source_s])
+
+    own_weights, own_out, small, own_tokens = local[:-6], local[-6:-4], local[-4:-1], local[-1]
     waited = set()
 
     def once(key, body):
@@ -465,25 +541,28 @@
         if kind == 0:
             make_bias()
         elif kind == 1:
-            once("tokens", own_tokens.wait)
+            once("tokens", lambda: wait_all(small + [own_tokens]))
             for k in range(n_tp - 1):
                 tok_copies[k, n].wait_recv()
-            norm(n)
+            norm(order[n])
         elif kind == 2:
             once(("part", side), lambda: finish(side))
-            project(side, [n])
-            if n == chunks - 1 and side in (1, 4):
+            project(side, order[n])
+            if n == 0 and side in (1, 4):
                 halo_out(0 if side == 1 else 1)
         elif kind == 3:
-            if n == 0:
-                halo_in(0)
-            attend(n)
+            once("halo", lambda: halo_in(0))
+            attend(attended[n])
         elif kind == 4:
             mix_out(0)
         elif kind == 5:
-            halo_in(1)
-            convolve()
-            mix_out(1)
+            once("product", lambda: halo_in(1))
+            if not tabled:
+                convolve(0, rows_total)
+            else:
+                convolve((t if n == 1 else 1 - t) * owned, owned)
+            if n == 0:
+                mix_out(1)
         elif kind == 6:
             mix_in()
         elif n == 0:
@@ -494,7 +573,6 @@
             when(s + n < n_sp, lambda: project_out(s + n, kind == 7))
 
     wait_all(own_weights)
-    tabled = (n_sp, n_out, n_tp) == TABLE_FOR
     if tabled:
         events = []
 
@@ -503,17 +581,19 @@
                 turn = [entry for entry in events if entry[5] == mine]
 
                 def body(mine=mine, turn=turn):
-                    for passing, number, k, distance, side, _ in turn:
+                    for way, number, k, distance, side, _ in turn:
                         part = parts[number]
                         at = mine - distance if side == 0 else mine + distance
-                        if passing:
+                        if way == HAND:
                             hand_over(part, source(k, at), False)
                             continue
                         if distance == 0 and k == 0 and number >= n_proj:
                             once(("own", mine), lambda: wait_all(own_out))
                             if not part.crossing:
                                 once(("direct", mine), wo_ready)
-                        handle(part, k, distance, side, at, False)
+                        piece = (mine, number, k, distance, side)
+                        handle(part, k, distance, side, at, False, (way,), piece not in waited)
+                        waited.add(piece)
 
                 if turn:
                     pl.when(s == mine)(body)
@@ -541,7 +621,7 @@
         for part in parts[:n_proj]:
             spread(part)
         job(0, 0, 0)
-        for n in order:
+        for n in range(chunks):
             job(1, n, 0)
             job(2, n, 0)
             job(2, n, 1)
@@ -549,7 +629,7 @@
             job(3, n, 0)
         job(4, 0, 0)
         for number in (2, 3, 4):
-            for n in order:
+            for n in range(chunks):
                 job(2, n, number)
         job(5, 0, 0)
         for part in parts[n_proj:]:
@@ -561,17 +641,19 @@
         for own in (True, False):
             lax.fori_loop(0, n_sp, lambda n, c, own=own: (project_out(n, own), c)[1], 0)
 
+    for source_s in range(n_sp):
+        out_copy(source_s).wait()
     if tabled:
         events = [entry for entry in TABLE if len(entry) == 6]
         for mine in range(n_sp):
 
             def drain(mine=mine):
-                for passing, number, k, distance, side, _ in [entry for entry in events if entry[5] == mine]:
+                for way, number, k, distance, side, _ in [entry for entry in events if entry[5] == mine]:
                     at = mine - distance if side == 0 else mine + distance
-                    if passing:
+                    if way == HAND:
                         hand_over(parts[number], source(k, at), True)
                     else:
-                        handle(parts[number], k, distance, side, at, True)
+                        handle(parts[number], k, distance, side, at, True, (way,))
 
             pl.when(s == mine)(drain)
     else:
@@ -609,12 +691,11 @@
     kv_here = kv_cols // HEAD
     group = q_cols // kv_cols
     dma = pltpu.SemaphoreType.DMA
-    vmem, anywhere = pl.BlockSpec(memory_space=pltpu.VMEM), pl.BlockSpec(memory_space=pl.ANY)
     summed = pl.pallas_call(
         functools.partial(layer_kernel, (n_sp, n_out, n_tp, 5, separate)),
         out_shape=jax.ShapeDtypeStruct((owned, width), BF16),
-        in_specs=[anywhere, vmem, vmem, pl.BlockSpec(memory_space=pltpu.SMEM)] + [anywhere] * (len(weights) + 2),
-        out_specs=vmem,
+        in_specs=[pl.BlockSpec(memory_space=pltpu.HBM)] * (len(weights) + 6),
+        out_specs=pl.BlockSpec(memory_space=pl.ANY),
         scratch_shapes=[
             pltpu.VMEM((rows, width), BF16),
             pltpu.VMEM((5, width, q_cols), BF16),
@@ -631,7 +712,7 @@
             pltpu.VMEM((kv_here, group * WINDOW, 2 * WINDOW), F32),
             dma((lanes * n_sp * 2,)),
             dma((len(kinds) * shards,)),
-            dma((9,)),
+            dma((12,)),
             dma((n_tp - 1, 2)),
             dma((n_tp - 1, 2)),
             dma((n_tp - 1, 4)),
@@ -644,12 +725,45 @@
             dma((n_tp - 1, shards)),
             dma((n_tp - 1, shards)),
             dma((n_tp - 1, shards)),
+            pltpu.VMEM((owned, width), BF16),
+            dma((n_sp,)),
+            pltpu.VMEM((1, width), F32),
+            pltpu.VMEM(conv_taps.shape, BF16),
+            pltpu.SMEM(sink_logits.shape, F32),
         ],
         compiler_params=pltpu.CompilerParams(
             collective_id=0, has_side_effects=True, vmem_limit_bytes=60 * 1024 * 1024
         ),
     )(tokens[0], norm_gain[None], conv_taps, sink_logits, *weights, w_attn_out, w_conv_out)
-    return summed[None]
+    return copy_out(summed)[None]
+
+
+def copy_out(array):
+    rows, width = array.shape
+    count = 8
+    step = rows // count
+
+    def kernel(source, target, held, sem):
+        cut = lambda n: pl.ds(n * step, step)
+        reads = [pltpu.make_async_copy(source.at[cut(n)], held.at[cut(n)], sem.at[0, n]) for n in range(count)]
+        writes = [pltpu.make_async_copy(held.at[cut(n)], target.at[cut(n)], sem.at[1, n]) for n in range(count)]
+        for copy in reads:
+            copy.start()
+        for read, write in zip(reads, writes):
+            read.wait()
+            write.start()
+        for copy in writes:
+            copy.wait()
+
+    anywhere = pl.BlockSpec(memory_space=pl.ANY)
+    return pl.pallas_call(
+        kernel,
+        out_shape=jax.ShapeDtypeStruct(array.shape, array.dtype),
+        in_specs=[anywhere],
+        out_specs=anywhere,
+        scratch_shapes=[pltpu.VMEM(array.shape, array.dtype), pltpu.SemaphoreType.DMA((2, count))],
+        compiler_params=pltpu.CompilerParams(vmem_limit_bytes=60 * 1024 * 1024),
+    )(array)
 
 
 def solution(mesh):

time: 120 us -> 107 us (0.89)
  Pallas kernels: 117 us -> 107 us
  local copies, waits for them, and re-layouts: 3.16 us -> 0 us
    pallas_call x1, Pallas kernels: 117 us -> 104 us  [on_device(): pl.pallas_call(functools.partial(layer_kernel, (n_sp, n_out, n_tp, 5, sep...]
    unnamed x1 -> x0, local copies, waits for them, and re-layouts: 3.16 us -> none
    pallas_call x0 -> x1, Pallas kernels: none -> 2.4 us  [copy_out(): pl.pallas_call(kernel, out_shape=jax.ShapeDtypeStruct(array.shape, array....]
where the time goes in v4:
time: 107 us
  Pallas kernels  107 us (100%)
    pallas_call x1, Pallas kernels, on_device(): pl.pallas_call(functools.partial(layer_kernel, (n_sp, n_out, n_tp, 5, sep...  104 us
    pallas_call x1, Pallas kernels, copy_out(): pl.pallas_call(kernel, out_shape=jax.ShapeDtypeStruct(array.shape, array....  2.4 us

profile of v4, /device:TPU:0, one launch (start us, length us, event | category | flops | bytes accessed | tf_op | source)
XLA Modules:
  0.0 106.7 jit_solution(4537433659564339505)
XLA Ops:
  0.0 104.2 %shard_map.118.source = bf16[512,2048]{1,0:T(8,128)(2,1)} custom-call(bf16[1024,1024]{1,0:T(8,128)(2,1)} %bitcast.3, f32[1,2048]{1,0:T(1,128)} %bitcast.4, bf16[3,512]{1,0:T(4,128)(2,1)} %refs_2_.1, f32[8]{0:T(128)} %refs_3_.1, bf16[128,512]{1,0:T(8,128)(2,1)} %refs_4_.1, bf16[128,256]{1,0:T(8,128)(2,1)} %refs_5_.1, bf16[128,256]{1,0:T(8,128)(2,1)} %refs_6_.1, ...), custom_call_target="tpu_custom_call" | custom-call | tf_op jit(solution)/shard_map/pallas_call | solution.py:694
  104.2 2.4 %shard_map.119 = bf16[512,2048]{1,0:T(8,128)(2,1)} custom-call(bf16[512,2048]{1,0:T(8,128)(2,1)} %shard_map.118.source), custom_call_target="tpu_custom_call" | custom-call | tf_op jit(solution)/shard_map/pallas_call | solution.py:759

commit v5 on v4

--- a/solution.py
+++ b/solution.py
@@ -489,7 +489,7 @@
                     for k in range(n_tp - 1):
                         pass_copy(parts[number], source_s * n_fs + source_o * 2 + (1 - i), k).wait_recv()
         block = n_fs * out_cols
-        tile = min(256, owned)
+        tile = min(512, owned)
 
         def weights(row):
             blocks = [wo_all[row, source_s * n_fs + n] for n in range(n_fs)]

time: 107 us -> 107 us (level)
  no operation moved by 1% of the time
where the time goes in v5:
time: 107 us; the launch traced here: 106 us
  Pallas kernels  106 us (99%)
    pallas_call x1, Pallas kernels, on_device(): pl.pallas_call(functools.partial(layer_kernel, (n_sp, n_out, n_tp, 5, sep...  103 us
    pallas_call x1, Pallas kernels, copy_out(): pl.pallas_call(kernel, out_shape=jax.ShapeDtypeStruct(array.shape, array....  2.4 us

profile of v5, /device:TPU:0, one launch (start us, length us, event | category | flops | bytes accessed | tf_op | source)
XLA Modules:
  0.0 105.7 jit_solution(15503084442504342375)
XLA Ops:
  0.0 103.1 %shard_map.118.source = bf16[512,2048]{1,0:T(8,128)(2,1)} custom-call(bf16[1024,1024]{1,0:T(8,128)(2,1)} %bitcast.3, f32[1,2048]{1,0:T(1,128)} %bitcast.4, bf16[3,512]{1,0:T(4,128)(2,1)} %refs_2_.1, f32[8]{0:T(128)} %refs_3_.1, bf16[128,512]{1,0:T(8,128)(2,1)} %refs_4_.1, bf16[128,256]{1,0:T(8,128)(2,1)} %refs_5_.1, bf16[128,256]{1,0:T(8,128)(2,1)} %refs_6_.1, ...), custom_call_target="tpu_custom_call" | custom-call | tf_op jit(solution)/shard_map/pallas_call | solution.py:694
  103.2 2.4 %shard_map.119 = bf16[512,2048]{1,0:T(8,128)(2,1)} custom-call(bf16[512,2048]{1,0:T(8,128)(2,1)} %shard_map.118.source), custom_call_target="tpu_custom_call" | custom-call | tf_op jit(solution)/shard_map/pallas_call | solution.py:759
